TPU v7x, 32 devices: a whole 2x2x4 slice. The times are simulated.
32 devices in a mesh: ep: 8 (over z, y), tp: 4 (over x, core).
Axes of the slice: x: 2, y: 2, z: 4, core: 2. Of those that a mesh axis runs over, the one named last changes fastest.
Arguments:
- queries: bfloat16 [1536, 2048], P('ep', 'tp'), may hold values from -8 to 8
- keys: bfloat16 [1536, 512], P('ep', 'tp'), may hold values from -8 to 8
- values: bfloat16 [1536, 512], P('ep', 'tp'), may hold values from -6 to 6
- query_gain: float32 [2048], P('tp'), may hold values from 0.5 to 6
- key_gain: float32 [512], P('tp'), may hold values from 0.7 to 6
- out_weight: bfloat16 [2048, 4096], P('tp'), may hold values from -0.125 to 0.125
- expert_input: bfloat16 [2048, 4096], P(('ep', 'tp')), may hold values from -6 to 6
- norm_gain: float32 [4096], replicated, may hold values from 0.1 to 1.9
- routes: int32 [2048, 2], P(('ep', 'tp')), may hold values from 0 to 7, all different within a row; in each aligned block of 64 rows (0 to 63, 64 to 127, ...) at most 32 rows name the same one
- route_weight: float32 [2048, 2], P(('ep', 'tp')), may hold values from 0.2 to 2
- gate_weight: bfloat16 [8, 4096, 1024], P('ep', None, 'tp'), may hold values from -0.09375 to 0.09375
- up_weight: bfloat16 [8, 4096, 1024], P('ep', None, 'tp'), may hold values from -0.09375 to 0.09375
- down_weight: bfloat16 [8, 1024, 4096], P('ep', 'tp'), may hold values from -0.1875 to 0.1875
Outputs:
- mixed: bfloat16 [1536, 4096], P(('ep', 'tp'))
- moe_out: bfloat16 [2048, 4096], P(('ep', 'tp'))
Inputs may be any that keep to these rules, and one draw needn't show every extreme that they name: `routes`: each row names 2 different experts; in the rows of one device no expert is named by more than 32 rows, and in some device one expert is named by exactly 32 rows.
All inputs are finite; a program needn't handle non-finite values.
Results may differ from a plain program's by a relative error of at most 0.013.
The roundings to bfloat16 on the way count: a program that leaves them out, or rounds other values in their place, can miss the bound.
Values may be sent and summed in bfloat16 or wider, within the bound.
A program may use at most 128 MiB of HBM per device.

v0:
```python
import functools

import jax
import jax.numpy as jnp
from jax import lax
from jax.experimental import pallas as pl
from jax.experimental.pallas import tpu as pltpu
from jax.sharding import PartitionSpec as P

HEAD_DIM = 64
GRID_W = 128


NORM_EPS = 1e-06
ROPE_BASE = 10000.0


def rotate(vectors, grid_rows, grid_cols):
    quarter = vectors.shape[-1] // 4
    inverse = ROPE_BASE ** (-jnp.arange(quarter, dtype=jnp.float32) / quarter)
    angle_row = grid_rows[:, None] * inverse
    angle_col = grid_cols[:, None] * inverse
    angles = jnp.concatenate([angle_row, angle_row, angle_col, angle_col], axis=-1)[:, None, :]
    part_one, part_two, part_three, part_four = jnp.split(vectors, 4, axis=-1)
    turned = jnp.concatenate([-part_two, part_one, -part_four, part_three], axis=-1)
    return vectors * jnp.cos(angles) + turned * jnp.sin(angles)


def head_norm(raw_rows, gains, head_count, offset):
    row_count = raw_rows.shape[0]
    flat_rows = raw_rows.astype(jnp.float32).reshape(row_count, head_count, -1)
    unit_vec = flat_rows * lax.rsqrt(
        jnp.mean(flat_rows * flat_rows, axis=-1, keepdims=True) + NORM_EPS
    )
    unit_vec = unit_vec * gains.reshape(head_count, -1)
    places = offset + jnp.arange(row_count, dtype=jnp.int32)
    grid_rows = (places // GRID_W).astype(jnp.float32)
    grid_cols = (places % GRID_W).astype(jnp.float32)
    return rotate(unit_vec, grid_rows, grid_cols).astype(jnp.bfloat16).reshape(row_count, -1)


def absorb(running, key_block, value_block, grouped, score_scale):
    run_max, weight_sum, summed = running
    kv_count = grouped.shape[1]
    key_heads = key_block.reshape(key_block.shape[0], kv_count, -1)
    value_heads = value_block.reshape(value_block.shape[0], kv_count, -1)
    scores = (
        jnp.einsum("qhgd,khd->hgqk", grouped, key_heads, preferred_element_type=jnp.float32)
        * score_scale
    )
    new_max = jnp.maximum(run_max, jnp.max(scores, axis=-1))
    rescale = jnp.exp(run_max - new_max)
    weights = jnp.exp(scores - new_max[..., None])
    weight_sum = weight_sum * rescale + jnp.sum(weights, axis=-1)
    update = jnp.einsum(
        "hgqk,khd->qhgd",
        weights.astype(jnp.bfloat16),
        value_heads,
        preferred_element_type=jnp.float32,
    )
    summed = summed * jnp.transpose(rescale, (2, 0, 1))[..., None] + update
    return (new_max, weight_sum, summed)


def run_experts(sending, gate_weight, up_weight, down_weight):
    arrived = lax.all_to_all(sending, "ep", split_axis=0, concat_axis=0, tiled=True)
    shard_rows = lax.all_gather(arrived, "tp", axis=0, tiled=True)
    gate_out = jnp.dot(shard_rows, gate_weight[0], preferred_element_type=jnp.float32)
    up_out = jnp.dot(shard_rows, up_weight[0], preferred_element_type=jnp.float32)
    hidden = (jax.nn.silu(gate_out) * up_out).astype(jnp.bfloat16)
    results = lax.psum_scatter(
        jnp.dot(hidden, down_weight[0], preferred_element_type=jnp.float32).astype(jnp.bfloat16),
        "tp",
        scatter_dimension=0,
        tiled=True,
    )
    return lax.all_to_all(results, "ep", split_axis=0, concat_axis=0, tiled=True)


MESH = pl.DeviceIdType.MESH
TILE = 1024


def flip(index, pattern, size):
    result = 0
    bit = 1
    while bit < size:
        both = lax.rem(lax.div(index, bit) + lax.div(pattern, bit), 2)
        result = result + both * bit
        bit = bit * 2
    return result


def fused_kernel(
    n,
    laid,
    q_ref,
    kv_ref,
    wg_hbm,
    wu_hbm,
    wd_hbm,
    ow_hbm,
    back,
    mixed,
    wg,
    wu,
    wd,
    ow,
    rows,
    partial,
    red,
    q_send,
    x_got,
    y_send,
    kv_all,
    attended,
    m_part,
    m_red,
    m_send,
    m_got,
    load_sem,
    kv_sems,
    disp_sems,
    fwd_sems,
    red_sems,
    ret_sems,
    mix_sems,
):
    e = lax.axis_index("ep")
    t = lax.axis_index("tp")
    side = lax.div(t, 2)
    core = lax.rem(t, 2)
    other_side = 1 - side
    other_core = 1 - core
    x_peer = (e, other_side * 2 + core)
    c_peer = (e, side * 2 + other_core)
    cap, width = laid.shape[1], laid.shape[2]
    pairs = attended.shape[0]
    tok = attended.shape[1]

    def remote(src, dst, send, recv, device):
        return pltpu.make_async_remote_copy(
            src_ref=src, dst_ref=dst, send_sem=send, recv_sem=recv, device_id=device, device_id_type=MESH
        )

    loads = [
        pltpu.make_async_copy(a, b, load_sem.at[k])
        for k, (a, b) in enumerate([(ow_hbm, ow), (wg_hbm, wg), (wu_hbm, wu), (wd_hbm, wd)])
    ]
    for load in loads:
        load.start()

    barrier = pltpu.get_barrier_semaphore()
    for s in range(1, n):
        pl.semaphore_signal(barrier, inc=1, device_id=(flip(e, s, n), t), device_id_type=MESH)
    pl.semaphore_signal(barrier, inc=1, device_id=x_peer, device_id_type=MESH)
    pl.semaphore_signal(barrier, inc=1, device_id=c_peer, device_id_type=MESH)
    pl.semaphore_wait(barrier, n + 1)

    def kv_direct(s):
        return remote(kv_ref, kv_all.at[:, e], kv_sems.at[0, s], kv_sems.at[1, s], (flip(e, s, n), t))

    def kv_direct_in(s):
        return remote(kv_ref, kv_all.at[:, flip(e, s, n)], kv_sems.at[0, s], kv_sems.at[1, s], (flip(e, s, n), t))

    def kv_relay(s):
        owner = flip(e, s, n)
        return remote(kv_all.at[:, owner], kv_all.at[:, owner], kv_sems.at[0, s + 1], kv_sems.at[1, s + 1], (flip(e, 1, n), t))

    def kv_relay_in(s):
        owner = flip(e, s + 1, n)
        return remote(kv_all.at[:, owner], kv_all.at[:, owner], kv_sems.at[0, s + 1], kv_sems.at[1, s + 1], (flip(e, 1, n), t))

    order = [0, 1] + sorted(range(2, n), key=lambda s: (s < 4, s % 2, -s))

    def pattern(i):
        chosen = order[0]
        for place in range(1, n):
            chosen = jnp.where(i == place, order[place], chosen)
        return chosen

    def dispatch(i):
        s = pattern(i)
        return remote(laid.at[flip(e, s, n)], rows.at[e, t], disp_sems.at[0, i], disp_sems.at[1, i], (flip(e, s, n), t))

    def dispatch_in(i):
        s = pattern(i)
        return remote(laid.at[flip(e, s, n)], rows.at[flip(e, s, n), t], disp_sems.at[0, i], disp_sems.at[1, i], (flip(e, s, n), t))

    def owner_of(i):
        return flip(e, pattern(i), n)

    def to_side(i):
        o = owner_of(i)
        return remote(rows.at[o, t], rows.at[o, t], fwd_sems.at[0, 0, i], fwd_sems.at[1, 0, i], x_peer)

    def from_side(i):
        o = owner_of(i)
        return remote(rows.at[o, t], rows.at[o, other_side * 2 + core], fwd_sems.at[0, 0, i], fwd_sems.at[1, 0, i], x_peer)

    def to_core(i):
        o = owner_of(i)
        return remote(rows.at[o, t], rows.at[o, t], fwd_sems.at[0, 1, i], fwd_sems.at[1, 1, i], c_peer)

    def from_core(i):
        o = owner_of(i)
        return remote(rows.at[o, t], rows.at[o, side * 2 + other_core], fwd_sems.at[0, 1, i], fwd_sems.at[1, 1, i], c_peer)

    def relay_core(i):
        o = owner_of(i)
        slot = other_side * 2 + core
        return remote(rows.at[o, slot], rows.at[o, slot], fwd_sems.at[0, 2, i], fwd_sems.at[1, 2, i], c_peer)

    def relayed_core(i):
        o = owner_of(i)
        slot = other_side * 2 + core
        return remote(rows.at[o, slot], rows.at[o, other_side * 2 + other_core], fwd_sems.at[0, 2, i], fwd_sems.at[1, 2, i], c_peer)

    def reduce_core(i):
        return remote(partial.at[i, :, other_core], red.at[i], red_sems.at[0, 0, i], red_sems.at[1, 0, i], c_peer)

    def reduce_side(i):
        return remote(q_send.at[i], x_got.at[i], red_sems.at[0, 1, i], red_sems.at[1, 1, i], x_peer)

    def give_back(i):
        o = owner_of(i)
        return remote(y_send.at[i], back.at[e], ret_sems.at[0, i], ret_sems.at[1, i], (o, t))

    def get_back(i):
        o = owner_of(i)
        return remote(y_send.at[i], back.at[o], ret_sems.at[0, i], ret_sems.at[1, i], (o, t))

    mix_core = remote(m_part.at[:, other_core], m_red, mix_sems.at[0, 0], mix_sems.at[1, 0], c_peer)
    mix_side = remote(m_send, m_got, mix_sems.at[0, 1], mix_sems.at[1, 1], x_peer)

    own = pltpu.make_async_copy(laid.at[e], rows.at[e, t], load_sem.at[4])
    own_kv = pltpu.make_async_copy(kv_ref, kv_all.at[:, e], load_sem.at[5])
    own.start()
    own_kv.start()
    for i in range(1, n):
        if i == 8:
            for s in range(2, n, 2):
                kv_direct(s).start()
            kv_direct(1).start()
        dispatch(i).start()
    for s in range(2, n, 2):
        kv_direct(s).start()
    kv_direct(1).start()
    own.wait()
    to_side(0).start()
    to_core(0).start()
    own_kv.wait()

    def attend(pair):
        kv = kv_all[lax.div(pair * 2 * kv_all.shape[0], pairs * 2)].reshape(n * tok, 128)
        halves = []
        for h in range(2):
            scores = lax.dot_general(
                q_ref[pair * 2 + h], kv, (((1,), (1,)), ((), ())), preferred_element_type=jnp.float32
            ) * (HEAD_DIM ** (-0.5))
            peak = jnp.max(scores, axis=1, keepdims=True)
            weights = jnp.exp(scores - peak)
            total = jnp.sum(weights, axis=1, keepdims=True)
            summed = jnp.dot(weights.astype(jnp.bfloat16), kv, preferred_element_type=jnp.float32)
            halves.append(summed / total)
        lane = lax.broadcasted_iota(jnp.int32, halves[0].shape, 1)
        joined = jnp.where(lane < HEAD_DIM, pltpu.roll(halves[0], HEAD_DIM, 1), halves[1])
        attended[pair] = joined.astype(jnp.bfloat16)

    def f32(value):
        return value.astype(jnp.float32)

    def step(i, carry):
        @pl.when(jnp.logical_and(i > 0, i < n))
        def _():
            dispatch_in(i).wait_recv()
            to_side(i).start()
            to_core(i).start()

        @pl.when(i == 6)
        def _():
            for s in range(2, n, 2):
                kv_direct_in(s).wait_recv()
                kv_relay(s).start()

        @pl.when(jnp.logical_and(i >= 1, i <= n))
        def _():
            from_side(i - 1).wait_recv()
            relay_core(i - 1).start()

        @pl.when(i == 7)
        def _():
            kv_direct_in(1).wait_recv()
            for s in range(2, n, 2):
                kv_relay_in(s).wait_recv()

        @pl.when(jnp.logical_and(i >= 7, i < 7 + pairs // 2))
        def _():
            attend(2 * (i - 7))
            attend(2 * (i - 7) + 1)

        @pl.when(i == 7 + pairs // 2)
        def _():
            loads[0].wait()
            for tile in range(0, width, TILE):
                product = jnp.dot(attended[0], ow[0, :, tile:tile + TILE], preferred_element_type=jnp.float32)
                for p in range(1, pairs):
                    product += jnp.dot(attended[p], ow[p, :, tile:tile + TILE], preferred_element_type=jnp.float32)
                m_part[:, :, :, tile:tile + TILE] = product.astype(jnp.bfloat16).reshape(2, 2, tok // 4, TILE)
            mix_core.start()

        @pl.when(jnp.logical_and(i >= 1, i <= n))
        def _():
            k = i - 1

            @pl.when(k == 0)
            def _():
                for load in loads[1:]:
                    load.wait()

            from_core(k).wait_recv()
            relayed_core(k).wait_recv()
            tokens = rows[owner_of(k)].reshape(4 * cap, width)
            gate = jnp.dot(tokens, wg[...], preferred_element_type=jnp.float32)
            up = jnp.dot(tokens, wu[...], preferred_element_type=jnp.float32)
            hidden = (gate / (1.0 + jnp.exp(-gate)) * up).astype(jnp.bfloat16)
            for tile in range(0, width, TILE):
                product = jnp.dot(hidden, wd[:, tile:tile + TILE], preferred_element_type=jnp.float32)
                partial[k, :, :, :, tile:tile + TILE] = product.astype(jnp.bfloat16).reshape(2, 2, cap, TILE)
            reduce_core(k).start()

        @pl.when(i == 7 + pairs // 2)
        def _():
            mix_core.wait_recv()
            m_send[...] = (f32(m_part[other_side, core]) + f32(m_red[other_side])).astype(jnp.bfloat16)
            mix_side.start()

        @pl.when(jnp.logical_and(i >= 2, i < n + 2))
        def _():
            k = i - 2
            reduce_side(k).wait_recv()
            y = (f32(partial[k, side, core]) + f32(red[k, side]) + f32(x_got[k])).astype(jnp.bfloat16)

            @pl.when(k == 0)
            def _():
                back[e] = y

            @pl.when(k > 0)
            def _():
                y_send[k] = y
                give_back(k).start()

        @pl.when(jnp.logical_and(i >= 1, i <= n))
        def _():
            k = i - 1
            reduce_core(k).wait_recv()
            q_send[k] = (f32(partial[k, other_side, core]) + f32(red[k, other_side])).astype(jnp.bfloat16)
            reduce_side(k).start()

        return carry

    lax.fori_loop(0, n + 2, step, 0)

    mix_side.wait_recv()
    mixed[...] = (f32(m_part[side, core]) + f32(m_red[side]) + f32(m_got[...])).astype(jnp.bfloat16)
    mix_core.wait_send()
    mix_side.wait_send()
    for s in range(2, n, 2):
        kv_direct(s).wait_send()
        kv_relay(s).wait_send()
    kv_direct(1).wait_send()

    def drain(i, carry):
        @pl.when(i > 0)
        def _():
            dispatch(i).wait_send()
            give_back(i).wait_send()
            get_back(i).wait_recv()

        to_side(i).wait_send()
        to_core(i).wait_send()
        relay_core(i).wait_send()
        reduce_core(i).wait_send()
        reduce_side(i).wait_send()
        return carry

    lax.fori_loop(0, n, drain, 0)


def fused(laid, q_heads, kv_pack, gate_weight, up_weight, down_weight, out_weight):
    n, cap, width = laid.shape
    heads, tok, _ = q_heads.shape
    kv_count = kv_pack.shape[0]
    pairs = heads // 2
    hidden = gate_weight.shape[1]
    bf = jnp.bfloat16
    vmem = pl.BlockSpec(memory_space=pltpu.VMEM)
    anywhere = pl.BlockSpec(memory_space=pl.ANY)
    dma = pltpu.SemaphoreType.DMA
    return pl.pallas_call(
        functools.partial(fused_kernel, n),
        out_shape=(
            jax.ShapeDtypeStruct((n, cap, width), bf),
            jax.ShapeDtypeStruct((tok // 4, width), bf),
        ),
        in_specs=[vmem] * 3 + [anywhere] * 4,
        out_specs=(vmem, vmem),
        scratch_shapes=[
            pltpu.VMEM((width, hidden), bf),
            pltpu.VMEM((width, hidden), bf),
            pltpu.VMEM((hidden, width), bf),
            pltpu.VMEM((pairs, 128, width), bf),
            pltpu.VMEM((n, 4, cap, width), bf),
            pltpu.VMEM((n, 2, 2, cap, width), bf),
            pltpu.VMEM((n, 2, cap, width), bf),
            pltpu.VMEM((n, cap, width), bf),
            pltpu.VMEM((n, cap, width), bf),
            pltpu.VMEM((n, cap, width), bf),
            pltpu.VMEM((kv_count, n, tok, 128), bf),
            pltpu.VMEM((pairs, tok, 128), bf),
            pltpu.VMEM((2, 2, tok // 4, width), bf),
            pltpu.VMEM((2, tok // 4, width), bf),
            pltpu.VMEM((tok // 4, width), bf),
            pltpu.VMEM((tok // 4, width), bf),
            dma((6,)),
            dma((2, n)),
            dma((2, n)),
            dma((2, 3, n)),
            dma((2, 2, n)),
            dma((2, n)),
            dma((2, 2)),
        ],
        compiler_params=pltpu.CompilerParams(
            collective_id=0, has_side_effects=True, vmem_limit_bytes=62 * 1024 * 1024
        ),
    )(laid, q_heads, kv_pack, gate_weight, up_weight, down_weight, out_weight.reshape(pairs, 128, width))


def plain_shards(
    queries,
    keys,
    values,
    query_gain,
    key_gain,
    out_weight,
    expert_input,
    norm_gain,
    routes,
    route_weight,
    gate_weight,
    up_weight,
    down_weight,
):
    tok_mix = queries.shape[0]
    head_count = query_gain.shape[0] // HEAD_DIM
    kv_count = key_gain.shape[0] // HEAD_DIM
    group_size = head_count // kv_count
    offset = lax.axis_index("ep") * tok_mix
    q_turned = head_norm(queries, query_gain, head_count, offset)
    k_turned = head_norm(keys, key_gain, kv_count, offset)
    grouped = q_turned.reshape(tok_mix, kv_count, group_size, HEAD_DIM)
    score_scale = HEAD_DIM ** (-0.5)
    start_state = (
        jnp.full((kv_count, group_size, tok_mix), -jnp.inf, jnp.float32),
        jnp.zeros((kv_count, group_size, tok_mix), jnp.float32),
        jnp.zeros((tok_mix, kv_count, group_size, HEAD_DIM), jnp.float32),
    )
    running = start_state
    key_piece = lax.all_gather(k_turned, "ep", axis=0, tiled=True)
    value_piece = lax.all_gather(values, "ep", axis=0, tiled=True)
    length = key_piece.shape[0]
    block_len = length
    while block_len > 2048 and block_len % 2 == 0:
        block_len = block_len // 2
    key_blocks = key_piece.reshape(length // block_len, block_len, key_piece.shape[1])
    value_blocks = value_piece.reshape(length // block_len, block_len, value_piece.shape[1])

    def advance(inner_state, key_value):
        return (absorb(inner_state, key_value[0], key_value[1], grouped, score_scale), None)

    running, unused = lax.scan(advance, running, (key_blocks, value_blocks))
    final_max, weight_sum, summed = running
    attended = (
        (summed / jnp.transpose(weight_sum, (2, 0, 1))[..., None])
        .reshape(tok_mix, -1)
        .astype(jnp.bfloat16)
    )
    mixed = lax.psum_scatter(
        jnp.dot(attended, out_weight, preferred_element_type=jnp.float32).astype(jnp.bfloat16),
        "tp",
        scatter_dimension=0,
        tiled=True,
    )
    tok_exp = expert_input.shape[0]
    top_count = routes.shape[1]
    expert_count = lax.axis_size("ep")
    capacity = 2 * top_count * tok_exp // expert_count
    as_float = expert_input.astype(jnp.float32)
    normed = (
        as_float
        * lax.rsqrt(jnp.mean(as_float * as_float, axis=-1, keepdims=True) + NORM_EPS)
        * norm_gain
    ).astype(jnp.bfloat16)
    flat_routes = routes.reshape(-1)
    route_hits = (
        flat_routes[:, None] == jnp.arange(expert_count, dtype=jnp.int32)[None, :]
    ).astype(jnp.int32)
    slot_rank = jnp.sum((jnp.cumsum(route_hits, axis=0) - route_hits) * route_hits, axis=1)
    slot_ids = flat_routes * capacity + slot_rank
    placed = jnp.arange(expert_count * capacity, dtype=jnp.int32)[:, None] == slot_ids[None, :]
    placed = jnp.any(placed.reshape(expert_count * capacity, tok_exp, top_count), axis=2).astype(
        jnp.bfloat16
    )
    outbound = jnp.dot(placed, normed, preferred_element_type=jnp.float32).astype(jnp.bfloat16)
    model_width = outbound.shape[1]
    half_cap = capacity // 2
    laid = outbound.reshape(expert_count, capacity, model_width)
    first_half = run_experts(
        laid[:, :half_cap].reshape(expert_count * half_cap, model_width),
        gate_weight,
        up_weight,
        down_weight,
    )
    second_half = run_experts(
        laid[:, half_cap:].reshape(expert_count * half_cap, model_width),
        gate_weight,
        up_weight,
        down_weight,
    )
    back_rows = jnp.concatenate(
        [
            first_half.reshape(expert_count, half_cap, model_width),
            second_half.reshape(expert_count, half_cap, model_width),
        ],
        axis=1,
    )
    back_rows = back_rows.reshape(expert_count * capacity, model_width)
    picked = back_rows[slot_ids.reshape(tok_exp, top_count)]
    moe_out = jnp.sum(picked.astype(jnp.float32) * route_weight[:, :, None], axis=1).astype(
        jnp.bfloat16
    )
    return (mixed, moe_out)


def shards(
    queries,
    keys,
    values,
    query_gain,
    key_gain,
    out_weight,
    expert_input,
    norm_gain,
    routes,
    route_weight,
    gate_weight,
    up_weight,
    down_weight,
):
    tok_exp, model_width = expert_input.shape
    top_count = routes.shape[1]
    expert_count = lax.axis_size("ep")
    capacity = 2 * top_count * tok_exp // expert_count
    if capacity % 16 != 0 or lax.axis_size("tp") != 4:
        return plain_shards(
            queries,
            keys,
            values,
            query_gain,
            key_gain,
            out_weight,
            expert_input,
            norm_gain,
            routes,
            route_weight,
            gate_weight,
            up_weight,
            down_weight,
        )
    tok_mix = queries.shape[0]
    head_count = query_gain.shape[0] // HEAD_DIM
    kv_count = key_gain.shape[0] // HEAD_DIM
    offset = lax.axis_index("ep") * tok_mix
    q_turned = head_norm(queries, query_gain, head_count, offset)
    k_turned = head_norm(keys, key_gain, kv_count, offset)
    q_heads = jnp.transpose(q_turned.reshape(tok_mix, head_count, HEAD_DIM), (1, 0, 2))
    q_heads = jnp.pad(q_heads, ((0, 0), (0, 0), (0, HEAD_DIM)))
    kv_pack = jnp.concatenate(
        [k_turned.reshape(tok_mix, kv_count, HEAD_DIM), values.reshape(tok_mix, kv_count, HEAD_DIM)],
        axis=-1,
    )
    kv_pack = jnp.transpose(kv_pack, (1, 0, 2))
    as_float = expert_input.astype(jnp.float32)
    normed = (
        as_float
        * lax.rsqrt(jnp.mean(as_float * as_float, axis=-1, keepdims=True) + NORM_EPS)
        * norm_gain
    ).astype(jnp.bfloat16)
    flat_routes = routes.reshape(-1)
    route_hits = (
        flat_routes[:, None] == jnp.arange(expert_count, dtype=jnp.int32)[None, :]
    ).astype(jnp.int32)
    slot_rank = jnp.sum((jnp.cumsum(route_hits, axis=0) - route_hits) * route_hits, axis=1)
    slot_ids = (flat_routes * capacity + slot_rank).reshape(tok_exp, top_count)
    slots = jnp.arange(expert_count * capacity, dtype=jnp.int32)
    placed = jnp.any(slots[:, None, None] == slot_ids[None], axis=2).astype(jnp.bfloat16)
    outbound = jnp.dot(placed, normed, preferred_element_type=jnp.float32).astype(jnp.bfloat16)
    back_rows, mixed = fused(
        outbound.reshape(expert_count, capacity, model_width),
        q_heads,
        kv_pack,
        gate_weight[0],
        up_weight[0],
        down_weight[0],
        out_weight,
    )
    back_rows = back_rows.reshape(expert_count * capacity, model_width)
    moe_sum = jnp.zeros((tok_exp, model_width), jnp.float32)
    for k in range(top_count):
        chosen = (slot_ids[:, k, None] == slots[None, :]).astype(jnp.bfloat16)
        picked = jnp.dot(chosen, back_rows, preferred_element_type=jnp.float32)
        moe_sum = moe_sum + picked * route_weight[:, k, None]
    return (mixed, moe_sum.astype(jnp.bfloat16))


def solution(mesh):
    placed = (
        P("ep", "tp"),
        P("ep", "tp"),
        P("ep", "tp"),
        P("tp"),
        P("tp"),
        P("tp", None),
        P(("ep", "tp"), None),
        P(),
        P(("ep", "tp"), None),
        P(("ep", "tp"), None),
        P("ep", None, "tp"),
        P("ep", None, "tp"),
        P("ep", "tp", None),
    )
    return jax.shard_map(
        shards,
        mesh=mesh,
        in_specs=placed,
        out_specs=(P(("ep", "tp"), None), P(("ep", "tp"), None)),
        check_vma=False,
    )
```

profile of v0, /device:TPU:0, one launch (start us, length us, event | category | flops | bytes accessed | tf_op | source)
XLA Modules:
  0.0 141.3 jit_solution(12294142639285014405)
XLA Ops:
  0.6 1.1 copy.39
  1.7 0.2 copy.40
  1.9 0.1 multiply_reduce_fusion
  2.0 0.8 mul.189
  2.7 0.3 multiply_multiply_fusion
  3.0 1.5 %slice_negate_fusion.1 = (f32[192,8,16]{2,0,1:T(8,128)S(1)}, f32[192,8,16]{2,0,1:T(8,128)S(1)}, f32[192,8,16]{2,0,1:T(8,128)S(1)}, f32[192,8,16]{2,0,1:T(8,128)}) fusion(f32[192,8,64]{2,0,1:T(8,128)S(1)} %multiply_multiply_fusion), kind=kLoop, calls=%fused_computation.11 | loop fusion | flops 49152 | bytes 786432 | tf_op jit(solution)/shard_map/neg | solution.py:25
  4.6 0.1 broadcast_multiply_fusion.1
  4.7 0.5 fusion.18
  5.2 2.0 %fusion.10 = bf16[8,192,64]{2,1,0:T(8,128)(2,1)S(1)} fusion(f32[192,64]{1,0:T(8,128)S(1)} %get-tuple-element.15, f32[192,8,16]{2,0,1:T(8,128)S(1)} %get-tuple-element.7, f32[192,8,16]{2,0,1:T(8,128)S(1)} %get-tuple-element.8, f32[192,8,16]{2,0,1:T(8,128)} %get-tuple-element.9, f32[192,8,16]{2,0,1:T(8,128)S(1)} %get-tuple-element.6, ...), kind=kLoop, calls=%fused_computation.19 | loop fusion | flops 884736 | bytes 1089536 | tf_op jit(solution)/shard_map/transpose | solution.py:586
  7.2 0.8 pad.4.q_ref
  8.1 0.1 copy.41
  8.2 0.1 copy.42
  8.4 0.1 mul.205
  8.4 0.1 multiply_multiply_fusion.1
  8.6 0.2 slice_negate_fusion.3
  8.8 0.3 fusion.12
  9.1 0.1 copy.43
  9.2 0.1 copy.44
  9.3 0.7 maximum_bitcast_fusion.kv_ref
  10.1 0.1 copy.37
  10.2 0.1 eq.62
  10.3 0.1 fusion.14
  10.4 0.2 reduce_window_sum.11
  10.6 0.2 select_reduce_fusion
  10.8 0.1 reduce_sum.39
  11.0 0.1 fusion.13
  11.1 0.2 fusion.2
  11.3 2.1 %convolution_convert_fusion = bf16[256,4096]{1,0:T(8,128)(2,1)} fusion(pred[256,64]{0,1:T(8,128)(4,1)S(1)} %fusion.13, bf16[64,4096]{1,0:T(8,128)(2,1)S(1)} %copy-done.1, f32[4096]{0:T(1024)S(1)} %copy-done.5, f32[64]{0:T(128)S(1)} %add_rsqrt_fusion.2), kind=kOutput, calls=%fused_computation | convolution fusion | flops 136314880 | bytes 2654464 | tf_op jit(solution)/shard_map/dot_general | solution.py:607
  13.5 123.4 %shard_map.140 = (bf16[8,32,4096]{2,1,0:T(8,128)(2,1)}, bf16[48,4096]{1,0:T(8,128)(2,1)}) custom-call(bf16[8,32,4096]{2,1,0:T(8,128)(2,1)} %bitcast.28, bf16[8,192,128]{2,1,0:T(8,128)(2,1)} %pad.4.q_ref, bf16[2,192,128]{2,1,0:T(8,128)(2,1)} %maximum_bitcast_fusion.kv_ref, bf16[4096,256]{1,0:T(8,128)(2,1)} %bitcast.33, bf16[4096,256]{1,0:T(8,128)(2,1)} %bitcast.34, ...), custom_call_target="tpu_custom_call" | custom-call | tf_op jit(solution)/shard_map/pallas_call | solution.py:400
  136.9 2.3 %convolution_multiply_fusion.1 = f32[64,4096]{1,0:T(8,128)S(1)} fusion(bf16[256,4096]{1,0:T(8,128)(2,1)} %bitcast.29, f32[64]{0:T(128)S(1)} %get-tuple-element.19, s32[64]{0:T(128)S(1)} %get-tuple-element.17), kind=kOutput, calls=%fused_computation.3 | convolution fusion | flops 134496256 | bytes 3146240 | tf_op jit(solution)/shard_map/dot_general | solution.py:621
  139.2 1.3 fusion.1
  140.5 0.7 copy.46
  (28 shorter events, 0.2 us)
Async XLA Ops:
  5.2 2.9 %copy-start.3 = (bf16[192,128]{1,0:T(8,128)(2,1)S(1)}, bf16[192,128]{1,0:T(8,128)(2,1)}, u32[]{:S(2)}) copy-start(bf16[192,128]{1,0:T(8,128)(2,1)} %param.14) | copy-start | bytes 147460
  5.2 3.2 %copy-start.8 = (f32[128]{0:T(128)S(1)}, f32[128]{0:T(128)}, u32[]{:S(2)}) copy-start(f32[128]{0:T(128)} %param.17) | copy-start | bytes 1540
  7.2 1.9 %copy-start.4 = (bf16[192,128]{1,0:T(8,128)(2,1)S(1)}, bf16[192,128]{1,0:T(8,128)(2,1)}, u32[]{:S(2)}) copy-start(bf16[192,128]{1,0:T(8,128)(2,1)} %param.15) | copy-start | bytes 147460
  8.2 1.9 %copy-start.6 = (s32[64,2]{0,1:T(2,128)S(1)}, s32[64,2]{0,1:T(2,128)}, u32[]{:S(2)}) copy-start(s32[64,2]{0,1:T(2,128)} %param.21) | copy-start | bytes 1540
  8.4 2.7 %copy-start.1 = (bf16[64,4096]{1,0:T(8,128)(2,1)S(1)}, bf16[64,4096]{1,0:T(8,128)(2,1)}, u32[]{:S(2)}) copy-start(bf16[64,4096]{1,0:T(8,128)(2,1)} %param.19) | copy-start | bytes 1572868
  8.6 2.8 %copy-start.5 = (f32[4096]{0:T(1024)S(1)}, f32[4096]{0:T(1024)}, u32[]{:S(2)}) copy-start(f32[4096]{0:T(1024)} %param.20) | copy-start | bytes 49156
  13.5 123.4 %copy-start.7 = (f32[64,2]{0,1:T(2,128)S(1)}, f32[64,2]{0,1:T(2,128)}, u32[]{:S(2)}) copy-start(f32[64,2]{0,1:T(2,128)} %param.22) | copy-start | bytes 1540
  136.9 2.3 %copy-start = (bf16[8,32,4096]{2,1,0:T(8,128)(2,1)S(1)}, bf16[8,32,4096]{2,1,0:T(8,128)(2,1)}, u32[]{:S(2)}) copy-start(bf16[8,32,4096]{2,1,0:T(8,128)(2,1)} %get-tuple-element.5) | copy-start | bytes 6291460
  139.2 1.3 copy-start.2
where the time goes:
time: 141 us
  Pallas kernels  123 us (87%)
  other arithmetic  6.7 us (5%)
  matrix products  5.71 us (4%)
  local copies, waits for them, and re-layouts  4.57 us (3%)
    pallas_call x1, Pallas kernels, fused(): pl.pallas_call(functools.partial(fused_kernel, n), out_shape=(jax.ShapeDt...  123 us
    dot_general x2, matrix products, shards(): picked = jnp.dot(chosen, back_rows, preferred_element_type=jnp.float32)  3.58 us

commit v1 on v0

--- a/solution.py
+++ b/solution.py
@@ -2,6 +2,7 @@
 
 import jax
 import jax.numpy as jnp
+import numpy as np
 from jax import lax
 from jax.experimental import pallas as pl
 from jax.experimental.pallas import tpu as pltpu
@@ -93,15 +94,29 @@
 
 def fused_kernel(
     n,
-    laid,
-    q_ref,
-    kv_ref,
+    x_ref,
+    x_gain,
+    routes_row,
+    routes_col,
+    weight_col,
+    q_raw,
+    k_raw,
+    v_raw,
+    q_gain,
+    k_gain,
+    turn_hbm,
     wg_hbm,
     wu_hbm,
     wd_hbm,
     ow_hbm,
+    moe,
+    mixed,
+    laid,
     back,
-    mixed,
+    total,
+    q_ref,
+    kv_ref,
+    turn,
     wg,
     wu,
     wd,
@@ -145,7 +160,15 @@
 
     loads = [
         pltpu.make_async_copy(a, b, load_sem.at[k])
-        for k, (a, b) in enumerate([(ow_hbm, ow), (wg_hbm, wg), (wu_hbm, wu), (wd_hbm, wd)])
+        for k, (a, b) in enumerate(
+            [
+                (ow_hbm, ow),
+                (wg_hbm, wg),
+                (wu_hbm, wu),
+                (wd_hbm, wd),
+                (turn_hbm.at[pl.ds(pl.multiple_of(e * tok, 8), tok)], turn),
+            ]
+        )
     ]
     for load in loads:
         load.start()
@@ -155,6 +178,39 @@
         pl.semaphore_signal(barrier, inc=1, device_id=(flip(e, s, n), t), device_id_type=MESH)
     pl.semaphore_signal(barrier, inc=1, device_id=x_peer, device_id_type=MESH)
     pl.semaphore_signal(barrier, inc=1, device_id=c_peer, device_id_type=MESH)
+
+    tokens_here = x_ref.shape[0]
+    as_float = x_ref[...].astype(jnp.float32)
+    mean = jnp.mean(as_float * as_float, axis=1, keepdims=True)
+    normed = (as_float * lax.rsqrt(mean + NORM_EPS) * x_gain[...]).astype(jnp.bfloat16)
+    row_id = lax.broadcasted_iota(jnp.int32, (tokens_here, tokens_here), 0)
+    col_id = lax.broadcasted_iota(jnp.int32, (tokens_here, tokens_here), 1)
+    before = (row_id < col_id).astype(jnp.bfloat16)
+    after = (col_id < row_id).astype(jnp.bfloat16)
+
+    def place(expert):
+        hit = jnp.logical_or(routes_row[0:1] == expert, routes_row[1:2] == expert)
+        spread = jnp.broadcast_to(hit.astype(jnp.float32), (cap, tokens_here))
+        rank = jnp.dot(spread.astype(jnp.bfloat16), before, preferred_element_type=jnp.float32)
+        slot = lax.broadcasted_iota(jnp.int32, rank.shape, 0).astype(jnp.float32)
+        return (jnp.where(rank == slot, 1.0, 0.0) * spread).astype(jnp.bfloat16)
+
+    def pick(expert):
+        hits = [(routes_col[:, k:k + 1] == expert).astype(jnp.float32) for k in range(routes_col.shape[1])]
+        scale = sum(hit * weight_col[:, k:k + 1] for k, hit in enumerate(hits))
+        spread = jnp.broadcast_to(sum(hits), (tokens_here, cap))
+        rank = jnp.dot(after, spread.astype(jnp.bfloat16), preferred_element_type=jnp.float32)
+        slot = lax.broadcasted_iota(jnp.int32, rank.shape, 1).astype(jnp.float32)
+        return (jnp.where(rank == slot, 1.0, 0.0) * spread).astype(jnp.bfloat16), scale
+
+    def lay(expert):
+        chosen = place(expert)
+        for tile in range(0, width, TILE):
+            laid[expert, :, tile:tile + TILE] = jnp.dot(
+                chosen, normed[:, tile:tile + TILE], preferred_element_type=jnp.float32
+            ).astype(jnp.bfloat16)
+
+    lay(e)
     pl.semaphore_wait(barrier, n + 1)
 
     def kv_direct(s):
@@ -233,22 +289,53 @@
     mix_core = remote(m_part.at[:, other_core], m_red, mix_sems.at[0, 0], mix_sems.at[1, 0], c_peer)
     mix_side = remote(m_send, m_got, mix_sems.at[0, 1], mix_sems.at[1, 1], x_peer)
 
-    own = pltpu.make_async_copy(laid.at[e], rows.at[e, t], load_sem.at[4])
-    own_kv = pltpu.make_async_copy(kv_ref, kv_all.at[:, e], load_sem.at[5])
+    own = pltpu.make_async_copy(laid.at[e], rows.at[e, t], load_sem.at[5])
+    own_kv = pltpu.make_async_copy(kv_ref, kv_all.at[:, e], load_sem.at[6])
     own.start()
+    for i in range(1, n):
+        lay(flip(e, order[i], n))
+        dispatch(i).start()
+    own.wait()
+    to_side(0).start()
+    to_core(0).start()
+
+    loads[4].wait()
+    lane = lax.broadcasted_iota(jnp.int32, (tok, 128), 1)
+    low = lane < HEAD_DIM
+    even = lax.rem(lax.div(lane, HEAD_DIM // 4), 2) == 0
+    table = turn[...]
+    swapped = pltpu.roll(table, HEAD_DIM, 1)
+    cosine = jnp.where(low, table, swapped)
+    sine = jnp.where(low, swapped, table)
+
+    def turned(raw, gain):
+        flat = raw.astype(jnp.float32)
+        square = flat * flat
+        left = jnp.sum(jnp.where(low, square, 0.0), axis=1, keepdims=True)
+        right = jnp.sum(jnp.where(low, 0.0, square), axis=1, keepdims=True)
+        mean_square = jnp.where(low, left, right) * (1.0 / HEAD_DIM)
+        unit = flat * lax.rsqrt(mean_square + NORM_EPS) * gain
+        partner = jnp.where(
+            even, -pltpu.roll(unit, 128 - HEAD_DIM // 4, 1), pltpu.roll(unit, HEAD_DIM // 4, 1)
+        )
+        return unit * cosine + partner * sine
+
+    for pair in range(kv_ref.shape[0] // 2):
+        span = slice(pair * 128, (pair + 1) * 128)
+        k_rows = turned(k_raw[:, span], k_gain[:, span])
+        v_rows = v_raw[:, span].astype(jnp.float32)
+        kv_ref[2 * pair] = jnp.where(low, k_rows, pltpu.roll(v_rows, HEAD_DIM, 1)).astype(jnp.bfloat16)
+        kv_ref[2 * pair + 1] = jnp.where(low, pltpu.roll(k_rows, HEAD_DIM, 1), v_rows).astype(jnp.bfloat16)
     own_kv.start()
-    for i in range(1, n):
-        if i == 8:
-            for s in range(2, n, 2):
-                kv_direct(s).start()
-            kv_direct(1).start()
-        dispatch(i).start()
     for s in range(2, n, 2):
         kv_direct(s).start()
     kv_direct(1).start()
-    own.wait()
-    to_side(0).start()
-    to_core(0).start()
+
+    for pair in range(pairs):
+        span = slice(pair * 128, (pair + 1) * 128)
+        q_rows = turned(q_raw[:, span], q_gain[:, span])
+        q_ref[2 * pair] = jnp.where(low, q_rows, 0.0).astype(jnp.bfloat16)
+        q_ref[2 * pair + 1] = jnp.where(low, pltpu.roll(q_rows, HEAD_DIM, 1), 0.0).astype(jnp.bfloat16)
     own_kv.wait()
 
     def attend(pair):
@@ -263,12 +350,18 @@
             total = jnp.sum(weights, axis=1, keepdims=True)
             summed = jnp.dot(weights.astype(jnp.bfloat16), kv, preferred_element_type=jnp.float32)
             halves.append(summed / total)
-        lane = lax.broadcasted_iota(jnp.int32, halves[0].shape, 1)
-        joined = jnp.where(lane < HEAD_DIM, pltpu.roll(halves[0], HEAD_DIM, 1), halves[1])
+        joined = jnp.where(low, pltpu.roll(halves[0], HEAD_DIM, 1), halves[1])
         attended[pair] = joined.astype(jnp.bfloat16)
 
     def f32(value):
         return value.astype(jnp.float32)
+
+    def gather(expert, first):
+        chosen, scale = pick(expert)
+        for tile in range(0, width, TILE):
+            span = slice(tile, tile + TILE)
+            found = jnp.dot(chosen, back[expert, :, span], preferred_element_type=jnp.float32) * scale
+            total[:, span] = found if first else total[:, span] + found
 
     def step(i, carry):
         @pl.when(jnp.logical_and(i > 0, i < n))
@@ -315,7 +408,7 @@
 
             @pl.when(k == 0)
             def _():
-                for load in loads[1:]:
+                for load in loads[1:4]:
                     load.wait()
 
             from_core(k).wait_recv()
@@ -344,6 +437,7 @@
             @pl.when(k == 0)
             def _():
                 back[e] = y
+                gather(e, True)
 
             @pl.when(k > 0)
             def _():
@@ -357,9 +451,16 @@
             q_send[k] = (f32(partial[k, other_side, core]) + f32(red[k, other_side])).astype(jnp.bfloat16)
             reduce_side(k).start()
 
+        @pl.when(i >= 5)
+        def _():
+            k = i - 4
+            get_back(k).wait_recv()
+            gather(owner_of(k), False)
+
         return carry
 
-    lax.fori_loop(0, n + 2, step, 0)
+    lax.fori_loop(0, n + 4, step, 0)
+    moe[...] = total[...].astype(jnp.bfloat16)
 
     mix_side.wait_recv()
     mixed[...] = (f32(m_part[side, core]) + f32(m_red[side]) + f32(m_got[...])).astype(jnp.bfloat16)
@@ -375,7 +476,6 @@
         def _():
             dispatch(i).wait_send()
             give_back(i).wait_send()
-            get_back(i).wait_recv()
 
         to_side(i).wait_send()
         to_core(i).wait_send()
@@ -387,10 +487,23 @@
     lax.fori_loop(0, n, drain, 0)
 
 
-def fused(laid, q_heads, kv_pack, gate_weight, up_weight, down_weight, out_weight):
-    n, cap, width = laid.shape
-    heads, tok, _ = q_heads.shape
-    kv_count = kv_pack.shape[0]
+def turn_table(tokens):
+    quarter = HEAD_DIM // 4
+    inverse = np.power(ROPE_BASE, -np.arange(quarter, dtype=np.float64) / quarter)
+    places = np.arange(tokens)
+    row = (places // GRID_W)[:, None] * inverse
+    col = (places % GRID_W)[:, None] * inverse
+    angles = np.concatenate([row, row, col, col], axis=1)
+    return np.concatenate([np.cos(angles), np.sin(angles)], axis=1).astype(np.float32)
+
+
+def fused(x, x_gain, routes, route_weight, queries, keys, values, q_gain, k_gain, gate_weight, up_weight, down_weight, out_weight):
+    n = lax.axis_size("ep")
+    tok_exp, width = x.shape
+    cap = 2 * routes.shape[1] * tok_exp // n
+    tok = queries.shape[0]
+    heads = queries.shape[1] // HEAD_DIM
+    kv_count = keys.shape[1] // HEAD_DIM
     pairs = heads // 2
     hidden = gate_weight.shape[1]
     bf = jnp.bfloat16
@@ -400,12 +513,18 @@
     return pl.pallas_call(
         functools.partial(fused_kernel, n),
         out_shape=(
-            jax.ShapeDtypeStruct((n, cap, width), bf),
+            jax.ShapeDtypeStruct((tok_exp, width), bf),
             jax.ShapeDtypeStruct((tok // 4, width), bf),
         ),
-        in_specs=[vmem] * 3 + [anywhere] * 4,
+        in_specs=[vmem] * 10 + [anywhere] * 5,
         out_specs=(vmem, vmem),
         scratch_shapes=[
+            pltpu.VMEM((n, cap, width), bf),
+            pltpu.VMEM((n, cap, width), bf),
+            pltpu.VMEM((tok_exp, width), jnp.float32),
+            pltpu.VMEM((heads, tok, 128), bf),
+            pltpu.VMEM((kv_count, tok, 128), bf),
+            pltpu.VMEM((tok, 128), jnp.float32),
             pltpu.VMEM((width, hidden), bf),
             pltpu.VMEM((width, hidden), bf),
             pltpu.VMEM((hidden, width), bf),
@@ -422,7 +541,7 @@
             pltpu.VMEM((2, tok // 4, width), bf),
             pltpu.VMEM((tok // 4, width), bf),
             pltpu.VMEM((tok // 4, width), bf),
-            dma((6,)),
+            dma((7,)),
             dma((2, n)),
             dma((2, n)),
             dma((2, 3, n)),
@@ -433,7 +552,23 @@
         compiler_params=pltpu.CompilerParams(
             collective_id=0, has_side_effects=True, vmem_limit_bytes=62 * 1024 * 1024
         ),
-    )(laid, q_heads, kv_pack, gate_weight, up_weight, down_weight, out_weight.reshape(pairs, 128, width))
+    )(
+        x,
+        x_gain.reshape(1, width),
+        jnp.transpose(routes),
+        routes,
+        route_weight,
+        queries,
+        keys,
+        values,
+        q_gain.reshape(1, -1),
+        k_gain.reshape(1, -1),
+        jnp.asarray(turn_table(n * tok)),
+        gate_weight,
+        up_weight,
+        down_weight,
+        out_weight.reshape(pairs, 128, width),
+    )
 
 
 def plain_shards(
@@ -557,7 +692,7 @@
     up_weight,
     down_weight,
 ):
-    tok_exp, model_width = expert_input.shape
+    tok_exp = expert_input.shape[0]
     top_count = routes.shape[1]
     expert_count = lax.axis_size("ep")
     capacity = 2 * top_count * tok_exp // expert_count
@@ -577,50 +712,22 @@
             up_weight,
             down_weight,
         )
-    tok_mix = queries.shape[0]
-    head_count = query_gain.shape[0] // HEAD_DIM
-    kv_count = key_gain.shape[0] // HEAD_DIM
-    offset = lax.axis_index("ep") * tok_mix
-    q_turned = head_norm(queries, query_gain, head_count, offset)
-    k_turned = head_norm(keys, key_gain, kv_count, offset)
-    q_heads = jnp.transpose(q_turned.reshape(tok_mix, head_count, HEAD_DIM), (1, 0, 2))
-    q_heads = jnp.pad(q_heads, ((0, 0), (0, 0), (0, HEAD_DIM)))
-    kv_pack = jnp.concatenate(
-        [k_turned.reshape(tok_mix, kv_count, HEAD_DIM), values.reshape(tok_mix, kv_count, HEAD_DIM)],
-        axis=-1,
-    )
-    kv_pack = jnp.transpose(kv_pack, (1, 0, 2))
-    as_float = expert_input.astype(jnp.float32)
-    normed = (
-        as_float
-        * lax.rsqrt(jnp.mean(as_float * as_float, axis=-1, keepdims=True) + NORM_EPS)
-        * norm_gain
-    ).astype(jnp.bfloat16)
-    flat_routes = routes.reshape(-1)
-    route_hits = (
-        flat_routes[:, None] == jnp.arange(expert_count, dtype=jnp.int32)[None, :]
-    ).astype(jnp.int32)
-    slot_rank = jnp.sum((jnp.cumsum(route_hits, axis=0) - route_hits) * route_hits, axis=1)
-    slot_ids = (flat_routes * capacity + slot_rank).reshape(tok_exp, top_count)
-    slots = jnp.arange(expert_count * capacity, dtype=jnp.int32)
-    placed = jnp.any(slots[:, None, None] == slot_ids[None], axis=2).astype(jnp.bfloat16)
-    outbound = jnp.dot(placed, normed, preferred_element_type=jnp.float32).astype(jnp.bfloat16)
-    back_rows, mixed = fused(
-        outbound.reshape(expert_count, capacity, model_width),
-        q_heads,
-        kv_pack,
+    moe_out, mixed = fused(
+        expert_input,
+        norm_gain,
+        routes,
+        route_weight,
+        queries,
+        keys,
+        values,
+        query_gain,
+        key_gain,
         gate_weight[0],
         up_weight[0],
         down_weight[0],
         out_weight,
     )
-    back_rows = back_rows.reshape(expert_count * capacity, model_width)
-    moe_sum = jnp.zeros((tok_exp, model_width), jnp.float32)
-    for k in range(top_count):
-        chosen = (slot_ids[:, k, None] == slots[None, :]).astype(jnp.bfloat16)
-        picked = jnp.dot(chosen, back_rows, preferred_element_type=jnp.float32)
-        moe_sum = moe_sum + picked * route_weight[:, k, None]
-    return (mixed, moe_sum.astype(jnp.bfloat16))
+    return (mixed, moe_out)
 
 
 def solution(mesh):

time: 141 us -> 132 us (0.936)
  other arithmetic: 6.7 us -> 0 us
  matrix products: 5.71 us -> 0 us
  Pallas kernels: 123 us -> 125 us
  local copies, waits for them, and re-layouts: 4.57 us -> 6.4 us
    dot_general x3 -> x0, matrix products: 5.71 us -> none  [the longest x2 3.58 us: shards(): picked = jnp.dot(chosen, back_rows, preferred_element_type=jnp.float32)]
    unnamed x23 -> x4, local copies, waits for them, and re-layouts: 2.16 us -> 6.4 us
    transpose x2 -> x0, other arithmetic: 2.78 us -> none  [the longest x1 2.04 us: shards(): jnp.transpose(q_turned.reshape(tok_mix, head_count, HEAD_DIM), (1, 0, 2))]
    neg x2 -> x0, other arithmetic: 1.76 us -> none  [rotate(): -part_two]
where the time goes in v1:
time: 132 us
  Pallas kernels  125 us (95%)
  local copies, waits for them, and re-layouts  6.4 us (5%)
    pallas_call x1, Pallas kernels, fused(): pl.pallas_call(functools.partial(fused_kernel, n), out_shape=(jax.ShapeDt...  125 us
    unnamed x4, local copies, waits for them, and re-layouts  6.4 us

profile of v1, /device:TPU:0, one launch (start us, length us, event | category | flops | bytes accessed | tf_op | source)
XLA Modules:
  0.0 131.6 jit_solution(15085323199095249059)
XLA Ops:
  0.6 1.4 %copy.17.weight_col = f32[64,2]{1,0:T(8,128)} copy(f32[64,2]{0,1:T(2,128)} %param.23) | data formatting | bytes 1024 | tf_op args[9]
  2.0 1.4 %copy.16.routes_col = s32[64,2]{1,0:T(8,128)} copy(s32[64,2]{0,1:T(2,128)} %param.22) | data formatting | bytes 1024 | tf_op args[8]
  3.4 124.5 %shard_map.149 = (bf16[64,4096]{1,0:T(8,128)(2,1)}, bf16[48,4096]{1,0:T(8,128)(2,1)}) custom-call(bf16[64,4096]{1,0:T(8,128)(2,1)} %x_ref.1, f32[1,4096]{1,0:T(1,128)} %bitcast.12, s32[2,64]{1,0:T(2,128)} %bitcast.13, s32[64,2]{1,0:T(8,128)} %copy.16.routes_col, f32[64,2]{1,0:T(8,128)} %copy.17.weight_col, bf16[192,512]{1,0:T(8,128)(2,1)} %q_raw.1, ...), custom_call_target="tpu_custom_call" | custom-call | tf_op jit(solution)/shard_map/pallas_call | solution.py:513
  127.9 1.8 %copy.20 = bf16[48,4096]{1,0:T(8,128)(2,1)} copy(bf16[48,4096]{1,0:T(8,128)(2,1)} %get-tuple-element.8) | data formatting | bytes 786432
  129.7 1.9 %copy.21 = bf16[64,4096]{1,0:T(8,128)(2,1)} copy(bf16[64,4096]{1,0:T(8,128)(2,1)} %get-tuple-element.9) | data formatting | bytes 1048576

commit v2 on v1

v2 whole, which is shorter than its diff:
```python
import functools

import jax
import jax.numpy as jnp
import numpy as np
from jax import lax
from jax.experimental import pallas as pl
from jax.experimental.pallas import tpu as pltpu
from jax.sharding import PartitionSpec as P

HEAD_DIM = 64
GRID_W = 128


NORM_EPS = 1e-06
ROPE_BASE = 10000.0


def rotate(vectors, grid_rows, grid_cols):
    quarter = vectors.shape[-1] // 4
    inverse = ROPE_BASE ** (-jnp.arange(quarter, dtype=jnp.float32) / quarter)
    angle_row = grid_rows[:, None] * inverse
    angle_col = grid_cols[:, None] * inverse
    angles = jnp.concatenate([angle_row, angle_row, angle_col, angle_col], axis=-1)[:, None, :]
    part_one, part_two, part_three, part_four = jnp.split(vectors, 4, axis=-1)
    turned = jnp.concatenate([-part_two, part_one, -part_four, part_three], axis=-1)
    return vectors * jnp.cos(angles) + turned * jnp.sin(angles)


def head_norm(raw_rows, gains, head_count, offset):
    row_count = raw_rows.shape[0]
    flat_rows = raw_rows.astype(jnp.float32).reshape(row_count, head_count, -1)
    unit_vec = flat_rows * lax.rsqrt(
        jnp.mean(flat_rows * flat_rows, axis=-1, keepdims=True) + NORM_EPS
    )
    unit_vec = unit_vec * gains.reshape(head_count, -1)
    places = offset + jnp.arange(row_count, dtype=jnp.int32)
    grid_rows = (places // GRID_W).astype(jnp.float32)
    grid_cols = (places % GRID_W).astype(jnp.float32)
    return rotate(unit_vec, grid_rows, grid_cols).astype(jnp.bfloat16).reshape(row_count, -1)


def absorb(running, key_block, value_block, grouped, score_scale):
    run_max, weight_sum, summed = running
    kv_count = grouped.shape[1]
    key_heads = key_block.reshape(key_block.shape[0], kv_count, -1)
    value_heads = value_block.reshape(value_block.shape[0], kv_count, -1)
    scores = (
        jnp.einsum("qhgd,khd->hgqk", grouped, key_heads, preferred_element_type=jnp.float32)
        * score_scale
    )
    new_max = jnp.maximum(run_max, jnp.max(scores, axis=-1))
    rescale = jnp.exp(run_max - new_max)
    weights = jnp.exp(scores - new_max[..., None])
    weight_sum = weight_sum * rescale + jnp.sum(weights, axis=-1)
    update = jnp.einsum(
        "hgqk,khd->qhgd",
        weights.astype(jnp.bfloat16),
        value_heads,
        preferred_element_type=jnp.float32,
    )
    summed = summed * jnp.transpose(rescale, (2, 0, 1))[..., None] + update
    return (new_max, weight_sum, summed)


def run_experts(sending, gate_weight, up_weight, down_weight):
    arrived = lax.all_to_all(sending, "ep", split_axis=0, concat_axis=0, tiled=True)
    shard_rows = lax.all_gather(arrived, "tp", axis=0, tiled=True)
    gate_out = jnp.dot(shard_rows, gate_weight[0], preferred_element_type=jnp.float32)
    up_out = jnp.dot(shard_rows, up_weight[0], preferred_element_type=jnp.float32)
    hidden = (jax.nn.silu(gate_out) * up_out).astype(jnp.bfloat16)
    results = lax.psum_scatter(
        jnp.dot(hidden, down_weight[0], preferred_element_type=jnp.float32).astype(jnp.bfloat16),
        "tp",
        scatter_dimension=0,
        tiled=True,
    )
    return lax.all_to_all(results, "ep", split_axis=0, concat_axis=0, tiled=True)


MESH = pl.DeviceIdType.MESH
TILE = 1024
CHUNKS = 2


def flip(index, pattern, size):
    result = 0
    bit = 1
    while bit < size:
        both = lax.rem(lax.div(index, bit) + lax.div(pattern, bit), 2)
        result = result + both * bit
        bit = bit * 2
    return result


def f32(value):
    return value.astype(jnp.float32)


ORDER = (0, 1, 4, 6, 5, 2, 7, 3)


def fused_kernel(
    n,
    x_ref,
    x_gain,
    routes_row,
    weight_row,
    q_raw,
    k_raw,
    v_raw,
    q_gain,
    k_gain,
    turn_hbm,
    wg_hbm,
    wu_hbm,
    wd_hbm,
    ow_hbm,
    moe,
    mixed,
    dense,
    meta,
    rows,
    y_send,
    partial,
    red,
    x_got,
    y_got,
    hold,
    sent,
    z_got,
    m_got,
    p_got,
    o_got,
    q_ref,
    kv_ref,
    turn,
    wg,
    wu,
    wd,
    ow,
    kv_all,
    attended,
    a_part,
    a_red,
    a_send,
    a_got,
    load_sem,
    kv_sems,
    dn_out,
    dn_in,
    meta_sems,
    row_y,
    row_c,
    row_x,
    red_sems,
    sum_x,
    sum_y,
    t_out,
    z_in,
    m_in,
    p_in,
    o_in,
    mix_sems,
):
    e = lax.axis_index("ep")
    t = lax.axis_index("tp")
    side = lax.div(t, 2)
    core = lax.rem(t, 2)
    other_side = 1 - side
    other_core = 1 - core
    layer = lax.div(e, 2)
    y = lax.rem(e, 2)
    other_y = 1 - y
    near = layer + 1 - 2 * lax.rem(layer, 2)
    last = n // 2 - 1
    across = last - layer
    inner = jnp.logical_and(layer > 0, layer < last)
    outer = jnp.logical_not(inner)
    half = lax.div(layer, 2)
    far_inner = 2 - half
    far_outer = last * (1 - half)
    x_tp = other_side * 2 + core
    x_peer = (e, x_tp)
    c_peer = (e, side * 2 + other_core)
    y_expert = layer * 2 + other_y
    y_peer = (y_expert, t)
    z_peer = (near * 2 + y, t)
    m_peer = (across * 2 + y, t)
    corner = (near * 2 + y, x_tp)
    cap, width = rows.shape[3], rows.shape[4]
    pairs = attended.shape[0]
    tok = attended.shape[1]
    tokens_here = x_ref.shape[0]
    chunks = dn_in.shape[1]
    part = width // chunks

    def remote(src, dst, send, recv, device):
        return pltpu.make_async_remote_copy(
            src_ref=src, dst_ref=dst, send_sem=send, recv_sem=recv, device_id=device, device_id_type=MESH
        )

    def cols(c):
        return pl.ds(c * part, part)

    loads = [
        pltpu.make_async_copy(a, b, load_sem.at[k])
        for k, (a, b) in enumerate(
            [
                (turn_hbm.at[pl.ds(pl.multiple_of(e * tok, 8), tok)], turn),
                (wg_hbm, wg),
                (wu_hbm, wu),
                (wd_hbm, wd),
                (ow_hbm, ow),
            ]
        )
    ]
    for load in loads:
        load.start()

    barrier = pltpu.get_barrier_semaphore()
    for s in range(1, n):
        pl.semaphore_signal(barrier, inc=1, device_id=(flip(e, s, n), t), device_id_type=MESH)
    for peer in (x_peer, c_peer, corner):
        pl.semaphore_signal(barrier, inc=1, device_id=peer, device_id_type=MESH)

    def kv_direct(s):
        return remote(kv_ref, kv_all.at[:, e], kv_sems.at[0, s], kv_sems.at[1, s], (flip(e, s, n), t))

    def kv_direct_in(s):
        return remote(kv_ref, kv_all.at[:, flip(e, s, n)], kv_sems.at[0, s], kv_sems.at[1, s], (flip(e, s, n), t))

    def kv_relay(s):
        owner = flip(e, s, n)
        return remote(kv_all.at[:, owner], kv_all.at[:, owner], kv_sems.at[0, s + 1], kv_sems.at[1, s + 1], (flip(e, 1, n), t))

    def kv_relay_in(s):
        owner = flip(e, s + 1, n)
        return remote(kv_all.at[:, owner], kv_all.at[:, owner], kv_sems.at[0, s + 1], kv_sems.at[1, s + 1], (flip(e, 1, n), t))

    own_kv = pltpu.make_async_copy(kv_ref, kv_all.at[:, e], load_sem.at[5])

    def block(source, target, number, c, device):
        return remote(
            dense.at[source, :, cols(c)],
            dense.at[target, :, cols(c)],
            dn_out.at[number, c],
            dn_in.at[target, c],
            device,
        )

    def to_x(c):
        return block(0, 1, 1, c, x_peer)

    def to_near(c):
        return block(0, 2, 2, c, z_peer)

    def x_to_near(c):
        return block(1, 3, 3, c, z_peer)

    def to_across(c):
        return block(0, 4, 4, c, m_peer)

    def near_to_across(c):
        return block(2, 5, 5, c, m_peer)

    def far_to_near(k, c):
        return block(4 + k, 4 + k, 6 + k, c, z_peer)

    def arrived(slot, c):
        block(slot, slot, 0, c, x_peer).wait_recv()

    far_slot = jnp.where(inner, 4, 5)

    def card(slot, number, device):
        return remote(meta.at[0], meta.at[slot], meta_sems.at[0, number], meta_sems.at[1, slot], device)

    cards = [
        card(1, 1, x_peer),
        card(2, 2, z_peer),
        card(3, 3, corner),
        card(far_slot, 4, (far_inner * 2 + y, t)),
        card(far_slot, 5, (far_outer * 2 + y, t)),
    ]

    def row_to_y(b):
        return remote(y_send.at[b], rows.at[b, core, y], row_y.at[0, b], row_y.at[1, b], y_peer)

    def row_from_y(b):
        return remote(y_send.at[b], rows.at[b, core, other_y], row_y.at[0, b], row_y.at[1, b], y_peer)

    def row_to_c(b, g):
        return remote(rows.at[b, core, g], rows.at[b, core, g], row_c.at[0, b, g], row_c.at[1, b, g], c_peer)

    def row_from_c(b, g):
        return remote(rows.at[b, core, g], rows.at[b, other_core, g], row_c.at[0, b, g], row_c.at[1, b, g], c_peer)

    def row_to_x(k, g):
        return remote(rows.at[4 + k, core, g], rows.at[6 + k, core, g], row_x.at[0, k, g], row_x.at[1, k, g], x_peer)

    def reduce_c(b):
        return remote(partial.at[b, other_core], red.at[b], red_sems.at[0, b], red_sems.at[1, b], c_peer)

    def reduce_x(k):
        return remote(partial.at[6 + k, core], x_got.at[k], sum_x.at[0, k], sum_x.at[1, k], x_peer)

    def give_y(b):
        return remote(partial.at[b, core, other_y], y_got.at[b], sum_y.at[0, b], sum_y.at[1, b], y_peer)

    def pass_on(b, place, where, arrive, c, device):
        return remote(sent.at[b, :, cols(c)], where.at[place, :, cols(c)], t_out.at[b, c], arrive.at[place, c], device)

    mix_core = remote(a_part.at[:, other_core], a_red, mix_sems.at[0, 0], mix_sems.at[1, 0], c_peer)
    mix_side = remote(a_send, a_got, mix_sems.at[0, 1], mix_sems.at[1, 1], x_peer)

    row_id = lax.broadcasted_iota(jnp.int32, (tokens_here, tokens_here), 0)
    col_id = lax.broadcasted_iota(jnp.int32, (tokens_here, tokens_here), 1)
    before = (row_id < col_id).astype(jnp.bfloat16)
    after = (col_id < row_id).astype(jnp.bfloat16)

    def tiles(size, body):
        def run(j, carry):
            body(pl.ds(pl.multiple_of(j * size, size), size))
            return carry

        lax.fori_loop(0, width // size, run, 0)

    def select(b):
        named = meta[b]
        spread = []
        for expert in (e, y_expert):
            wanted = expert.astype(jnp.float32)
            hit = jnp.logical_or(named[0:1] == wanted, named[1:2] == wanted)
            spread.append(jnp.broadcast_to(hit.astype(jnp.float32)[:, :tokens_here], (cap, tokens_here)))
        spread = jnp.concatenate(spread, axis=0)
        rank = jnp.dot(spread.astype(jnp.bfloat16), before, preferred_element_type=jnp.float32)
        slot = f32(lax.rem(lax.broadcasted_iota(jnp.int32, rank.shape, 0), cap))
        chosen = (jnp.where(rank == slot, 1.0, 0.0) * spread).astype(jnp.bfloat16)

        def body(span):
            found = jnp.dot(chosen, dense[b, :, span], preferred_element_type=jnp.float32).astype(jnp.bfloat16)
            rows[b, core, y, :, span] = found[:cap]
            y_send[b, :, span] = found[cap:]

        tiles(512, body)
        row_to_y(b).start()
        row_to_c(b, y).start()
        if b >= 4:
            row_to_x(b - 4, y).start()

    def arrive(b):
        if b < 6:
            row_from_y(b).wait_recv()
            if b >= 4:
                row_to_x(b - 4, other_y).start()
            row_to_c(b, other_y).start()
        else:
            for g in (y, other_y):
                remote(
                    rows.at[b - 2, core, g], rows.at[b, core, g], row_x.at[0, b - 6, g], row_x.at[1, b - 6, g], x_peer
                ).wait_recv()
                row_to_c(b, g).start()

    def finish(b):
        reduce_c(b).wait_recv()
        if b in (4, 5):
            reduce_x(b - 4).wait_recv()

        def body(span):
            value = f32(partial[b, core, :, :, span]) + f32(red[b, :, :, span])
            if b in (4, 5):
                value = value + f32(x_got[b - 4, :, :, span])
            partial[b, core, :, :, span] = value.astype(jnp.bfloat16)

        tiles(512, body)
        if b >= 6:
            reduce_x(b - 6).start()
        else:
            give_y(b).start()

    def gather(b):
        remote(partial.at[b, core, other_y], y_got.at[b], sum_y.at[0, b], sum_y.at[1, b], y_peer).wait_recv()
        turned_meta = jnp.transpose(meta[b])[:tokens_here]
        parts = []
        for expert in (e, y_expert):
            wanted = expert.astype(jnp.float32)
            hits = [(turned_meta[:, k:k + 1] == wanted).astype(jnp.float32) for k in range(2)]
            scale = hits[0] * turned_meta[:, 2:3] + hits[1] * turned_meta[:, 3:4]
            spread = jnp.broadcast_to(hits[0] + hits[1], (tokens_here, cap))
            rank = jnp.dot(after, spread.astype(jnp.bfloat16), preferred_element_type=jnp.float32)
            slot = f32(lax.broadcasted_iota(jnp.int32, rank.shape, 1))
            parts.append(((jnp.where(rank == slot, 1.0, 0.0) * spread).astype(jnp.bfloat16), scale))

        def body(span):
            mine = jnp.dot(parts[0][0], partial[b, core, y, :, span], preferred_element_type=jnp.float32)
            theirs = jnp.dot(parts[1][0], y_got[b, :, span], preferred_element_type=jnp.float32)
            hold[b, :, span] = mine * parts[0][1] + theirs * parts[1][1]

        tiles(512, body)

    def release(b, sources, place, where, arrive_sem, device):
        for c in range(chunks):
            for got, at, sem in sources:
                remote(got.at[at, :, cols(c)], got.at[at, :, cols(c)], t_out.at[0, c], sem.at[at, c], device).wait_recv()

            def run(j, carry):
                span = pl.ds(pl.multiple_of(c * part + j * 512, 512), 512)
                value = hold[b, :, span]
                for got, at, sem in sources:
                    value = value + f32(got[at, :, span])
                sent[b, :, span] = value.astype(jnp.bfloat16)
                return carry

            lax.fori_loop(0, part // 512, run, 0)
            pass_on(b, place, where, arrive_sem, c, device).start()

    as_float = f32(x_ref[...])
    mean = jnp.mean(as_float * as_float, axis=1, keepdims=True)
    dense[0] = (as_float * lax.rsqrt(mean + NORM_EPS) * x_gain[...]).astype(jnp.bfloat16)
    meta[0] = jnp.zeros(meta.shape[1:], jnp.float32)
    meta[0, 0:2, 0:tokens_here] = f32(routes_row[...])
    meta[0, 2:4, 0:tokens_here] = weight_row[...]

    pl.semaphore_wait(barrier, n + 2)
    for item in cards:
        item.start()
    for c in range(chunks):
        to_x(c).start()

        @pl.when(inner)
        def _():
            to_across(c).start()

        if c == 0:
            to_near(c).start()
        else:
            @pl.when(outer)
            def _():
                to_near(c).start()

    select(0)

    loads[0].wait()
    lane = lax.broadcasted_iota(jnp.int32, (tok, 128), 1)
    low = lane < HEAD_DIM
    even = lax.rem(lax.div(lane, HEAD_DIM // 4), 2) == 0
    table = turn[...]
    swapped = pltpu.roll(table, HEAD_DIM, 1)
    cosine = jnp.where(low, table, swapped)
    sine = jnp.where(low, swapped, table)

    def turned(raw, gain):
        flat = f32(raw)
        square = flat * flat
        left = jnp.sum(jnp.where(low, square, 0.0), axis=1, keepdims=True)
        right = jnp.sum(jnp.where(low, 0.0, square), axis=1, keepdims=True)
        mean_square = jnp.where(low, left, right) * (1.0 / HEAD_DIM)
        unit = flat * lax.rsqrt(mean_square + NORM_EPS) * gain
        partner = jnp.where(
            even, -pltpu.roll(unit, 128 - HEAD_DIM // 4, 1), pltpu.roll(unit, HEAD_DIM // 4, 1)
        )
        return unit * cosine + partner * sine

    for pair in range(kv_ref.shape[0] // 2):
        span = slice(pair * 128, (pair + 1) * 128)
        k_rows = turned(k_raw[:, span], k_gain[:, span])
        v_rows = f32(v_raw[:, span])
        kv_ref[2 * pair] = jnp.where(low, k_rows, pltpu.roll(v_rows, HEAD_DIM, 1)).astype(jnp.bfloat16)
        kv_ref[2 * pair + 1] = jnp.where(low, pltpu.roll(k_rows, HEAD_DIM, 1), v_rows).astype(jnp.bfloat16)
    own_kv.start()
    for s in range(2, n, 2):
        kv_direct(s).start()
    kv_direct(1).start()

    for pair in range(pairs):
        span = slice(pair * 128, (pair + 1) * 128)
        q_rows = turned(q_raw[:, span], q_gain[:, span])
        q_ref[2 * pair] = jnp.where(low, q_rows, 0.0).astype(jnp.bfloat16)
        q_ref[2 * pair + 1] = jnp.where(low, pltpu.roll(q_rows, HEAD_DIM, 1), 0.0).astype(jnp.bfloat16)
    own_kv.wait()

    for slot in range(1, 6):
        remote(meta.at[0], meta.at[slot], meta_sems.at[0, 0], meta_sems.at[1, slot], x_peer).wait_recv()
    for c in range(chunks):
        arrived(1, c)

        @pl.when(outer)
        def _():
            x_to_near(c).start()

        @pl.when(inner)
        def _():
            arrived(4, c)
            far_to_near(0, c).start()
            arrived(2, c)
            near_to_across(c).start()

    select(1)

    def attend(pair):
        kv = kv_all[lax.div(pair * 2 * kv_all.shape[0], pairs * 2)].reshape(n * tok, 128)
        halves = []
        for h in range(2):
            scores = lax.dot_general(
                q_ref[pair * 2 + h], kv, (((1,), (1,)), ((), ())), preferred_element_type=jnp.float32
            ) * (HEAD_DIM ** (-0.5))
            peak = jnp.max(scores, axis=1, keepdims=True)
            weights = jnp.exp(scores - peak)
            total = jnp.sum(weights, axis=1, keepdims=True)
            summed = jnp.dot(weights.astype(jnp.bfloat16), kv, preferred_element_type=jnp.float32)
            halves.append(summed / total)
        joined = jnp.where(low, pltpu.roll(halves[0], HEAD_DIM, 1), halves[1])
        attended[pair] = joined.astype(jnp.bfloat16)

    def mix_product():
        loads[4].wait()
        for tile in range(0, width, TILE):
            product = jnp.dot(attended[0], ow[0, :, tile:tile + TILE], preferred_element_type=jnp.float32)
            for p in range(1, pairs):
                product += jnp.dot(attended[p], ow[p, :, tile:tile + TILE], preferred_element_type=jnp.float32)
            a_part[:, :, :, tile:tile + TILE] = product.astype(jnp.bfloat16).reshape(2, 2, tok // 4, TILE)
        mix_core.start()

    def mix_sum():
        mix_core.wait_recv()
        a_send[...] = (f32(a_part[other_side, core]) + f32(a_red[other_side])).astype(jnp.bfloat16)
        mix_side.start()

    def unit_of(s):
        chosen = ORDER[0]
        for place in range(1, len(ORDER)):
            chosen = jnp.where(s == place, ORDER[place], chosen)
        return chosen

    def step(s, carry):
        u = unit_of(s)

        def at(number):
            return pl.when(s == number)

        @at(1)
        def _():
            @pl.when(inner)
            def _():
                arrived(5, 0)
                far_to_near(1, 0).start()

        for place, b in enumerate(ORDER):
            @at(place)
            def _(b=b):
                arrive(b)

        @at(0)
        def _():
            for load in loads[1:4]:
                load.wait()

        @at(1)
        def _():
            for s2 in range(2, n, 2):
                kv_direct_in(s2).wait_recv()
                kv_relay(s2).start()
            finish(0)

        @at(2)
        def _():
            finish(1)

        @at(3)
        def _():
            gather(0)

        @at(4)
        def _():
            finish(6)
            mix_product()

        @at(5)
        def _():
            mix_sum()
            gather(1)

        @at(6)
        def _():
            finish(4)
            finish(2)

        @at(7)
        def _():
            finish(7)
            gather(4)

            @pl.when(outer)
            def _():
                release(4, [], 0, z_got, z_in, z_peer)

        for g in range(2):
            row_from_c(u, g).wait_recv()
        tokens = rows[u].reshape(4 * cap, width)
        gate = jnp.dot(tokens, wg[...], preferred_element_type=jnp.float32)
        up = jnp.dot(tokens, wu[...], preferred_element_type=jnp.float32)
        hidden = (gate / (1.0 + jnp.exp(-gate)) * up).astype(jnp.bfloat16)
        for tile in range(0, width, TILE):
            product = jnp.dot(hidden, wd[:, tile:tile + TILE], preferred_element_type=jnp.float32)
            partial[u, :, :, :, tile:tile + TILE] = product.astype(jnp.bfloat16).reshape(2, 2, cap, TILE)
        reduce_c(u).start()

        @at(0)
        def _():
            @pl.when(outer)
            def _():
                for c in range(chunks):
                    arrived(4, c)

            select(4)

        @at(1)
        def _():
            @pl.when(inner)
            def _():
                for c in range(1, chunks):
                    arrived(5, c)
                    far_to_near(1, c).start()
                    to_near(c).start()
                for c in range(chunks):
                    x_to_near(c).start()

            kv_direct_in(1).wait_recv()
            for s2 in range(2, n, 2):
                kv_relay_in(s2).wait_recv()

        @pl.when(jnp.logical_or(s == 1, s == 2))
        def _():
            attend(2 * (s - 1))
            attend(2 * (s - 1) + 1)

        @at(2)
        def _():
            @pl.when(outer)
            def _():
                for c in range(chunks):
                    arrived(5, c)

            select(5)

        @at(3)
        def _():
            @pl.when(outer)
            def _():
                for c in range(chunks):
                    arrived(2, c)

            select(2)

        @at(5)
        def _():
            for c in range(chunks):
                arrived(3, c)
            select(3)

        return carry

    lax.fori_loop(0, len(ORDER), step, 0)

    finish(5)
    finish(3)
    gather(2)
    gather(5)

    @pl.when(outer)
    def _():
        release(5, [], 1, z_got, z_in, z_peer)

    @pl.when(inner)
    def _():
        release(4, [(z_got, 0, z_in)], 0, m_got, m_in, m_peer)

    gather(3)
    release(3, [], 1, p_got, p_in, z_peer)

    @pl.when(inner)
    def _():
        release(5, [(z_got, 1, z_in)], 1, m_got, m_in, m_peer)

    mix_side.wait_recv()
    mixed[...] = (f32(a_part[side, core]) + f32(a_red[side]) + f32(a_got[...])).astype(jnp.bfloat16)

    release(1, [(p_got, 1, p_in)], 0, o_got, o_in, x_peer)

    @pl.when(outer)
    def _():
        release(2, [], 0, p_got, p_in, z_peer)

    @pl.when(inner)
    def _():
        release(2, [(m_got, 1, m_in)], 0, p_got, p_in, z_peer)
        for c in range(chunks):
            remote(m_got.at[0, :, cols(c)], m_got.at[0, :, cols(c)], t_out.at[0, c], m_in.at[0, c], m_peer).wait_recv()

        def fold(span):
            hold[0, :, span] = hold[0, :, span] + f32(m_got[0, :, span])

        tiles(512, fold)

    for c in range(chunks):
        for got, sem in ((o_got, o_in), (p_got, p_in)):
            remote(got.at[0, :, cols(c)], got.at[0, :, cols(c)], t_out.at[0, c], sem.at[0, c], x_peer).wait_recv()

        def final(j, carry):
            span = pl.ds(pl.multiple_of(c * part + j * 512, 512), 512)
            value = hold[0, :, span] + f32(o_got[0, :, span]) + f32(p_got[0, :, span])
            moe[:, span] = value.astype(jnp.bfloat16)
            return carry

        lax.fori_loop(0, part // 512, final, 0)

    mix_core.wait_send()
    mix_side.wait_send()
    for s in range(2, n, 2):
        kv_direct(s).wait_send()
        kv_relay(s).wait_send()
    kv_direct(1).wait_send()
    for item in cards:
        item.wait_send()
    for c in range(chunks):
        to_x(c).wait_send()
        to_near(c).wait_send()
        x_to_near(c).wait_send()

        @pl.when(inner)
        def _():
            to_across(c).wait_send()
            near_to_across(c).wait_send()
            far_to_near(0, c).wait_send()
            far_to_near(1, c).wait_send()

        for b in range(1, 6):
            pass_on(b, 0, o_got, o_in, c, x_peer).wait_send()
    for k in range(2):
        for g in range(2):
            row_to_x(k, g).wait_send()
        reduce_x(k).wait_send()
    for b in range(6):
        row_to_y(b).wait_send()
        give_y(b).wait_send()
    for b in range(8):
        for g in range(2):
            row_to_c(b, g).wait_send()
        reduce_c(b).wait_send()


def turn_table(tokens):
    quarter = HEAD_DIM // 4
    inverse = np.power(ROPE_BASE, -np.arange(quarter, dtype=np.float64) / quarter)
    places = np.arange(tokens)
    row = (places // GRID_W)[:, None] * inverse
    col = (places % GRID_W)[:, None] * inverse
    angles = np.concatenate([row, row, col, col], axis=1)
    return np.concatenate([np.cos(angles), np.sin(angles)], axis=1).astype(np.float32)


def fused(x, x_gain, routes, route_weight, queries, keys, values, q_gain, k_gain, gate_weight, up_weight, down_weight, out_weight):
    n = lax.axis_size("ep")
    tok_exp, width = x.shape
    cap = 2 * routes.shape[1] * tok_exp // n
    tok = queries.shape[0]
    heads = queries.shape[1] // HEAD_DIM
    kv_count = keys.shape[1] // HEAD_DIM
    pairs = heads // 2
    hidden = gate_weight.shape[1]
    bf = jnp.bfloat16
    vmem = pl.BlockSpec(memory_space=pltpu.VMEM)
    anywhere = pl.BlockSpec(memory_space=pl.ANY)
    dma = pltpu.SemaphoreType.DMA
    return pl.pallas_call(
        functools.partial(fused_kernel, n),
        out_shape=(
            jax.ShapeDtypeStruct((tok_exp, width), bf),
            jax.ShapeDtypeStruct((tok // 4, width), bf),
        ),
        in_specs=[vmem] * 9 + [anywhere] * 5,
        out_specs=(vmem, vmem),
        scratch_shapes=[
            pltpu.VMEM((6, tok_exp, width), bf),
            pltpu.VMEM((6, 8, 128), jnp.float32),
            pltpu.VMEM((8, 2, 2, cap, width), bf),
            pltpu.VMEM((6, cap, width), bf),
            pltpu.VMEM((8, 2, 2, cap, width), bf),
            pltpu.VMEM((8, 2, cap, width), bf),
            pltpu.VMEM((2, 2, cap, width), bf),
            pltpu.VMEM((6, cap, width), bf),
            pltpu.VMEM((6, tok_exp, width), jnp.float32),
            pltpu.VMEM((6, tok_exp, width), bf),
            pltpu.VMEM((2, tok_exp, width), bf),
            pltpu.VMEM((2, tok_exp, width), bf),
            pltpu.VMEM((2, tok_exp, width), bf),
            pltpu.VMEM((1, tok_exp, width), bf),
            pltpu.VMEM((heads, tok, 128), bf),
            pltpu.VMEM((kv_count, tok, 128), bf),
            pltpu.VMEM((tok, 128), jnp.float32),
            pltpu.VMEM((width, hidden), bf),
            pltpu.VMEM((width, hidden), bf),
            pltpu.VMEM((hidden, width), bf),
            pltpu.VMEM((pairs, 128, width), bf),
            pltpu.VMEM((kv_count, n, tok, 128), bf),
            pltpu.VMEM((pairs, tok, 128), bf),
            pltpu.VMEM((2, 2, tok // 4, width), bf),
            pltpu.VMEM((2, tok // 4, width), bf),
            pltpu.VMEM((tok // 4, width), bf),
            pltpu.VMEM((tok // 4, width), bf),
            dma((6,)),
            dma((2, n)),
            dma((8, CHUNKS)),
            dma((6, CHUNKS)),
            dma((2, 6)),
            dma((2, 6)),
            dma((2, 8, 2)),
            dma((2, 2, 2)),
            dma((2, 8)),
            dma((2, 2)),
            dma((2, 6)),
            dma((6, CHUNKS)),
            dma((2, CHUNKS)),
            dma((2, CHUNKS)),
            dma((2, CHUNKS)),
            dma((1, CHUNKS)),
            dma((2, 2)),
        ],
        compiler_params=pltpu.CompilerParams(
            collective_id=0, has_side_effects=True, vmem_limit_bytes=62 * 1024 * 1024
        ),
    )(
        x,
        x_gain.reshape(1, width),
        jnp.transpose(routes),
        jnp.transpose(route_weight),
        queries,
        keys,
        values,
        q_gain.reshape(1, -1),
        k_gain.reshape(1, -1),
        jnp.asarray(turn_table(n * tok)),
        gate_weight,
        up_weight,
        down_weight,
        out_weight.reshape(pairs, 128, width),
    )


def plain_shards(
    queries,
    keys,
    values,
    query_gain,
    key_gain,
    out_weight,
    expert_input,
    norm_gain,
    routes,
    route_weight,
    gate_weight,
    up_weight,
    down_weight,
):
    tok_mix = queries.shape[0]
    head_count = query_gain.shape[0] // HEAD_DIM
    kv_count = key_gain.shape[0] // HEAD_DIM
    group_size = head_count // kv_count
    offset = lax.axis_index("ep") * tok_mix
    q_turned = head_norm(queries, query_gain, head_count, offset)
    k_turned = head_norm(keys, key_gain, kv_count, offset)
    grouped = q_turned.reshape(tok_mix, kv_count, group_size, HEAD_DIM)
    score_scale = HEAD_DIM ** (-0.5)
    start_state = (
        jnp.full((kv_count, group_size, tok_mix), -jnp.inf, jnp.float32),
        jnp.zeros((kv_count, group_size, tok_mix), jnp.float32),
        jnp.zeros((tok_mix, kv_count, group_size, HEAD_DIM), jnp.float32),
    )
    running = start_state
    key_piece = lax.all_gather(k_turned, "ep", axis=0, tiled=True)
    value_piece = lax.all_gather(values, "ep", axis=0, tiled=True)
    length = key_piece.shape[0]
    block_len = length
    while block_len > 2048 and block_len % 2 == 0:
        block_len = block_len // 2
    key_blocks = key_piece.reshape(length // block_len, block_len, key_piece.shape[1])
    value_blocks = value_piece.reshape(length // block_len, block_len, value_piece.shape[1])

    def advance(inner_state, key_value):
        return (absorb(inner_state, key_value[0], key_value[1], grouped, score_scale), None)

    running, unused = lax.scan(advance, running, (key_blocks, value_blocks))
    final_max, weight_sum, summed = running
    attended = (
        (summed / jnp.transpose(weight_sum, (2, 0, 1))[..., None])
        .reshape(tok_mix, -1)
        .astype(jnp.bfloat16)
    )
    mixed = lax.psum_scatter(
        jnp.dot(attended, out_weight, preferred_element_type=jnp.float32).astype(jnp.bfloat16),
        "tp",
        scatter_dimension=0,
        tiled=True,
    )
    tok_exp = expert_input.shape[0]
    top_count = routes.shape[1]
    expert_count = lax.axis_size("ep")
    capacity = 2 * top_count * tok_exp // expert_count
    as_float = expert_input.astype(jnp.float32)
    normed = (
        as_float
        * lax.rsqrt(jnp.mean(as_float * as_float, axis=-1, keepdims=True) + NORM_EPS)
        * norm_gain
    ).astype(jnp.bfloat16)
    flat_routes = routes.reshape(-1)
    route_hits = (
        flat_routes[:, None] == jnp.arange(expert_count, dtype=jnp.int32)[None, :]
    ).astype(jnp.int32)
    slot_rank = jnp.sum((jnp.cumsum(route_hits, axis=0) - route_hits) * route_hits, axis=1)
    slot_ids = flat_routes * capacity + slot_rank
    placed = jnp.arange(expert_count * capacity, dtype=jnp.int32)[:, None] == slot_ids[None, :]
    placed = jnp.any(placed.reshape(expert_count * capacity, tok_exp, top_count), axis=2).astype(
        jnp.bfloat16
    )
    outbound = jnp.dot(placed, normed, preferred_element_type=jnp.float32).astype(jnp.bfloat16)
    model_width = outbound.shape[1]
    half_cap = capacity // 2
    laid = outbound.reshape(expert_count, capacity, model_width)
    first_half = run_experts(
        laid[:, :half_cap].reshape(expert_count * half_cap, model_width),
        gate_weight,
        up_weight,
        down_weight,
    )
    second_half = run_experts(
        laid[:, half_cap:].reshape(expert_count * half_cap, model_width),
        gate_weight,
        up_weight,
        down_weight,
    )
    back_rows = jnp.concatenate(
        [
            first_half.reshape(expert_count, half_cap, model_width),
            second_half.reshape(expert_count, half_cap, model_width),
        ],
        axis=1,
    )
    back_rows = back_rows.reshape(expert_count * capacity, model_width)
    picked = back_rows[slot_ids.reshape(tok_exp, top_count)]
    moe_out = jnp.sum(picked.astype(jnp.float32) * route_weight[:, :, None], axis=1).astype(
        jnp.bfloat16
    )
    return (mixed, moe_out)


def shards(
    queries,
    keys,
    values,
    query_gain,
    key_gain,
    out_weight,
    expert_input,
    norm_gain,
    routes,
    route_weight,
    gate_weight,
    up_weight,
    down_weight,
):
    tok_exp = expert_input.shape[0]
    top_count = routes.shape[1]
    expert_count = lax.axis_size("ep")
    capacity = 2 * top_count * tok_exp // expert_count
    if capacity % 16 != 0 or lax.axis_size("tp") != 4 or expert_count != 8:
        return plain_shards(
            queries,
            keys,
            values,
            query_gain,
            key_gain,
            out_weight,
            expert_input,
            norm_gain,
            routes,
            route_weight,
            gate_weight,
            up_weight,
            down_weight,
        )
    moe_out, mixed = fused(
        expert_input,
        norm_gain,
        routes,
        route_weight,
        queries,
        keys,
        values,
        query_gain,
        key_gain,
        gate_weight[0],
        up_weight[0],
        down_weight[0],
        out_weight,
    )
    return (mixed, moe_out)


def solution(mesh):
    placed = (
        P("ep", "tp"),
        P("ep", "tp"),
        P("ep", "tp"),
        P("tp"),
        P("tp"),
        P("tp", None),
        P(("ep", "tp"), None),
        P(),
        P(("ep", "tp"), None),
        P(("ep", "tp"), None),
        P("ep", None, "tp"),
        P("ep", None, "tp"),
        P("ep", "tp", None),
    )
    return jax.shard_map(
        shards,
        mesh=mesh,
        in_specs=placed,
        out_specs=(P(("ep", "tp"), None), P(("ep", "tp"), None)),
        check_vma=False,
    )
```

time: 132 us -> 154 us (1.17)
  Pallas kernels: 125 us -> 149 us
  local copies, waits for them, and re-layouts: 6.4 us -> 3.63 us
    pallas_call x1, Pallas kernels: 125 us -> 149 us  [fused(): pl.pallas_call(functools.partial(fused_kernel, n), out_shape=(jax.ShapeDt...]
    unnamed x4 -> x2, local copies, waits for them, and re-layouts: 6.4 us -> 3.63 us
where the time goes in v2:
time: 154 us
  Pallas kernels  149 us (97%)
  local copies, waits for them, and re-layouts  3.63 us (2%)
    pallas_call x1, Pallas kernels, fused(): pl.pallas_call(functools.partial(fused_kernel, n), out_shape=(jax.ShapeDt...  149 us
    unnamed x2, local copies, waits for them, and re-layouts  3.63 us

profile of v2, /device:TPU:0, one launch (start us, length us, event | category | flops | bytes accessed | tf_op | source)
XLA Modules:
  0.0 153.7 jit_solution(4345362503246117333)
XLA Ops:
  0.6 149.4 %shard_map.149 = (bf16[64,4096]{1,0:T(8,128)(2,1)}, bf16[48,4096]{1,0:T(8,128)(2,1)}) custom-call(bf16[64,4096]{1,0:T(8,128)(2,1)} %x_ref.1, f32[1,4096]{1,0:T(1,128)} %bitcast.13, s32[2,64]{1,0:T(2,128)} %bitcast.15, f32[2,64]{1,0:T(2,128)} %bitcast.16, bf16[192,512]{1,0:T(8,128)(2,1)} %q_raw.1, bf16[192,128]{1,0:T(8,128)(2,1)} %k_raw.1, ...), custom_call_target="tpu_custom_call" | custom-call | tf_op jit(solution)/shard_map/pallas_call | solution.py:775
  150.1 1.8 %copy.18 = bf16[48,4096]{1,0:T(8,128)(2,1)} copy(bf16[48,4096]{1,0:T(8,128)(2,1)} %get-tuple-element.8) | data formatting | bytes 786432
  151.9 1.9 %copy.19 = bf16[64,4096]{1,0:T(8,128)(2,1)} copy(bf16[64,4096]{1,0:T(8,128)(2,1)} %get-tuple-element.9) | data formatting | bytes 1048576

commit v3 on v2

--- a/solution.py
+++ b/solution.py
@@ -97,7 +97,40 @@
     return value.astype(jnp.float32)
 
 
-ORDER = (0, 1, 4, 6, 5, 2, 7, 3)
+INNER_ORDER = (
+    ("meta",), ("F6", 0), ("arr", 0, 0), ("F5", 0), ("sel", 4, 0), ("F6", 1), ("F3", 0), ("sel", 1, 1),
+    ("sel", 4, 1), ("sel", 5, 0), ("F5", 1), ("sel", 3, 0), ("F3", 1), ("arr", 4, 1), ("sel", 3, 1),
+    ("sel", 1, 0), ("arr", 5, 0), ("arx", 0, 0, 1), ("kvf", 0), ("arr", 0, 1), ("arr", 3, 0), ("F7", 1),
+    ("arr", 4, 0), ("arr", 3, 1), ("F7", 0), ("sel", 5, 1), ("kvs",), ("cmp", 0), ("kvf", 2),
+    ("arx", 0, 1, 0), ("D2", 1), ("arr", 5, 1), ("arx", 1, 0, 0), ("arx", 1, 1, 0), ("cmp", 3), ("fin", 0, 1),
+    ("sel", 2, 1), ("fin", 3, 0), ("cmp", 4), ("arx", 1, 0, 1), ("arx", 1, 1, 1), ("sel", 2, 0),
+    ("arr", 1, 0), ("arx", 0, 1, 1), ("arx", 0, 0, 0), ("fin", 3, 1), ("cmp", 7), ("fin", 7, 1),
+    ("arr", 1, 1), ("kvf", 1), ("cmp", 6), ("cmp", 5), ("fin", 6, 1), ("fin", 7, 0), ("cmp", 1),
+    ("arr", 2, 1), ("fin", 6, 0), ("gat", 3, 1), ("gat", 0, 1), ("att", 0), ("fin", 5, 1), ("gat", 3, 0),
+    ("fin", 1, 1), ("fin", 4, 1), ("rel", 3, 0), ("rel", 3, 1), ("att", 1), ("mixp",), ("fin", 5, 0),
+    ("arr", 2, 0), ("cmp", 2), ("gat", 4, 1), ("rel", 4, 1), ("fin", 1, 0), ("gat", 5, 0), ("mixs",),
+    ("fin", 2, 1), ("gat", 5, 1), ("rel", 5, 1), ("gat", 1, 1), ("gat", 1, 0), ("fin", 0, 0), ("rel", 1, 0),
+    ("fin", 4, 0), ("rel", 5, 0), ("fin", 2, 0), ("gat", 2, 1), ("rel", 2, 1), ("mixf",), ("gat", 0, 0),
+    ("gat", 4, 0), ("gat", 2, 0), ("rel", 2, 0), ("rel", 4, 0), ("rel", 1, 1), ("final", 1), ("final", 0),
+)
+OUTER_ORDER = (
+    ("meta",), ("F3", 0), ("sel", 1, 0), ("sel", 1, 1), ("sel", 4, 0), ("F3", 1), ("sel", 2, 0), ("kvs",),
+    ("sel", 4, 1), ("arx", 0, 0, 1), ("arr", 1, 0), ("arr", 4, 1), ("arr", 1, 1), ("sel", 3, 0),
+    ("arr", 0, 1), ("arx", 0, 1, 1), ("arr", 4, 0), ("arr", 3, 0), ("sel", 3, 1), ("sel", 5, 1), ("cmp", 1),
+    ("arx", 0, 0, 0), ("arx", 0, 1, 0), ("arr", 3, 1), ("arr", 5, 1), ("sel", 5, 0), ("cmp", 3), ("cmp", 6),
+    ("arr", 0, 0), ("fin", 3, 0), ("arr", 5, 0), ("fin", 6, 1), ("fin", 3, 1), ("cmp", 0), ("kvf", 0),
+    ("cmp", 4), ("gat", 3, 0), ("arx", 1, 0, 1), ("kvf", 2), ("arx", 1, 1, 1), ("arx", 1, 0, 0),
+    ("arx", 1, 1, 0), ("rel", 3, 0), ("sel", 2, 1), ("cmp", 7), ("gat", 3, 1), ("fin", 7, 1), ("arr", 2, 0),
+    ("rel", 3, 1), ("fin", 7, 0), ("fin", 4, 1), ("arr", 2, 1), ("kvf", 1), ("cmp", 5), ("gat", 4, 1),
+    ("fin", 6, 0), ("rel", 4, 1), ("fin", 5, 1), ("fin", 1, 1), ("att", 0), ("gat", 5, 1), ("rel", 5, 1),
+    ("fin", 5, 0), ("fin", 1, 0), ("att", 1), ("gat", 1, 1), ("rel", 1, 1), ("gat", 5, 0), ("rel", 5, 0),
+    ("fin", 4, 0), ("cmp", 2), ("fin", 2, 1), ("gat", 4, 0), ("rel", 4, 0), ("gat", 1, 0), ("rel", 1, 0),
+    ("fin", 2, 0), ("fin", 0, 0), ("mixp",), ("gat", 2, 1), ("rel", 2, 1), ("mixs",), ("fin", 0, 1),
+    ("gat", 2, 0), ("gat", 0, 0), ("rel", 2, 0), ("gat", 0, 1), ("final", 1), ("mixf",), ("final", 0),
+)
+
+
+BIG = {"cmp": 0, "att": 8, "mixp": 10}
 
 
 def fused_kernel(
@@ -120,6 +153,9 @@
     mixed,
     dense,
     meta,
+    chosen,
+    picks,
+    scales,
     rows,
     y_send,
     partial,
@@ -133,7 +169,6 @@
     p_got,
     o_got,
     q_ref,
-    kv_ref,
     turn,
     wg,
     wu,
@@ -146,7 +181,9 @@
     a_send,
     a_got,
     load_sem,
-    kv_sems,
+    kvz_out,
+    kvz_in,
+    kvy_sems,
     dn_out,
     dn_in,
     meta_sems,
@@ -194,6 +231,7 @@
     tokens_here = x_ref.shape[0]
     chunks = dn_in.shape[1]
     part = width // chunks
+    groups = (y, other_y)
 
     def remote(src, dst, send, recv, device):
         return pltpu.make_async_remote_copy(
@@ -218,27 +256,28 @@
     for load in loads:
         load.start()
 
+    far_peers = [(far_inner * 2 + y, t), (far_outer * 2 + y, t)]
     barrier = pltpu.get_barrier_semaphore()
-    for s in range(1, n):
-        pl.semaphore_signal(barrier, inc=1, device_id=(flip(e, s, n), t), device_id_type=MESH)
-    for peer in (x_peer, c_peer, corner):
+    greeted = [x_peer, c_peer, y_peer, z_peer, corner] + far_peers
+    for peer in greeted:
         pl.semaphore_signal(barrier, inc=1, device_id=peer, device_id_type=MESH)
 
-    def kv_direct(s):
-        return remote(kv_ref, kv_all.at[:, e], kv_sems.at[0, s], kv_sems.at[1, s], (flip(e, s, n), t))
-
-    def kv_direct_in(s):
-        return remote(kv_ref, kv_all.at[:, flip(e, s, n)], kv_sems.at[0, s], kv_sems.at[1, s], (flip(e, s, n), t))
-
-    def kv_relay(s):
-        owner = flip(e, s, n)
-        return remote(kv_all.at[:, owner], kv_all.at[:, owner], kv_sems.at[0, s + 1], kv_sems.at[1, s + 1], (flip(e, 1, n), t))
-
-    def kv_relay_in(s):
-        owner = flip(e, s + 1, n)
-        return remote(kv_all.at[:, owner], kv_all.at[:, owner], kv_sems.at[0, s + 1], kv_sems.at[1, s + 1], (flip(e, 1, n), t))
-
-    own_kv = pltpu.make_async_copy(kv_ref, kv_all.at[:, e], load_sem.at[5])
+    def kv_z(owner, out, place, device):
+        return remote(kv_all.at[:, owner], kv_all.at[:, owner], kvz_out.at[out], kvz_in.at[place], device)
+
+    stops = [layer, near, far_inner, far_outer]
+
+    def kv_y(j):
+        owner = stops[j] * 2 + y
+        return remote(kv_all.at[:, owner], kv_all.at[:, owner], kvy_sems.at[0, j], kvy_sems.at[1, j], y_peer)
+
+    kv_sends = [
+        kv_z(e, 0, 0, z_peer),
+        kv_z(e, 1, 1, m_peer),
+        kv_z(near * 2 + y, 2, 2, m_peer),
+        kv_z(far_inner * 2 + y, 3, 1, z_peer),
+        kv_z(far_outer * 2 + y, 4, 2, z_peer),
+    ]
 
     def block(source, target, number, c, device):
         return remote(
@@ -267,9 +306,6 @@
     def far_to_near(k, c):
         return block(4 + k, 4 + k, 6 + k, c, z_peer)
 
-    def arrived(slot, c):
-        block(slot, slot, 0, c, x_peer).wait_recv()
-
     far_slot = jnp.where(inner, 4, 5)
 
     def card(slot, number, device):
@@ -279,53 +315,120 @@
         card(1, 1, x_peer),
         card(2, 2, z_peer),
         card(3, 3, corner),
-        card(far_slot, 4, (far_inner * 2 + y, t)),
-        card(far_slot, 5, (far_outer * 2 + y, t)),
+        card(far_slot, 4, far_peers[0]),
+        card(far_slot, 5, far_peers[1]),
     ]
 
-    def row_to_y(b):
-        return remote(y_send.at[b], rows.at[b, core, y], row_y.at[0, b], row_y.at[1, b], y_peer)
-
-    def row_from_y(b):
-        return remote(y_send.at[b], rows.at[b, core, other_y], row_y.at[0, b], row_y.at[1, b], y_peer)
-
-    def row_to_c(b, g):
-        return remote(rows.at[b, core, g], rows.at[b, core, g], row_c.at[0, b, g], row_c.at[1, b, g], c_peer)
-
-    def row_from_c(b, g):
-        return remote(rows.at[b, core, g], rows.at[b, other_core, g], row_c.at[0, b, g], row_c.at[1, b, g], c_peer)
-
-    def row_to_x(k, g):
-        return remote(rows.at[4 + k, core, g], rows.at[6 + k, core, g], row_x.at[0, k, g], row_x.at[1, k, g], x_peer)
-
-    def reduce_c(b):
-        return remote(partial.at[b, other_core], red.at[b], red_sems.at[0, b], red_sems.at[1, b], c_peer)
-
-    def reduce_x(k):
-        return remote(partial.at[6 + k, core], x_got.at[k], sum_x.at[0, k], sum_x.at[1, k], x_peer)
-
-    def give_y(b):
-        return remote(partial.at[b, core, other_y], y_got.at[b], sum_y.at[0, b], sum_y.at[1, b], y_peer)
+    def row_to_y(b, c):
+        return remote(
+            y_send.at[b, :, cols(c)], rows.at[b, core, y, :, cols(c)], row_y.at[0, b, c], row_y.at[1, b, c], y_peer
+        )
+
+    def row_to_c(b, g, c):
+        here = rows.at[b, core, g, :, cols(c)]
+        return remote(here, here, row_c.at[0, b, g, c], row_c.at[1, b, g, c], c_peer)
+
+    def row_to_x(k, g, c):
+        return remote(
+            rows.at[4 + k, core, g, :, cols(c)],
+            rows.at[6 + k, core, g, :, cols(c)],
+            row_x.at[0, k, g, c],
+            row_x.at[1, k, g, c],
+            x_peer,
+        )
+
+    def reduce_c(b, c):
+        return remote(
+            partial.at[b, other_core, :, :, cols(c)],
+            red.at[b, :, :, cols(c)],
+            red_sems.at[0, b, c],
+            red_sems.at[1, b, c],
+            c_peer,
+        )
+
+    def reduce_x(k, c):
+        return remote(
+            partial.at[6 + k, core, :, :, cols(c)],
+            x_got.at[k, :, :, cols(c)],
+            sum_x.at[0, k, c],
+            sum_x.at[1, k, c],
+            x_peer,
+        )
+
+    def give_y(b, c):
+        return remote(
+            partial.at[b, core, other_y, :, cols(c)],
+            y_got.at[b, :, cols(c)],
+            sum_y.at[0, b, c],
+            sum_y.at[1, b, c],
+            y_peer,
+        )
 
     def pass_on(b, place, where, arrive, c, device):
         return remote(sent.at[b, :, cols(c)], where.at[place, :, cols(c)], t_out.at[b, c], arrive.at[place, c], device)
 
     mix_core = remote(a_part.at[:, other_core], a_red, mix_sems.at[0, 0], mix_sems.at[1, 0], c_peer)
     mix_side = remote(a_send, a_got, mix_sems.at[0, 1], mix_sems.at[1, 1], x_peer)
+
+    def wait_for(message):
+        kind = message[0]
+        c = message[-1]
+        k = message[1] if len(message) > 1 else 0
+        if kind == "d":
+            block(k, k, 0, c, x_peer).wait_recv()
+        elif kind == "ry":
+            remote(
+                y_send.at[k, :, cols(c)],
+                rows.at[k, core, other_y, :, cols(c)],
+                row_y.at[0, k, c],
+                row_y.at[1, k, c],
+                y_peer,
+            ).wait_recv()
+        elif kind == "rc":
+            g = groups[message[2]]
+            there = rows.at[k, other_core, g, :, cols(c)]
+            remote(there, there, row_c.at[0, k, g, c], row_c.at[1, k, g, c], c_peer).wait_recv()
+        elif kind == "rx":
+            row_to_x(k, groups[message[2]], c).wait_recv()
+        elif kind == "red":
+            reduce_c(k, c).wait_recv()
+        elif kind == "xg":
+            reduce_x(k, c).wait_recv()
+        elif kind == "gy":
+            give_y(k, c).wait_recv()
+        elif kind == "zg":
+            pass_on(1, k, z_got, z_in, c, z_peer).wait_recv()
+        elif kind == "mg":
+            pass_on(1, k, m_got, m_in, c, z_peer).wait_recv()
+        elif kind == "pg":
+            pass_on(1, k, p_got, p_in, c, z_peer).wait_recv()
+        elif kind == "og":
+            pass_on(1, 0, o_got, o_in, c, z_peer).wait_recv()
+        elif kind == "kvz":
+            kv_z(stops[k + 1] * 2 + y, 0, k, z_peer).wait_recv()
+        elif kind == "kvy":
+            owner = stops[k] * 2 + other_y
+            remote(
+                kv_all.at[:, owner], kv_all.at[:, owner], kvy_sems.at[0, k], kvy_sems.at[1, k], y_peer
+            ).wait_recv()
+        elif kind == "mc":
+            mix_core.wait_recv()
+        else:
+            mix_side.wait_recv()
 
     row_id = lax.broadcasted_iota(jnp.int32, (tokens_here, tokens_here), 0)
     col_id = lax.broadcasted_iota(jnp.int32, (tokens_here, tokens_here), 1)
     before = (row_id < col_id).astype(jnp.bfloat16)
     after = (col_id < row_id).astype(jnp.bfloat16)
 
-    def tiles(size, body):
+    def tiles(c, body):
         def run(j, carry):
-            body(pl.ds(pl.multiple_of(j * size, size), size))
+            body(pl.ds(pl.multiple_of(c * part + j * 512, 512), 512))
             return carry
 
-        lax.fori_loop(0, width // size, run, 0)
-
-    def select(b):
+        lax.fori_loop(0, part // 512, run, 0)
+
+    def build(b):
         named = meta[b]
         spread = []
         for expert in (e, y_expert):
@@ -335,84 +438,186 @@
         spread = jnp.concatenate(spread, axis=0)
         rank = jnp.dot(spread.astype(jnp.bfloat16), before, preferred_element_type=jnp.float32)
         slot = f32(lax.rem(lax.broadcasted_iota(jnp.int32, rank.shape, 0), cap))
-        chosen = (jnp.where(rank == slot, 1.0, 0.0) * spread).astype(jnp.bfloat16)
+        chosen[b] = (jnp.where(rank == slot, 1.0, 0.0) * spread).astype(jnp.bfloat16)
+        columns = jnp.transpose(named)[:tokens_here]
+        for place, expert in enumerate((e, y_expert)):
+            wanted = expert.astype(jnp.float32)
+            hits = [(columns[:, k:k + 1] == wanted).astype(jnp.float32) for k in range(2)]
+            scale = hits[0] * columns[:, 2:3] + hits[1] * columns[:, 3:4]
+            spread = jnp.broadcast_to(hits[0] + hits[1], (tokens_here, cap))
+            rank = jnp.dot(after, spread.astype(jnp.bfloat16), preferred_element_type=jnp.float32)
+            slot = f32(lax.broadcasted_iota(jnp.int32, rank.shape, 1))
+            picks[b, place] = (jnp.where(rank == slot, 1.0, 0.0) * spread).astype(jnp.bfloat16)
+            scales[b, place] = jnp.broadcast_to(scale, (tokens_here, 128))
+
+    def select(b, c):
+        table = chosen[b]
 
         def body(span):
-            found = jnp.dot(chosen, dense[b, :, span], preferred_element_type=jnp.float32).astype(jnp.bfloat16)
+            found = jnp.dot(table, dense[b, :, span], preferred_element_type=jnp.float32).astype(jnp.bfloat16)
             rows[b, core, y, :, span] = found[:cap]
             y_send[b, :, span] = found[cap:]
 
-        tiles(512, body)
-        row_to_y(b).start()
-        row_to_c(b, y).start()
+        tiles(c, body)
+        row_to_y(b, c).start()
+        row_to_c(b, y, c).start()
         if b >= 4:
-            row_to_x(b - 4, y).start()
-
-    def arrive(b):
-        if b < 6:
-            row_from_y(b).wait_recv()
-            if b >= 4:
-                row_to_x(b - 4, other_y).start()
-            row_to_c(b, other_y).start()
-        else:
-            for g in (y, other_y):
-                remote(
-                    rows.at[b - 2, core, g], rows.at[b, core, g], row_x.at[0, b - 6, g], row_x.at[1, b - 6, g], x_peer
-                ).wait_recv()
-                row_to_c(b, g).start()
-
-    def finish(b):
-        reduce_c(b).wait_recv()
-        if b in (4, 5):
-            reduce_x(b - 4).wait_recv()
-
+            row_to_x(b - 4, y, c).start()
+
+    def finish(b, c):
         def body(span):
             value = f32(partial[b, core, :, :, span]) + f32(red[b, :, :, span])
             if b in (4, 5):
                 value = value + f32(x_got[b - 4, :, :, span])
             partial[b, core, :, :, span] = value.astype(jnp.bfloat16)
 
-        tiles(512, body)
+        tiles(c, body)
         if b >= 6:
-            reduce_x(b - 6).start()
+            reduce_x(b - 6, c).start()
         else:
-            give_y(b).start()
-
-    def gather(b):
-        remote(partial.at[b, core, other_y], y_got.at[b], sum_y.at[0, b], sum_y.at[1, b], y_peer).wait_recv()
-        turned_meta = jnp.transpose(meta[b])[:tokens_here]
-        parts = []
-        for expert in (e, y_expert):
-            wanted = expert.astype(jnp.float32)
-            hits = [(turned_meta[:, k:k + 1] == wanted).astype(jnp.float32) for k in range(2)]
-            scale = hits[0] * turned_meta[:, 2:3] + hits[1] * turned_meta[:, 3:4]
-            spread = jnp.broadcast_to(hits[0] + hits[1], (tokens_here, cap))
-            rank = jnp.dot(after, spread.astype(jnp.bfloat16), preferred_element_type=jnp.float32)
-            slot = f32(lax.broadcasted_iota(jnp.int32, rank.shape, 1))
-            parts.append(((jnp.where(rank == slot, 1.0, 0.0) * spread).astype(jnp.bfloat16), scale))
+            give_y(b, c).start()
+
+    def gather(b, c):
+        mine, theirs = picks[b, 0], picks[b, 1]
+        scale_mine, scale_theirs = scales[b, 0, :, 0:1], scales[b, 1, :, 0:1]
 
         def body(span):
-            mine = jnp.dot(parts[0][0], partial[b, core, y, :, span], preferred_element_type=jnp.float32)
-            theirs = jnp.dot(parts[1][0], y_got[b, :, span], preferred_element_type=jnp.float32)
-            hold[b, :, span] = mine * parts[0][1] + theirs * parts[1][1]
-
-        tiles(512, body)
-
-    def release(b, sources, place, where, arrive_sem, device):
-        for c in range(chunks):
-            for got, at, sem in sources:
-                remote(got.at[at, :, cols(c)], got.at[at, :, cols(c)], t_out.at[0, c], sem.at[at, c], device).wait_recv()
-
-            def run(j, carry):
-                span = pl.ds(pl.multiple_of(c * part + j * 512, 512), 512)
-                value = hold[b, :, span]
-                for got, at, sem in sources:
-                    value = value + f32(got[at, :, span])
-                sent[b, :, span] = value.astype(jnp.bfloat16)
+            first = jnp.dot(mine, partial[b, core, y, :, span], preferred_element_type=jnp.float32)
+            second = jnp.dot(theirs, y_got[b, :, span], preferred_element_type=jnp.float32)
+            hold[b, :, span] = first * scale_mine + second * scale_theirs
+
+        tiles(c, body)
+
+    def release(b, c, sources, place, where, arrive, device):
+        def body(span):
+            value = hold[b, :, span]
+            for got, at in sources:
+                value = value + f32(got[at, :, span])
+            sent[b, :, span] = value.astype(jnp.bfloat16)
+
+        tiles(c, body)
+        pass_on(b, place, where, arrive, c, device).start()
+
+    def messages(task, is_inner):
+        kind = task[0]
+        c = task[-1]
+        b = task[1] if len(task) > 1 else 0
+        whole = range(chunks)
+        if kind in ("F3", "F6", "F5", "F7"):
+            return [("d", {"F3": 1, "F6": 4, "F5": 2, "F7": 5}[kind], c)]
+        if kind == "sel":
+            return [("d", b, c)]
+        if kind == "arr":
+            return [("ry", b, c)]
+        if kind == "arx":
+            return [("rx", b, task[2], c)]
+        if kind == "cmp":
+            return [("rc", b, g, c) for g in range(2) for c in whole]
+        if kind == "fin":
+            return [("red", b, c)] + ([("xg", b - 4, c)] if b in (4, 5) else [])
+        if kind == "gat":
+            return [("gy", b, c)]
+        if kind == "rel":
+            if b == 1:
+                return [("pg", 1, c)]
+            if is_inner and b in (4, 5):
+                return [("zg", b - 4, c)]
+            return [("mg", 1, c)] if is_inner and b == 2 else []
+        if kind == "final":
+            return [("og", c), ("pg", 0, c)] + ([("mg", 0, c)] if is_inner else [])
+        if kind == "kvf":
+            return [("kvz", b)]
+        if kind == "att":
+            return [("kvy", j) for j in range(4)]
+        return {"mixs": [("mc",)], "mixf": [("mx",)]}.get(kind, [])
+
+    def perform(task, is_inner):
+        kind = task[0]
+        c = task[-1]
+        b = task[1] if len(task) > 1 else 0
+        if kind == "D2":
+            to_near(c).start()
+        elif kind == "F3":
+            x_to_near(c).start()
+        elif kind == "F6":
+            far_to_near(0, c).start()
+        elif kind == "F5":
+            near_to_across(c).start()
+        elif kind == "F7":
+            far_to_near(1, c).start()
+        elif kind == "meta":
+            for slot in range(1, 6):
+                card(slot, 0, x_peer).wait_recv()
+
+            def run(slot, carry):
+                build(slot)
                 return carry
 
-            lax.fori_loop(0, part // 512, run, 0)
-            pass_on(b, place, where, arrive_sem, c, device).start()
+            lax.fori_loop(1, 6, run, 0)
+        elif kind == "sel":
+            select(b, c)
+        elif kind == "arr":
+            row_to_c(b, other_y, c).start()
+            if b >= 4:
+                row_to_x(b - 4, other_y, c).start()
+        elif kind == "arx":
+            row_to_c(6 + b, groups[task[2]], c).start()
+        elif kind == "fin":
+            finish(b, c)
+        elif kind == "gat":
+            gather(b, c)
+        elif kind == "rel":
+            if b == 1:
+                release(b, c, [(p_got, 1)], 0, o_got, o_in, x_peer)
+            elif b == 2:
+                release(b, c, [(m_got, 1)] if is_inner else [], 0, p_got, p_in, z_peer)
+            elif b == 3:
+                release(b, c, [], 1, p_got, p_in, z_peer)
+            elif is_inner:
+                release(b, c, [(z_got, b - 4)], b - 4, m_got, m_in, m_peer)
+            else:
+                release(b, c, [], b - 4, z_got, z_in, z_peer)
+        elif kind == "final":
+            def body(span):
+                value = hold[0, :, span] + f32(o_got[0, :, span]) + f32(p_got[0, :, span])
+                if is_inner:
+                    value = value + f32(m_got[0, :, span])
+                moe[:, span] = value.astype(jnp.bfloat16)
+
+            tiles(c, body)
+        elif kind == "kvs":
+            kv_sends[0].start()
+            if is_inner:
+                kv_sends[1].start()
+            kv_y(0).start()
+        elif kind == "kvf":
+            if is_inner:
+                kv_sends[2 + b].start()
+            kv_y(b + 1).start()
+        elif kind == "mixs":
+            a_send[...] = (f32(a_part[other_side, core]) + f32(a_red[other_side])).astype(jnp.bfloat16)
+            mix_side.start()
+        elif kind == "mixf":
+            mixed[...] = (f32(a_part[side, core]) + f32(a_red[side]) + f32(a_got[...])).astype(jnp.bfloat16)
+
+    def plan(order, is_inner):
+        seen = {("d", 0, c) for c in range(chunks)}
+        pieces, kinds = [[]], []
+        for task in order:
+            fresh = [message for message in messages(task, is_inner) if message not in seen]
+            seen.update(fresh)
+            pieces[-1].append((fresh, task))
+            if task[0] in BIG:
+                kinds.append(BIG[task[0]] + (task[1] if len(task) > 1 else 0))
+                pieces.append([])
+        return pieces, kinds
+
+    def emit(piece, is_inner):
+        for fresh, task in piece:
+            for message in fresh:
+                wait_for(message)
+            if task[0] not in BIG:
+                perform(task, is_inner)
 
     as_float = f32(x_ref[...])
     mean = jnp.mean(as_float * as_float, axis=1, keepdims=True)
@@ -421,7 +626,7 @@
     meta[0, 0:2, 0:tokens_here] = f32(routes_row[...])
     meta[0, 2:4, 0:tokens_here] = weight_row[...]
 
-    pl.semaphore_wait(barrier, n + 2)
+    pl.semaphore_wait(barrier, len(greeted))
     for item in cards:
         item.start()
     for c in range(chunks):
@@ -438,7 +643,9 @@
             def _():
                 to_near(c).start()
 
-    select(0)
+    build(0)
+    for c in range(chunks):
+        select(0, c)
 
     loads[0].wait()
     lane = lax.broadcasted_iota(jnp.int32, (tok, 128), 1)
@@ -461,41 +668,21 @@
         )
         return unit * cosine + partner * sine
 
-    for pair in range(kv_ref.shape[0] // 2):
+    for pair in range(kv_all.shape[0] // 2):
         span = slice(pair * 128, (pair + 1) * 128)
         k_rows = turned(k_raw[:, span], k_gain[:, span])
         v_rows = f32(v_raw[:, span])
-        kv_ref[2 * pair] = jnp.where(low, k_rows, pltpu.roll(v_rows, HEAD_DIM, 1)).astype(jnp.bfloat16)
-        kv_ref[2 * pair + 1] = jnp.where(low, pltpu.roll(k_rows, HEAD_DIM, 1), v_rows).astype(jnp.bfloat16)
-    own_kv.start()
-    for s in range(2, n, 2):
-        kv_direct(s).start()
-    kv_direct(1).start()
+        kv_all[2 * pair, e] = jnp.where(low, k_rows, pltpu.roll(v_rows, HEAD_DIM, 1)).astype(jnp.bfloat16)
+        kv_all[2 * pair + 1, e] = jnp.where(low, pltpu.roll(k_rows, HEAD_DIM, 1), v_rows).astype(jnp.bfloat16)
 
     for pair in range(pairs):
         span = slice(pair * 128, (pair + 1) * 128)
         q_rows = turned(q_raw[:, span], q_gain[:, span])
         q_ref[2 * pair] = jnp.where(low, q_rows, 0.0).astype(jnp.bfloat16)
         q_ref[2 * pair + 1] = jnp.where(low, pltpu.roll(q_rows, HEAD_DIM, 1), 0.0).astype(jnp.bfloat16)
-    own_kv.wait()
-
-    for slot in range(1, 6):
-        remote(meta.at[0], meta.at[slot], meta_sems.at[0, 0], meta_sems.at[1, slot], x_peer).wait_recv()
-    for c in range(chunks):
-        arrived(1, c)
-
-        @pl.when(outer)
-        def _():
-            x_to_near(c).start()
-
-        @pl.when(inner)
-        def _():
-            arrived(4, c)
-            far_to_near(0, c).start()
-            arrived(2, c)
-            near_to_across(c).start()
-
-    select(1)
+
+    for load in loads[1:]:
+        load.wait()
 
     def attend(pair):
         kv = kv_all[lax.div(pair * 2 * kv_all.shape[0], pairs * 2)].reshape(n * tok, 128)
@@ -512,216 +699,74 @@
         joined = jnp.where(low, pltpu.roll(halves[0], HEAD_DIM, 1), halves[1])
         attended[pair] = joined.astype(jnp.bfloat16)
 
-    def mix_product():
-        loads[4].wait()
-        for tile in range(0, width, TILE):
-            product = jnp.dot(attended[0], ow[0, :, tile:tile + TILE], preferred_element_type=jnp.float32)
-            for p in range(1, pairs):
-                product += jnp.dot(attended[p], ow[p, :, tile:tile + TILE], preferred_element_type=jnp.float32)
-            a_part[:, :, :, tile:tile + TILE] = product.astype(jnp.bfloat16).reshape(2, 2, tok // 4, TILE)
-        mix_core.start()
-
-    def mix_sum():
-        mix_core.wait_recv()
-        a_send[...] = (f32(a_part[other_side, core]) + f32(a_red[other_side])).astype(jnp.bfloat16)
-        mix_side.start()
-
-    def unit_of(s):
-        chosen = ORDER[0]
-        for place in range(1, len(ORDER)):
-            chosen = jnp.where(s == place, ORDER[place], chosen)
-        return chosen
+    inner_pieces, inner_kinds = plan(INNER_ORDER, True)
+    outer_pieces, outer_kinds = plan(OUTER_ORDER, False)
+    count = len(inner_kinds)
 
     def step(s, carry):
-        u = unit_of(s)
-
-        def at(number):
-            return pl.when(s == number)
-
-        @at(1)
+        u = jnp.where(inner, inner_kinds[0], outer_kinds[0])
+        for place in range(1, count):
+            u = jnp.where(s == place, jnp.where(inner, inner_kinds[place], outer_kinds[place]), u)
+        for place in range(count):
+            @pl.when(jnp.logical_and(s == place, inner))
+            def _():
+                emit(inner_pieces[place], True)
+
+            @pl.when(jnp.logical_and(s == place, outer))
+            def _():
+                emit(outer_pieces[place], False)
+
+        @pl.when(u < 8)
         def _():
-            @pl.when(inner)
-            def _():
-                arrived(5, 0)
-                far_to_near(1, 0).start()
-
-        for place, b in enumerate(ORDER):
-            @at(place)
-            def _(b=b):
-                arrive(b)
-
-        @at(0)
+            tokens = rows[u].reshape(4 * cap, width)
+            gate = jnp.dot(tokens, wg[...], preferred_element_type=jnp.float32)
+            up = jnp.dot(tokens, wu[...], preferred_element_type=jnp.float32)
+            hidden = (gate / (1.0 + jnp.exp(-gate)) * up).astype(jnp.bfloat16)
+            for tile in range(0, width, TILE):
+                product = jnp.dot(hidden, wd[:, tile:tile + TILE], preferred_element_type=jnp.float32)
+                partial[u, :, :, :, tile:tile + TILE] = product.astype(jnp.bfloat16).reshape(2, 2, cap, TILE)
+                if (tile + TILE) % part == 0:
+                    reduce_c(u, tile // part).start()
+
+        @pl.when(jnp.logical_and(u >= 8, u < 10))
         def _():
-            for load in loads[1:4]:
-                load.wait()
-
-        @at(1)
+            attend(2 * (u - 8))
+            attend(2 * (u - 8) + 1)
+
+        @pl.when(u == 10)
         def _():
-            for s2 in range(2, n, 2):
-                kv_direct_in(s2).wait_recv()
-                kv_relay(s2).start()
-            finish(0)
-
-        @at(2)
-        def _():
-            finish(1)
-
-        @at(3)
-        def _():
-            gather(0)
-
-        @at(4)
-        def _():
-            finish(6)
-            mix_product()
-
-        @at(5)
-        def _():
-            mix_sum()
-            gather(1)
-
-        @at(6)
-        def _():
-            finish(4)
-            finish(2)
-
-        @at(7)
-        def _():
-            finish(7)
-            gather(4)
-
-            @pl.when(outer)
-            def _():
-                release(4, [], 0, z_got, z_in, z_peer)
-
-        for g in range(2):
-            row_from_c(u, g).wait_recv()
-        tokens = rows[u].reshape(4 * cap, width)
-        gate = jnp.dot(tokens, wg[...], preferred_element_type=jnp.float32)
-        up = jnp.dot(tokens, wu[...], preferred_element_type=jnp.float32)
-        hidden = (gate / (1.0 + jnp.exp(-gate)) * up).astype(jnp.bfloat16)
-        for tile in range(0, width, TILE):
-            product = jnp.dot(hidden, wd[:, tile:tile + TILE], preferred_element_type=jnp.float32)
-            partial[u, :, :, :, tile:tile + TILE] = product.astype(jnp.bfloat16).reshape(2, 2, cap, TILE)
-        reduce_c(u).start()
-
-        @at(0)
-        def _():
-            @pl.when(outer)
-            def _():
-                for c in range(chunks):
-                    arrived(4, c)
-
-            select(4)
-
-        @at(1)
-        def _():
-            @pl.when(inner)
-            def _():
-                for c in range(1, chunks):
-                    arrived(5, c)
-                    far_to_near(1, c).start()
-                    to_near(c).start()
-                for c in range(chunks):
-                    x_to_near(c).start()
-
-            kv_direct_in(1).wait_recv()
-            for s2 in range(2, n, 2):
-                kv_relay_in(s2).wait_recv()
-
-        @pl.when(jnp.logical_or(s == 1, s == 2))
-        def _():
-            attend(2 * (s - 1))
-            attend(2 * (s - 1) + 1)
-
-        @at(2)
-        def _():
-            @pl.when(outer)
-            def _():
-                for c in range(chunks):
-                    arrived(5, c)
-
-            select(5)
-
-        @at(3)
-        def _():
-            @pl.when(outer)
-            def _():
-                for c in range(chunks):
-                    arrived(2, c)
-
-            select(2)
-
-        @at(5)
-        def _():
-            for c in range(chunks):
-                arrived(3, c)
-            select(3)
+            for tile in range(0, width, TILE):
+                product = jnp.dot(attended[0], ow[0, :, tile:tile + TILE], preferred_element_type=jnp.float32)
+                for p in range(1, pairs):
+                    product += jnp.dot(attended[p], ow[p, :, tile:tile + TILE], preferred_element_type=jnp.float32)
+                a_part[:, :, :, tile:tile + TILE] = product.astype(jnp.bfloat16).reshape(2, 2, tok // 4, TILE)
+            mix_core.start()
 
         return carry
 
-    lax.fori_loop(0, len(ORDER), step, 0)
-
-    finish(5)
-    finish(3)
-    gather(2)
-    gather(5)
+    lax.fori_loop(0, count, step, 0)
+
+    @pl.when(inner)
+    def _():
+        emit(inner_pieces[count], True)
 
     @pl.when(outer)
     def _():
-        release(5, [], 1, z_got, z_in, z_peer)
+        emit(outer_pieces[count], False)
+
+    mix_core.wait_send()
+    mix_side.wait_send()
+    for j in range(4):
+        kv_y(j).wait_send()
+    kv_sends[0].wait_send()
+    for item in cards:
+        item.wait_send()
 
     @pl.when(inner)
     def _():
-        release(4, [(z_got, 0, z_in)], 0, m_got, m_in, m_peer)
-
-    gather(3)
-    release(3, [], 1, p_got, p_in, z_peer)
-
-    @pl.when(inner)
-    def _():
-        release(5, [(z_got, 1, z_in)], 1, m_got, m_in, m_peer)
-
-    mix_side.wait_recv()
-    mixed[...] = (f32(a_part[side, core]) + f32(a_red[side]) + f32(a_got[...])).astype(jnp.bfloat16)
-
-    release(1, [(p_got, 1, p_in)], 0, o_got, o_in, x_peer)
-
-    @pl.when(outer)
-    def _():
-        release(2, [], 0, p_got, p_in, z_peer)
-
-    @pl.when(inner)
-    def _():
-        release(2, [(m_got, 1, m_in)], 0, p_got, p_in, z_peer)
-        for c in range(chunks):
-            remote(m_got.at[0, :, cols(c)], m_got.at[0, :, cols(c)], t_out.at[0, c], m_in.at[0, c], m_peer).wait_recv()
-
-        def fold(span):
-            hold[0, :, span] = hold[0, :, span] + f32(m_got[0, :, span])
-
-        tiles(512, fold)
-
-    for c in range(chunks):
-        for got, sem in ((o_got, o_in), (p_got, p_in)):
-            remote(got.at[0, :, cols(c)], got.at[0, :, cols(c)], t_out.at[0, c], sem.at[0, c], x_peer).wait_recv()
-
-        def final(j, carry):
-            span = pl.ds(pl.multiple_of(c * part + j * 512, 512), 512)
-            value = hold[0, :, span] + f32(o_got[0, :, span]) + f32(p_got[0, :, span])
-            moe[:, span] = value.astype(jnp.bfloat16)
-            return carry
-
-        lax.fori_loop(0, part // 512, final, 0)
-
-    mix_core.wait_send()
-    mix_side.wait_send()
-    for s in range(2, n, 2):
-        kv_direct(s).wait_send()
-        kv_relay(s).wait_send()
-    kv_direct(1).wait_send()
-    for item in cards:
-        item.wait_send()
+        for item in kv_sends[1:]:
+            item.wait_send()
+
     for c in range(chunks):
         to_x(c).wait_send()
         to_near(c).wait_send()
@@ -736,17 +781,17 @@
 
         for b in range(1, 6):
             pass_on(b, 0, o_got, o_in, c, x_peer).wait_send()
-    for k in range(2):
-        for g in range(2):
-            row_to_x(k, g).wait_send()
-        reduce_x(k).wait_send()
-    for b in range(6):
-        row_to_y(b).wait_send()
-        give_y(b).wait_send()
-    for b in range(8):
-        for g in range(2):
-            row_to_c(b, g).wait_send()
-        reduce_c(b).wait_send()
+        for k in range(2):
+            for g in range(2):
+                row_to_x(k, g, c).wait_send()
+            reduce_x(k, c).wait_send()
+        for b in range(6):
+            row_to_y(b, c).wait_send()
+            give_y(b, c).wait_send()
+        for b in range(8):
+            for g in range(2):
+                row_to_c(b, g, c).wait_send()
+            reduce_c(b, c).wait_send()
 
 
 def turn_table(tokens):
@@ -783,6 +828,9 @@
         scratch_shapes=[
             pltpu.VMEM((6, tok_exp, width), bf),
             pltpu.VMEM((6, 8, 128), jnp.float32),
+            pltpu.VMEM((6, 2 * cap, tok_exp), bf),
+            pltpu.VMEM((6, 2, tok_exp, cap), bf),
+            pltpu.VMEM((6, 2, tok_exp, 128), jnp.float32),
             pltpu.VMEM((8, 2, 2, cap, width), bf),
             pltpu.VMEM((6, cap, width), bf),
             pltpu.VMEM((8, 2, 2, cap, width), bf),
@@ -796,7 +844,6 @@
             pltpu.VMEM((2, tok_exp, width), bf),
             pltpu.VMEM((1, tok_exp, width), bf),
             pltpu.VMEM((heads, tok, 128), bf),
-            pltpu.VMEM((kv_count, tok, 128), bf),
             pltpu.VMEM((tok, 128), jnp.float32),
             pltpu.VMEM((width, hidden), bf),
             pltpu.VMEM((width, hidden), bf),
@@ -808,17 +855,19 @@
             pltpu.VMEM((2, tok // 4, width), bf),
             pltpu.VMEM((tok // 4, width), bf),
             pltpu.VMEM((tok // 4, width), bf),
-            dma((6,)),
-            dma((2, n)),
+            dma((5,)),
+            dma((5,)),
+            dma((3,)),
+            dma((2, 4)),
             dma((8, CHUNKS)),
             dma((6, CHUNKS)),
             dma((2, 6)),
-            dma((2, 6)),
-            dma((2, 8, 2)),
-            dma((2, 2, 2)),
-            dma((2, 8)),
-            dma((2, 2)),
-            dma((2, 6)),
+            dma((2, 6, CHUNKS)),
+            dma((2, 8, 2, CHUNKS)),
+            dma((2, 2, 2, CHUNKS)),
+            dma((2, 8, CHUNKS)),
+            dma((2, 2, CHUNKS)),
+            dma((2, 6, CHUNKS)),
             dma((6, CHUNKS)),
             dma((2, CHUNKS)),
             dma((2, CHUNKS)),

time: 154 us -> 115 us (0.75)
  Pallas kernels: 149 us -> 110 us
    pallas_call x1, Pallas kernels: 149 us -> 110 us  [fused(): pl.pallas_call(functools.partial(fused_kernel, n), out_shape=(jax.ShapeDt...]
where the time goes in v3:
time: 115 us; the launch traced here: 114 us
  Pallas kernels  110 us (96%)
  local copies, waits for them, and re-layouts  3.63 us (3%)
    pallas_call x1, Pallas kernels, fused(): pl.pallas_call(functools.partial(fused_kernel, n), out_shape=(jax.ShapeDt...  110 us
    unnamed x2, local copies, waits for them, and re-layouts  3.63 us

profile of v3, /device:TPU:0, one launch (start us, length us, event | category | flops | bytes accessed | tf_op | source)
XLA Modules:
  0.0 114.4 jit_solution(10730464801368382102)
XLA Ops:
  0.6 110.1 %shard_map.149 = (bf16[64,4096]{1,0:T(8,128)(2,1)}, bf16[48,4096]{1,0:T(8,128)(2,1)}) custom-call(bf16[64,4096]{1,0:T(8,128)(2,1)} %x_ref.1, f32[1,4096]{1,0:T(1,128)} %bitcast.13, s32[2,64]{1,0:T(2,128)} %bitcast.15, f32[2,64]{1,0:T(2,128)} %bitcast.16, bf16[192,512]{1,0:T(8,128)(2,1)} %q_raw.1, bf16[192,128]{1,0:T(8,128)(2,1)} %k_raw.1, ...), custom_call_target="tpu_custom_call" | custom-call | tf_op jit(solution)/shard_map/pallas_call | solution.py:820
  110.8 1.8 %copy.18 = bf16[48,4096]{1,0:T(8,128)(2,1)} copy(bf16[48,4096]{1,0:T(8,128)(2,1)} %get-tuple-element.8) | data formatting | bytes 786432
  112.6 1.9 %copy.19 = bf16[64,4096]{1,0:T(8,128)(2,1)} copy(bf16[64,4096]{1,0:T(8,128)(2,1)} %get-tuple-element.9) | data formatting | bytes 1048576

commit v4 on v3

--- a/solution.py
+++ b/solution.py
@@ -80,7 +80,7 @@
 
 MESH = pl.DeviceIdType.MESH
 TILE = 1024
-CHUNKS = 2
+CHUNKS = 4
 
 
 def flip(index, pattern, size):
@@ -98,35 +98,58 @@
 
 
 INNER_ORDER = (
-    ("meta",), ("F6", 0), ("arr", 0, 0), ("F5", 0), ("sel", 4, 0), ("F6", 1), ("F3", 0), ("sel", 1, 1),
-    ("sel", 4, 1), ("sel", 5, 0), ("F5", 1), ("sel", 3, 0), ("F3", 1), ("arr", 4, 1), ("sel", 3, 1),
-    ("sel", 1, 0), ("arr", 5, 0), ("arx", 0, 0, 1), ("kvf", 0), ("arr", 0, 1), ("arr", 3, 0), ("F7", 1),
-    ("arr", 4, 0), ("arr", 3, 1), ("F7", 0), ("sel", 5, 1), ("kvs",), ("cmp", 0), ("kvf", 2),
-    ("arx", 0, 1, 0), ("D2", 1), ("arr", 5, 1), ("arx", 1, 0, 0), ("arx", 1, 1, 0), ("cmp", 3), ("fin", 0, 1),
-    ("sel", 2, 1), ("fin", 3, 0), ("cmp", 4), ("arx", 1, 0, 1), ("arx", 1, 1, 1), ("sel", 2, 0),
-    ("arr", 1, 0), ("arx", 0, 1, 1), ("arx", 0, 0, 0), ("fin", 3, 1), ("cmp", 7), ("fin", 7, 1),
-    ("arr", 1, 1), ("kvf", 1), ("cmp", 6), ("cmp", 5), ("fin", 6, 1), ("fin", 7, 0), ("cmp", 1),
-    ("arr", 2, 1), ("fin", 6, 0), ("gat", 3, 1), ("gat", 0, 1), ("att", 0), ("fin", 5, 1), ("gat", 3, 0),
-    ("fin", 1, 1), ("fin", 4, 1), ("rel", 3, 0), ("rel", 3, 1), ("att", 1), ("mixp",), ("fin", 5, 0),
-    ("arr", 2, 0), ("cmp", 2), ("gat", 4, 1), ("rel", 4, 1), ("fin", 1, 0), ("gat", 5, 0), ("mixs",),
-    ("fin", 2, 1), ("gat", 5, 1), ("rel", 5, 1), ("gat", 1, 1), ("gat", 1, 0), ("fin", 0, 0), ("rel", 1, 0),
-    ("fin", 4, 0), ("rel", 5, 0), ("fin", 2, 0), ("gat", 2, 1), ("rel", 2, 1), ("mixf",), ("gat", 0, 0),
-    ("gat", 4, 0), ("gat", 2, 0), ("rel", 2, 0), ("rel", 4, 0), ("rel", 1, 1), ("final", 1), ("final", 0),
+    ("F6", 0), ("meta",), ("sel", 2, 0), ("F6", 1), ("sel", 2, 1), ("sel", 4, 0), ("F5", 0), ("F6", 2),
+    ("F5", 2), ("sel", 4, 1), ("F5", 1), ("sel", 1, 1), ("sel", 4, 2), ("arr", 2, 0), ("F3", 0),
+    ("arr", 0, 1), ("arr", 0, 2), ("arr", 0, 0), ("sel", 1, 3), ("F3", 1), ("sel", 5, 0), ("F3", 3),
+    ("sel", 2, 3), ("arr", 4, 1), ("arr", 1, 3), ("sel", 3, 0), ("arr", 1, 1), ("arx", 0, 0, 1), ("F3", 2),
+    ("sel", 2, 2), ("sel", 4, 3), ("arr", 5, 0), ("sel", 1, 0), ("F6", 3), ("sel", 5, 2), ("F5", 3),
+    ("sel", 1, 2), ("F7", 3), ("F7", 0), ("sel", 5, 3), ("F7", 2), ("sel", 3, 1), ("arr", 0, 3),
+    ("arr", 2, 3), ("arr", 4, 3), ("sel", 3, 2), ("F7", 1), ("sel", 5, 1), ("arr", 1, 2), ("arr", 5, 2),
+    ("sel", 3, 3), ("arr", 4, 0), ("arr", 4, 2), ("arr", 1, 0), ("arx", 0, 1, 1), ("arx", 0, 1, 3),
+    ("cmp", 4), ("kvf", 0), ("arx", 1, 1, 0), ("arr", 2, 2), ("kvs",), ("arx", 0, 1, 0), ("arr", 2, 1),
+    ("cmp", 0), ("arx", 0, 0, 2), ("arr", 3, 1), ("arr", 3, 2), ("cmp", 1), ("arx", 0, 0, 3), ("arr", 3, 0),
+    ("arx", 0, 1, 2), ("arx", 1, 0, 1), ("arx", 0, 0, 0), ("arr", 3, 3), ("arr", 5, 3), ("kvf", 1),
+    ("kvf", 2), ("arx", 1, 1, 2), ("arx", 1, 0, 3), ("fin", 1, 3), ("arx", 1, 0, 0), ("arr", 5, 1),
+    ("cmp", 6), ("fin", 1, 2), ("D2", 1), ("cmp", 3), ("fin", 6, 2), ("fin", 6, 1), ("D2", 2), ("fin", 6, 3),
+    ("cmp", 2), ("arx", 1, 1, 3), ("cmp", 5), ("fin", 3, 2), ("arx", 1, 1, 1), ("fin", 3, 0), ("att", 0),
+    ("fin", 1, 0), ("arx", 1, 0, 2), ("fin", 6, 0), ("gat", 1, 3), ("fin", 4, 1), ("fin", 3, 1),
+    ("fin", 4, 2), ("fin", 3, 3), ("fin", 2, 0), ("cmp", 7), ("fin", 7, 2), ("gat", 3, 2), ("D2", 3),
+    ("fin", 7, 0), ("fin", 4, 0), ("fin", 2, 2), ("att", 1), ("fin", 2, 3), ("fin", 4, 3), ("rel", 3, 2),
+    ("fin", 7, 1), ("gat", 3, 1), ("gat", 4, 2), ("gat", 3, 3), ("rel", 3, 3), ("gat", 2, 0), ("fin", 7, 3),
+    ("fin", 5, 0), ("mixp",), ("gat", 1, 2), ("fin", 0, 0), ("gat", 3, 0), ("rel", 4, 2), ("rel", 1, 2),
+    ("rel", 3, 0), ("fin", 2, 1), ("fin", 5, 1), ("gat", 5, 0), ("rel", 3, 1), ("fin", 5, 2), ("gat", 4, 3),
+    ("rel", 5, 0), ("gat", 1, 0), ("gat", 4, 0), ("mixs",), ("gat", 2, 2), ("gat", 2, 1), ("fin", 5, 3),
+    ("fin", 1, 1), ("fin", 0, 2), ("fin", 0, 1), ("rel", 4, 3), ("gat", 5, 2), ("gat", 0, 0), ("rel", 2, 0),
+    ("rel", 1, 0), ("gat", 5, 1), ("rel", 5, 2), ("gat", 5, 3), ("rel", 5, 1), ("gat", 0, 1), ("rel", 2, 2),
+    ("rel", 5, 3), ("mixf",), ("gat", 4, 1), ("gat", 2, 3), ("rel", 1, 3), ("gat", 1, 1), ("fin", 0, 3),
+    ("rel", 2, 1), ("rel", 4, 0), ("rel", 1, 1), ("rel", 2, 3), ("rel", 4, 1), ("gat", 0, 3), ("gat", 0, 2),
+    ("final", 2), ("final", 1), ("final", 0), ("final", 3),
 )
 OUTER_ORDER = (
-    ("meta",), ("F3", 0), ("sel", 1, 0), ("sel", 1, 1), ("sel", 4, 0), ("F3", 1), ("sel", 2, 0), ("kvs",),
-    ("sel", 4, 1), ("arx", 0, 0, 1), ("arr", 1, 0), ("arr", 4, 1), ("arr", 1, 1), ("sel", 3, 0),
-    ("arr", 0, 1), ("arx", 0, 1, 1), ("arr", 4, 0), ("arr", 3, 0), ("sel", 3, 1), ("sel", 5, 1), ("cmp", 1),
-    ("arx", 0, 0, 0), ("arx", 0, 1, 0), ("arr", 3, 1), ("arr", 5, 1), ("sel", 5, 0), ("cmp", 3), ("cmp", 6),
-    ("arr", 0, 0), ("fin", 3, 0), ("arr", 5, 0), ("fin", 6, 1), ("fin", 3, 1), ("cmp", 0), ("kvf", 0),
-    ("cmp", 4), ("gat", 3, 0), ("arx", 1, 0, 1), ("kvf", 2), ("arx", 1, 1, 1), ("arx", 1, 0, 0),
-    ("arx", 1, 1, 0), ("rel", 3, 0), ("sel", 2, 1), ("cmp", 7), ("gat", 3, 1), ("fin", 7, 1), ("arr", 2, 0),
-    ("rel", 3, 1), ("fin", 7, 0), ("fin", 4, 1), ("arr", 2, 1), ("kvf", 1), ("cmp", 5), ("gat", 4, 1),
-    ("fin", 6, 0), ("rel", 4, 1), ("fin", 5, 1), ("fin", 1, 1), ("att", 0), ("gat", 5, 1), ("rel", 5, 1),
-    ("fin", 5, 0), ("fin", 1, 0), ("att", 1), ("gat", 1, 1), ("rel", 1, 1), ("gat", 5, 0), ("rel", 5, 0),
-    ("fin", 4, 0), ("cmp", 2), ("fin", 2, 1), ("gat", 4, 0), ("rel", 4, 0), ("gat", 1, 0), ("rel", 1, 0),
-    ("fin", 2, 0), ("fin", 0, 0), ("mixp",), ("gat", 2, 1), ("rel", 2, 1), ("mixs",), ("fin", 0, 1),
-    ("gat", 2, 0), ("gat", 0, 0), ("rel", 2, 0), ("gat", 0, 1), ("final", 1), ("mixf",), ("final", 0),
+    ("F3", 0), ("meta",), ("arr", 0, 0), ("sel", 1, 0), ("F3", 1), ("sel", 4, 0), ("F3", 2), ("sel", 2, 0),
+    ("arr", 0, 3), ("sel", 1, 2), ("arr", 0, 2), ("kvs",), ("arr", 0, 1), ("sel", 4, 1), ("sel", 1, 3),
+    ("sel", 1, 1), ("arr", 1, 0), ("F3", 3), ("sel", 3, 0), ("arr", 4, 0), ("sel", 4, 2), ("cmp", 0),
+    ("arx", 0, 0, 0), ("arr", 1, 2), ("sel", 3, 1), ("sel", 3, 3), ("arr", 4, 1), ("fin", 0, 3),
+    ("sel", 3, 2), ("arr", 1, 3), ("arr", 4, 2), ("arr", 3, 1), ("fin", 0, 0), ("sel", 4, 3), ("arr", 3, 0),
+    ("arr", 3, 2), ("fin", 0, 2), ("arx", 0, 1, 2), ("arr", 3, 3), ("sel", 5, 3), ("cmp", 3),
+    ("arx", 0, 0, 3), ("arr", 4, 3), ("arx", 0, 1, 0), ("sel", 5, 0), ("arx", 0, 0, 2), ("arr", 5, 3),
+    ("fin", 3, 1), ("arx", 0, 1, 3), ("fin", 3, 3), ("arx", 0, 1, 1), ("arx", 0, 0, 1), ("gat", 0, 3),
+    ("sel", 5, 2), ("arr", 5, 0), ("cmp", 6), ("fin", 3, 0), ("gat", 3, 1), ("sel", 5, 1), ("fin", 3, 2),
+    ("fin", 6, 2), ("cmp", 4), ("kvf", 0), ("rel", 3, 1), ("arr", 1, 1), ("arx", 1, 0, 3), ("gat", 3, 3),
+    ("arx", 1, 0, 2), ("arx", 1, 0, 0), ("arx", 1, 1, 0), ("gat", 3, 0), ("arr", 5, 2), ("arr", 5, 1),
+    ("kvf", 1), ("fin", 6, 3), ("arx", 1, 1, 3), ("rel", 3, 0), ("cmp", 1), ("cmp", 5), ("arx", 1, 1, 2),
+    ("arx", 1, 0, 1), ("fin", 4, 2), ("rel", 3, 3), ("gat", 3, 2), ("fin", 6, 1), ("arx", 1, 1, 1),
+    ("rel", 3, 2), ("kvf", 2), ("cmp", 7), ("fin", 4, 3), ("fin", 7, 0), ("sel", 2, 2), ("gat", 4, 2),
+    ("rel", 4, 2), ("fin", 7, 2), ("fin", 7, 3), ("fin", 7, 1), ("fin", 4, 1), ("fin", 1, 3), ("sel", 2, 1),
+    ("gat", 4, 3), ("rel", 4, 3), ("att", 0), ("gat", 4, 1), ("fin", 5, 0), ("rel", 4, 1), ("att", 1),
+    ("fin", 5, 2), ("gat", 5, 0), ("rel", 5, 0), ("sel", 2, 3), ("fin", 6, 0), ("fin", 5, 3), ("mixp",),
+    ("gat", 5, 2), ("rel", 5, 2), ("fin", 5, 1), ("fin", 1, 0), ("gat", 1, 3), ("gat", 0, 0), ("rel", 1, 3),
+    ("arr", 2, 2), ("arr", 2, 1), ("mixs",), ("gat", 5, 3), ("rel", 5, 3), ("arr", 2, 0), ("fin", 4, 0),
+    ("fin", 1, 1), ("arr", 2, 3), ("gat", 5, 1), ("rel", 5, 1), ("fin", 1, 2), ("cmp", 2), ("gat", 4, 0),
+    ("fin", 2, 1), ("fin", 2, 2), ("fin", 2, 3), ("rel", 4, 0), ("fin", 2, 0), ("gat", 1, 0), ("gat", 1, 2),
+    ("gat", 0, 2), ("gat", 1, 1), ("rel", 1, 1), ("gat", 2, 1), ("rel", 2, 1), ("rel", 1, 0), ("gat", 2, 2),
+    ("rel", 2, 2), ("gat", 2, 0), ("gat", 2, 3), ("rel", 2, 0), ("rel", 1, 2), ("fin", 0, 1), ("rel", 2, 3),
+    ("gat", 0, 1), ("mixf",), ("final", 3), ("final", 2), ("final", 0), ("final", 1),
 )
 
 

time: 115 us -> 109 us (0.948)
  Pallas kernels: 110 us -> 104 us
    pallas_call x1, Pallas kernels: 110 us -> 104 us  [fused(): pl.pallas_call(functools.partial(fused_kernel, n), out_shape=(jax.ShapeDt...]
where the time goes in v4:
time: 109 us
  Pallas kernels  104 us (95%)
  local copies, waits for them, and re-layouts  3.63 us (3%)
    pallas_call x1, Pallas kernels, fused(): pl.pallas_call(functools.partial(fused_kernel, n), out_shape=(jax.ShapeDt...  104 us
    unnamed x2, local copies, waits for them, and re-layouts  3.63 us

profile of v4, /device:TPU:0, one launch (start us, length us, event | category | flops | bytes accessed | tf_op | source)
XLA Modules:
  0.0 108.7 jit_solution(1010119280932152938)
XLA Ops:
  0.6 104.5 %shard_map.149 = (bf16[64,4096]{1,0:T(8,128)(2,1)}, bf16[48,4096]{1,0:T(8,128)(2,1)}) custom-call(bf16[64,4096]{1,0:T(8,128)(2,1)} %x_ref.1, f32[1,4096]{1,0:T(1,128)} %bitcast.13, s32[2,64]{1,0:T(2,128)} %bitcast.15, f32[2,64]{1,0:T(2,128)} %bitcast.16, bf16[192,512]{1,0:T(8,128)(2,1)} %q_raw.1, bf16[192,128]{1,0:T(8,128)(2,1)} %k_raw.1, ...), custom_call_target="tpu_custom_call" | custom-call | tf_op jit(solution)/shard_map/pallas_call | solution.py:843
  105.1 1.8 %copy.18 = bf16[48,4096]{1,0:T(8,128)(2,1)} copy(bf16[48,4096]{1,0:T(8,128)(2,1)} %get-tuple-element.8) | data formatting | bytes 786432
  106.9 1.9 %copy.19 = bf16[64,4096]{1,0:T(8,128)(2,1)} copy(bf16[64,4096]{1,0:T(8,128)(2,1)} %get-tuple-element.9) | data formatting | bytes 1048576

commit v5 on v3

--- a/solution.py
+++ b/solution.py
@@ -80,7 +80,7 @@
 
 MESH = pl.DeviceIdType.MESH
 TILE = 1024
-CHUNKS = 2
+CHUNKS = 4
 
 
 def flip(index, pattern, size):
@@ -98,35 +98,58 @@
 
 
 INNER_ORDER = (
-    ("meta",), ("F6", 0), ("arr", 0, 0), ("F5", 0), ("sel", 4, 0), ("F6", 1), ("F3", 0), ("sel", 1, 1),
-    ("sel", 4, 1), ("sel", 5, 0), ("F5", 1), ("sel", 3, 0), ("F3", 1), ("arr", 4, 1), ("sel", 3, 1),
-    ("sel", 1, 0), ("arr", 5, 0), ("arx", 0, 0, 1), ("kvf", 0), ("arr", 0, 1), ("arr", 3, 0), ("F7", 1),
-    ("arr", 4, 0), ("arr", 3, 1), ("F7", 0), ("sel", 5, 1), ("kvs",), ("cmp", 0), ("kvf", 2),
-    ("arx", 0, 1, 0), ("D2", 1), ("arr", 5, 1), ("arx", 1, 0, 0), ("arx", 1, 1, 0), ("cmp", 3), ("fin", 0, 1),
-    ("sel", 2, 1), ("fin", 3, 0), ("cmp", 4), ("arx", 1, 0, 1), ("arx", 1, 1, 1), ("sel", 2, 0),
-    ("arr", 1, 0), ("arx", 0, 1, 1), ("arx", 0, 0, 0), ("fin", 3, 1), ("cmp", 7), ("fin", 7, 1),
-    ("arr", 1, 1), ("kvf", 1), ("cmp", 6), ("cmp", 5), ("fin", 6, 1), ("fin", 7, 0), ("cmp", 1),
-    ("arr", 2, 1), ("fin", 6, 0), ("gat", 3, 1), ("gat", 0, 1), ("att", 0), ("fin", 5, 1), ("gat", 3, 0),
-    ("fin", 1, 1), ("fin", 4, 1), ("rel", 3, 0), ("rel", 3, 1), ("att", 1), ("mixp",), ("fin", 5, 0),
-    ("arr", 2, 0), ("cmp", 2), ("gat", 4, 1), ("rel", 4, 1), ("fin", 1, 0), ("gat", 5, 0), ("mixs",),
-    ("fin", 2, 1), ("gat", 5, 1), ("rel", 5, 1), ("gat", 1, 1), ("gat", 1, 0), ("fin", 0, 0), ("rel", 1, 0),
-    ("fin", 4, 0), ("rel", 5, 0), ("fin", 2, 0), ("gat", 2, 1), ("rel", 2, 1), ("mixf",), ("gat", 0, 0),
-    ("gat", 4, 0), ("gat", 2, 0), ("rel", 2, 0), ("rel", 4, 0), ("rel", 1, 1), ("final", 1), ("final", 0),
+    ("arr", 0, 0), ("F6", 0), ("meta",), ("sel", 4, 0), ("sel", 1, 0), ("F6", 1), ("F5", 0), ("sel", 1, 1),
+    ("arr", 0, 3), ("F6", 2), ("sel", 4, 2), ("sel", 4, 1), ("F5", 1), ("F6", 3), ("sel", 1, 2), ("F3", 1),
+    ("sel", 5, 0), ("F3", 0), ("arr", 4, 0), ("F3", 3), ("arr", 4, 2), ("F5", 3), ("sel", 4, 3),
+    ("sel", 5, 1), ("sel", 2, 3), ("sel", 5, 3), ("sel", 1, 3), ("F3", 2), ("arx", 0, 1, 0), ("F5", 2),
+    ("F7", 1), ("arr", 5, 3), ("sel", 3, 1), ("sel", 2, 0), ("arr", 4, 3), ("F7", 2), ("F7", 3),
+    ("arx", 0, 0, 0), ("arr", 4, 1), ("sel", 3, 0), ("kvf", 0), ("cmp", 4), ("sel", 5, 2), ("sel", 3, 2),
+    ("arx", 1, 0, 0), ("arr", 5, 0), ("arr", 1, 3), ("arr", 1, 2), ("arx", 0, 1, 2), ("arr", 3, 0),
+    ("sel", 2, 1), ("arr", 2, 3), ("sel", 3, 3), ("F7", 0), ("arx", 0, 0, 2), ("arx", 0, 0, 1),
+    ("arx", 1, 1, 3), ("kvs",), ("arx", 0, 1, 3), ("arr", 0, 1), ("arx", 0, 1, 1), ("kvf", 2), ("arr", 1, 0),
+    ("arr", 0, 2), ("arr", 1, 1), ("arx", 0, 0, 3), ("arx", 1, 0, 1), ("arr", 5, 1), ("cmp", 6),
+    ("arr", 5, 2), ("arr", 2, 0), ("cmp", 1), ("fin", 6, 1), ("arr", 3, 3), ("arr", 3, 2), ("fin", 6, 0),
+    ("arx", 1, 0, 3), ("arr", 3, 1), ("arx", 1, 1, 0), ("arx", 1, 1, 1), ("arx", 1, 1, 2), ("cmp", 3),
+    ("arx", 1, 0, 2), ("fin", 6, 3), ("kvf", 1), ("fin", 6, 2), ("cmp", 0), ("fin", 3, 0), ("sel", 2, 2),
+    ("fin", 3, 2), ("fin", 4, 0), ("fin", 1, 3), ("D2", 2), ("cmp", 7), ("D2", 1), ("att", 0), ("D2", 3),
+    ("fin", 7, 1), ("arr", 2, 1), ("fin", 4, 1), ("fin", 3, 1), ("arr", 2, 2), ("cmp", 5), ("fin", 7, 0),
+    ("gat", 3, 2), ("rel", 3, 2), ("gat", 4, 0), ("gat", 3, 0), ("fin", 1, 0), ("fin", 4, 2), ("fin", 3, 3),
+    ("cmp", 2), ("rel", 3, 0), ("fin", 5, 1), ("fin", 7, 3), ("gat", 3, 1), ("fin", 2, 2), ("fin", 7, 2),
+    ("att", 1), ("fin", 2, 1), ("rel", 3, 1), ("rel", 4, 0), ("mixp",), ("fin", 5, 2), ("fin", 4, 3),
+    ("gat", 1, 3), ("gat", 3, 3), ("gat", 4, 2), ("mixs",), ("rel", 4, 2), ("gat", 1, 0), ("fin", 1, 2),
+    ("gat", 5, 2), ("fin", 5, 0), ("fin", 5, 3), ("rel", 5, 2), ("fin", 1, 1), ("gat", 5, 1), ("fin", 2, 0),
+    ("fin", 0, 3), ("rel", 3, 3), ("rel", 5, 1), ("fin", 2, 3), ("gat", 4, 1), ("gat", 5, 3), ("fin", 0, 0),
+    ("gat", 2, 1), ("gat", 4, 3), ("gat", 2, 2), ("rel", 1, 0), ("rel", 2, 2), ("rel", 5, 3), ("gat", 1, 2),
+    ("fin", 0, 2), ("gat", 2, 0), ("gat", 1, 1), ("gat", 5, 0), ("rel", 2, 1), ("rel", 1, 1), ("rel", 1, 2),
+    ("mixf",), ("rel", 1, 3), ("rel", 5, 0), ("rel", 4, 1), ("fin", 0, 1), ("gat", 2, 3), ("rel", 2, 3),
+    ("gat", 0, 1), ("rel", 2, 0), ("rel", 4, 3), ("gat", 0, 3), ("gat", 0, 0), ("gat", 0, 2), ("final", 0),
+    ("final", 3), ("final", 2), ("final", 1),
 )
 OUTER_ORDER = (
-    ("meta",), ("F3", 0), ("sel", 1, 0), ("sel", 1, 1), ("sel", 4, 0), ("F3", 1), ("sel", 2, 0), ("kvs",),
-    ("sel", 4, 1), ("arx", 0, 0, 1), ("arr", 1, 0), ("arr", 4, 1), ("arr", 1, 1), ("sel", 3, 0),
-    ("arr", 0, 1), ("arx", 0, 1, 1), ("arr", 4, 0), ("arr", 3, 0), ("sel", 3, 1), ("sel", 5, 1), ("cmp", 1),
-    ("arx", 0, 0, 0), ("arx", 0, 1, 0), ("arr", 3, 1), ("arr", 5, 1), ("sel", 5, 0), ("cmp", 3), ("cmp", 6),
-    ("arr", 0, 0), ("fin", 3, 0), ("arr", 5, 0), ("fin", 6, 1), ("fin", 3, 1), ("cmp", 0), ("kvf", 0),
-    ("cmp", 4), ("gat", 3, 0), ("arx", 1, 0, 1), ("kvf", 2), ("arx", 1, 1, 1), ("arx", 1, 0, 0),
-    ("arx", 1, 1, 0), ("rel", 3, 0), ("sel", 2, 1), ("cmp", 7), ("gat", 3, 1), ("fin", 7, 1), ("arr", 2, 0),
-    ("rel", 3, 1), ("fin", 7, 0), ("fin", 4, 1), ("arr", 2, 1), ("kvf", 1), ("cmp", 5), ("gat", 4, 1),
-    ("fin", 6, 0), ("rel", 4, 1), ("fin", 5, 1), ("fin", 1, 1), ("att", 0), ("gat", 5, 1), ("rel", 5, 1),
-    ("fin", 5, 0), ("fin", 1, 0), ("att", 1), ("gat", 1, 1), ("rel", 1, 1), ("gat", 5, 0), ("rel", 5, 0),
-    ("fin", 4, 0), ("cmp", 2), ("fin", 2, 1), ("gat", 4, 0), ("rel", 4, 0), ("gat", 1, 0), ("rel", 1, 0),
-    ("fin", 2, 0), ("fin", 0, 0), ("mixp",), ("gat", 2, 1), ("rel", 2, 1), ("mixs",), ("fin", 0, 1),
-    ("gat", 2, 0), ("gat", 0, 0), ("rel", 2, 0), ("gat", 0, 1), ("final", 1), ("mixf",), ("final", 0),
+    ("meta",), ("arr", 0, 1), ("kvs",), ("arr", 0, 0), ("sel", 2, 0), ("sel", 1, 1), ("arr", 0, 3), ("F3", 1),
+    ("sel", 4, 0), ("sel", 4, 1), ("arr", 0, 2), ("sel", 1, 0), ("sel", 1, 2), ("arr", 4, 0), ("sel", 4, 2),
+    ("arr", 4, 1), ("F3", 0), ("cmp", 0), ("F3", 3), ("sel", 4, 3), ("arx", 0, 0, 1), ("fin", 0, 0),
+    ("fin", 0, 1), ("F3", 2), ("arr", 4, 2), ("arx", 0, 1, 1), ("arx", 0, 0, 2), ("arr", 4, 3), ("fin", 0, 2),
+    ("arr", 1, 2), ("arx", 0, 0, 0), ("arx", 0, 0, 3), ("arx", 0, 1, 0), ("sel", 1, 3), ("arx", 0, 1, 2),
+    ("arx", 0, 1, 3), ("sel", 3, 1), ("cmp", 6), ("sel", 3, 0), ("sel", 3, 3), ("fin", 6, 0), ("cmp", 4),
+    ("fin", 6, 2), ("sel", 3, 2), ("arr", 3, 1), ("sel", 5, 1), ("arr", 3, 3), ("arr", 3, 0), ("fin", 4, 0),
+    ("arr", 3, 2), ("sel", 5, 2), ("cmp", 3), ("fin", 4, 2), ("arr", 5, 1), ("sel", 5, 3), ("arx", 1, 0, 1),
+    ("gat", 4, 0), ("rel", 4, 0), ("fin", 3, 2), ("arr", 1, 1), ("arr", 5, 2), ("sel", 5, 0), ("fin", 3, 1),
+    ("gat", 0, 0), ("arx", 1, 1, 1), ("fin", 3, 0), ("arr", 5, 3), ("gat", 4, 2), ("gat", 3, 2),
+    ("fin", 3, 3), ("arx", 1, 0, 2), ("rel", 4, 2), ("arr", 5, 0), ("kvf", 2), ("arx", 1, 0, 0),
+    ("gat", 3, 1), ("arx", 1, 1, 2), ("arx", 1, 0, 3), ("rel", 3, 1), ("fin", 6, 1), ("fin", 6, 3),
+    ("arx", 1, 1, 3), ("arr", 1, 0), ("arr", 1, 3), ("gat", 3, 0), ("kvf", 1), ("kvf", 0), ("rel", 3, 0),
+    ("arx", 1, 1, 0), ("gat", 3, 3), ("rel", 3, 3), ("cmp", 7), ("cmp", 1), ("fin", 4, 1), ("fin", 7, 2),
+    ("fin", 7, 1), ("cmp", 5), ("fin", 7, 3), ("sel", 2, 1), ("fin", 7, 0), ("rel", 3, 2), ("fin", 4, 3),
+    ("fin", 1, 0), ("att", 0), ("gat", 4, 1), ("rel", 4, 1), ("fin", 5, 2), ("sel", 2, 2), ("arr", 2, 0),
+    ("gat", 4, 3), ("rel", 4, 3), ("arr", 2, 1), ("fin", 5, 1), ("sel", 2, 3), ("att", 1), ("gat", 5, 2),
+    ("gat", 1, 0), ("rel", 1, 0), ("rel", 5, 2), ("fin", 5, 3), ("mixp",), ("arr", 2, 2), ("gat", 5, 1),
+    ("fin", 1, 1), ("arr", 2, 3), ("rel", 5, 1), ("gat", 5, 3), ("fin", 5, 0), ("mixs",), ("fin", 1, 2),
+    ("rel", 5, 3), ("cmp", 2), ("fin", 2, 0), ("gat", 5, 0), ("fin", 2, 2), ("fin", 1, 3), ("fin", 0, 3),
+    ("rel", 5, 0), ("gat", 0, 2), ("fin", 2, 3), ("fin", 2, 1), ("gat", 0, 1), ("gat", 2, 0), ("rel", 2, 0),
+    ("gat", 2, 2), ("gat", 1, 2), ("gat", 1, 1), ("rel", 1, 1), ("rel", 2, 2), ("mixf",), ("rel", 1, 2),
+    ("gat", 2, 3), ("rel", 2, 3), ("gat", 2, 1), ("gat", 1, 3), ("rel", 2, 1), ("rel", 1, 3), ("gat", 0, 3),
+    ("final", 2), ("final", 0), ("final", 3), ("final", 1),
 )
 
 
@@ -135,6 +158,22 @@
 
 def fused_kernel(
     n,
+    x_hbm,
+    x_gain_hbm,
+    routes_hbm,
+    weight_hbm,
+    q_hbm,
+    k_hbm,
+    v_hbm,
+    q_gain_hbm,
+    k_gain_hbm,
+    turn_hbm,
+    wg_hbm,
+    wu_hbm,
+    wd_hbm,
+    ow_hbm,
+    moe,
+    mixed,
     x_ref,
     x_gain,
     routes_row,
@@ -144,13 +183,6 @@
     v_raw,
     q_gain,
     k_gain,
-    turn_hbm,
-    wg_hbm,
-    wu_hbm,
-    wd_hbm,
-    ow_hbm,
-    moe,
-    mixed,
     dense,
     meta,
     chosen,
@@ -190,10 +222,10 @@
     row_y,
     row_c,
     row_x,
-    red_sems,
+    red_in,
     sum_x,
     sum_y,
-    t_out,
+    outs,
     z_in,
     m_in,
     p_in,
@@ -241,11 +273,26 @@
     def cols(c):
         return pl.ds(c * part, part)
 
+    far_peers = [(far_inner * 2 + y, t), (far_outer * 2 + y, t)]
+    barrier = pltpu.get_barrier_semaphore()
+    greeted = [x_peer, c_peer, y_peer, z_peer, corner] + far_peers
+    for peer in greeted:
+        pl.semaphore_signal(barrier, inc=1, device_id=peer, device_id_type=MESH)
+
     loads = [
         pltpu.make_async_copy(a, b, load_sem.at[k])
         for k, (a, b) in enumerate(
             [
+                (x_hbm, x_ref),
+                (x_gain_hbm, x_gain),
+                (routes_hbm, routes_row),
+                (weight_hbm, weight_row),
                 (turn_hbm.at[pl.ds(pl.multiple_of(e * tok, 8), tok)], turn),
+                (k_hbm, k_raw),
+                (v_hbm, v_raw),
+                (k_gain_hbm, k_gain),
+                (q_hbm, q_raw),
+                (q_gain_hbm, q_gain),
                 (wg_hbm, wg),
                 (wu_hbm, wu),
                 (wd_hbm, wd),
@@ -256,20 +303,14 @@
     for load in loads:
         load.start()
 
-    far_peers = [(far_inner * 2 + y, t), (far_outer * 2 + y, t)]
-    barrier = pltpu.get_barrier_semaphore()
-    greeted = [x_peer, c_peer, y_peer, z_peer, corner] + far_peers
-    for peer in greeted:
-        pl.semaphore_signal(barrier, inc=1, device_id=peer, device_id_type=MESH)
-
     def kv_z(owner, out, place, device):
-        return remote(kv_all.at[:, owner], kv_all.at[:, owner], kvz_out.at[out], kvz_in.at[place], device)
+        return remote(kv_all.at[:, owner], kv_all.at[:, owner], kvz_out.at[min(out, 1)], kvz_in.at[place], device)
 
     stops = [layer, near, far_inner, far_outer]
 
     def kv_y(j):
         owner = stops[j] * 2 + y
-        return remote(kv_all.at[:, owner], kv_all.at[:, owner], kvy_sems.at[0, j], kvy_sems.at[1, j], y_peer)
+        return remote(kv_all.at[:, owner], kv_all.at[:, owner], kvy_sems.at[0], kvy_sems.at[1], y_peer)
 
     kv_sends = [
         kv_z(e, 0, 0, z_peer),
@@ -283,8 +324,8 @@
         return remote(
             dense.at[source, :, cols(c)],
             dense.at[target, :, cols(c)],
-            dn_out.at[number, c],
-            dn_in.at[target, c],
+            dn_out.at[number // 4],
+            dn_in.at[target - 1, c],
             device,
         )
 
@@ -309,7 +350,7 @@
     far_slot = jnp.where(inner, 4, 5)
 
     def card(slot, number, device):
-        return remote(meta.at[0], meta.at[slot], meta_sems.at[0, number], meta_sems.at[1, slot], device)
+        return remote(meta.at[0], meta.at[slot], meta_sems.at[0], meta_sems.at[1], device)
 
     cards = [
         card(1, 1, x_peer),
@@ -321,19 +362,19 @@
 
     def row_to_y(b, c):
         return remote(
-            y_send.at[b, :, cols(c)], rows.at[b, core, y, :, cols(c)], row_y.at[0, b, c], row_y.at[1, b, c], y_peer
+            y_send.at[b, :, cols(c)], rows.at[b, core, y, :, cols(c)], outs.at[0], row_y.at[b, c], y_peer
         )
 
     def row_to_c(b, g, c):
         here = rows.at[b, core, g, :, cols(c)]
-        return remote(here, here, row_c.at[0, b, g, c], row_c.at[1, b, g, c], c_peer)
+        return remote(here, here, outs.at[1], row_c.at[b], c_peer)
 
     def row_to_x(k, g, c):
         return remote(
             rows.at[4 + k, core, g, :, cols(c)],
             rows.at[6 + k, core, g, :, cols(c)],
-            row_x.at[0, k, g, c],
-            row_x.at[1, k, g, c],
+            outs.at[2],
+            row_x.at[k, g, c],
             x_peer,
         )
 
@@ -341,8 +382,8 @@
         return remote(
             partial.at[b, other_core, :, :, cols(c)],
             red.at[b, :, :, cols(c)],
-            red_sems.at[0, b, c],
-            red_sems.at[1, b, c],
+            outs.at[3],
+            red_in.at[b],
             c_peer,
         )
 
@@ -350,8 +391,8 @@
         return remote(
             partial.at[6 + k, core, :, :, cols(c)],
             x_got.at[k, :, :, cols(c)],
-            sum_x.at[0, k, c],
-            sum_x.at[1, k, c],
+            outs.at[4],
+            sum_x.at[k, c],
             x_peer,
         )
 
@@ -359,13 +400,13 @@
         return remote(
             partial.at[b, core, other_y, :, cols(c)],
             y_got.at[b, :, cols(c)],
-            sum_y.at[0, b, c],
-            sum_y.at[1, b, c],
+            outs.at[5],
+            sum_y.at[b, c],
             y_peer,
         )
 
     def pass_on(b, place, where, arrive, c, device):
-        return remote(sent.at[b, :, cols(c)], where.at[place, :, cols(c)], t_out.at[b, c], arrive.at[place, c], device)
+        return remote(sent.at[b, :, cols(c)], where.at[place, :, cols(c)], outs.at[6], arrive.at[place, c], device)
 
     mix_core = remote(a_part.at[:, other_core], a_red, mix_sems.at[0, 0], mix_sems.at[1, 0], c_peer)
     mix_side = remote(a_send, a_got, mix_sems.at[0, 1], mix_sems.at[1, 1], x_peer)
@@ -380,18 +421,17 @@
             remote(
                 y_send.at[k, :, cols(c)],
                 rows.at[k, core, other_y, :, cols(c)],
-                row_y.at[0, k, c],
-                row_y.at[1, k, c],
+                outs.at[0],
+                row_y.at[k, c],
                 y_peer,
             ).wait_recv()
         elif kind == "rc":
-            g = groups[message[2]]
-            there = rows.at[k, other_core, g, :, cols(c)]
-            remote(there, there, row_c.at[0, k, g, c], row_c.at[1, k, g, c], c_peer).wait_recv()
+            there = rows.at[k, other_core]
+            remote(there, there, outs.at[1], row_c.at[k], c_peer).wait_recv()
         elif kind == "rx":
             row_to_x(k, groups[message[2]], c).wait_recv()
         elif kind == "red":
-            reduce_c(k, c).wait_recv()
+            remote(red.at[k], red.at[k], outs.at[3], red_in.at[k], c_peer).wait_recv()
         elif kind == "xg":
             reduce_x(k, c).wait_recv()
         elif kind == "gy":
@@ -407,10 +447,8 @@
         elif kind == "kvz":
             kv_z(stops[k + 1] * 2 + y, 0, k, z_peer).wait_recv()
         elif kind == "kvy":
-            owner = stops[k] * 2 + other_y
-            remote(
-                kv_all.at[:, owner], kv_all.at[:, owner], kvy_sems.at[0, k], kvy_sems.at[1, k], y_peer
-            ).wait_recv()
+            four = kv_all.at[:, 0:4]
+            remote(four, four, kvy_sems.at[0], kvy_sems.at[1], y_peer).wait_recv()
         elif kind == "mc":
             mix_core.wait_recv()
         else:
@@ -502,7 +540,6 @@
         kind = task[0]
         c = task[-1]
         b = task[1] if len(task) > 1 else 0
-        whole = range(chunks)
         if kind in ("F3", "F6", "F5", "F7"):
             return [("d", {"F3": 1, "F6": 4, "F5": 2, "F7": 5}[kind], c)]
         if kind == "sel":
@@ -512,9 +549,9 @@
         if kind == "arx":
             return [("rx", b, task[2], c)]
         if kind == "cmp":
-            return [("rc", b, g, c) for g in range(2) for c in whole]
+            return [("rc", b, 0)]
         if kind == "fin":
-            return [("red", b, c)] + ([("xg", b - 4, c)] if b in (4, 5) else [])
+            return [("red", b, 0)] + ([("xg", b - 4, c)] if b in (4, 5) else [])
         if kind == "gat":
             return [("gy", b, c)]
         if kind == "rel":
@@ -528,7 +565,7 @@
         if kind == "kvf":
             return [("kvz", b)]
         if kind == "att":
-            return [("kvy", j) for j in range(4)]
+            return [("kvy", 0)]
         return {"mixs": [("mc",)], "mixf": [("mx",)]}.get(kind, [])
 
     def perform(task, is_inner):
@@ -546,8 +583,7 @@
         elif kind == "F7":
             far_to_near(1, c).start()
         elif kind == "meta":
-            for slot in range(1, 6):
-                card(slot, 0, x_peer).wait_recv()
+            remote(meta.at[1:6], meta.at[1:6], meta_sems.at[0], meta_sems.at[1], x_peer).wait_recv()
 
             def run(slot, carry):
                 build(slot)
@@ -619,6 +655,8 @@
             if task[0] not in BIG:
                 perform(task, is_inner)
 
+    for load in loads[:4]:
+        load.wait()
     as_float = f32(x_ref[...])
     mean = jnp.mean(as_float * as_float, axis=1, keepdims=True)
     dense[0] = (as_float * lax.rsqrt(mean + NORM_EPS) * x_gain[...]).astype(jnp.bfloat16)
@@ -647,7 +685,8 @@
     for c in range(chunks):
         select(0, c)
 
-    loads[0].wait()
+    for load in loads[4:10]:
+        load.wait()
     lane = lax.broadcasted_iota(jnp.int32, (tok, 128), 1)
     low = lane < HEAD_DIM
     even = lax.rem(lax.div(lane, HEAD_DIM // 4), 2) == 0
@@ -681,7 +720,7 @@
         q_ref[2 * pair] = jnp.where(low, q_rows, 0.0).astype(jnp.bfloat16)
         q_ref[2 * pair + 1] = jnp.where(low, pltpu.roll(q_rows, HEAD_DIM, 1), 0.0).astype(jnp.bfloat16)
 
-    for load in loads[1:]:
+    for load in loads[10:]:
         load.wait()
 
     def attend(pair):
@@ -756,42 +795,27 @@
 
     mix_core.wait_send()
     mix_side.wait_send()
-    for j in range(4):
-        kv_y(j).wait_send()
+
+    def sent_all(ref, sem):
+        remote(ref, ref, sem, meta_sems.at[1], x_peer).wait_send()
+
+    sent_all(kv_all.at[:, 0:4], kvy_sems.at[0])
     kv_sends[0].wait_send()
-    for item in cards:
-        item.wait_send()
+    sent_all(meta.at[0:5], meta_sems.at[0])
+    sent_all(dense.at[0:3], dn_out.at[0])
 
     @pl.when(inner)
     def _():
-        for item in kv_sends[1:]:
-            item.wait_send()
-
-    for c in range(chunks):
-        to_x(c).wait_send()
-        to_near(c).wait_send()
-        x_to_near(c).wait_send()
-
-        @pl.when(inner)
-        def _():
-            to_across(c).wait_send()
-            near_to_across(c).wait_send()
-            far_to_near(0, c).wait_send()
-            far_to_near(1, c).wait_send()
-
-        for b in range(1, 6):
-            pass_on(b, 0, o_got, o_in, c, x_peer).wait_send()
-        for k in range(2):
-            for g in range(2):
-                row_to_x(k, g, c).wait_send()
-            reduce_x(k, c).wait_send()
-        for b in range(6):
-            row_to_y(b, c).wait_send()
-            give_y(b, c).wait_send()
-        for b in range(8):
-            for g in range(2):
-                row_to_c(b, g, c).wait_send()
-            reduce_c(b, c).wait_send()
+        sent_all(kv_all.at[:, 0:4], kvz_out.at[1])
+        sent_all(dense.at[0:4], dn_out.at[1])
+
+    sent_all(y_send, outs.at[0])
+    sent_all(rows.at[:, core], outs.at[1])
+    sent_all(rows.at[4:6, core], outs.at[2])
+    sent_all(partial.at[:, other_core], outs.at[3])
+    sent_all(partial.at[6:8, core], outs.at[4])
+    sent_all(partial.at[0:6, core, other_y], outs.at[5])
+    sent_all(sent.at[1:6], outs.at[6])
 
 
 def turn_table(tokens):
@@ -820,12 +844,21 @@
     return pl.pallas_call(
         functools.partial(fused_kernel, n),
         out_shape=(
-            jax.ShapeDtypeStruct((tok_exp, width), bf),
-            jax.ShapeDtypeStruct((tok // 4, width), bf),
+            pltpu.VMEM((tok_exp, width), bf),
+            pltpu.VMEM((tok // 4, width), bf),
         ),
-        in_specs=[vmem] * 9 + [anywhere] * 5,
+        in_specs=[anywhere] * 14,
         out_specs=(vmem, vmem),
         scratch_shapes=[
+            pltpu.VMEM((tok_exp, width), bf),
+            pltpu.VMEM((1, width), jnp.float32),
+            pltpu.VMEM((routes.shape[1], tok_exp), jnp.int32),
+            pltpu.VMEM((routes.shape[1], tok_exp), jnp.float32),
+            pltpu.VMEM((tok, heads * HEAD_DIM), bf),
+            pltpu.VMEM((tok, kv_count * HEAD_DIM), bf),
+            pltpu.VMEM((tok, kv_count * HEAD_DIM), bf),
+            pltpu.VMEM((1, heads * HEAD_DIM), jnp.float32),
+            pltpu.VMEM((1, kv_count * HEAD_DIM), jnp.float32),
             pltpu.VMEM((6, tok_exp, width), bf),
             pltpu.VMEM((6, 8, 128), jnp.float32),
             pltpu.VMEM((6, 2 * cap, tok_exp), bf),
@@ -855,20 +888,20 @@
             pltpu.VMEM((2, tok // 4, width), bf),
             pltpu.VMEM((tok // 4, width), bf),
             pltpu.VMEM((tok // 4, width), bf),
-            dma((5,)),
-            dma((5,)),
+            dma((14,)),
+            dma((2,)),
             dma((3,)),
-            dma((2, 4)),
-            dma((8, CHUNKS)),
+            dma((2,)),
+            dma((2,)),
+            dma((5, CHUNKS)),
+            dma((2,)),
             dma((6, CHUNKS)),
-            dma((2, 6)),
-            dma((2, 6, CHUNKS)),
-            dma((2, 8, 2, CHUNKS)),
-            dma((2, 2, 2, CHUNKS)),
-            dma((2, 8, CHUNKS)),
+            dma((8,)),
             dma((2, 2, CHUNKS)),
-            dma((2, 6, CHUNKS)),
+            dma((8,)),
+            dma((2, CHUNKS)),
             dma((6, CHUNKS)),
+            dma((7,)),
             dma((2, CHUNKS)),
             dma((2, CHUNKS)),
             dma((2, CHUNKS)),

time: 115 us -> 100 us (0.87)
  Pallas kernels: 110 us -> 97.8 us
  local copies, waits for them, and re-layouts: 3.63 us -> 1.54 us
    pallas_call x1, Pallas kernels: 110 us -> 97.8 us  [fused(): pl.pallas_call(functools.partial(fused_kernel, n), out_shape=(pltpu.VMEM(...]
    unnamed x2, local copies, waits for them, and re-layouts: 3.63 us -> 1.54 us
where the time goes in v5:
time: 100 us
  Pallas kernels  97.8 us (98%)
  local copies, waits for them, and re-layouts  1.54 us (2%)
    pallas_call x1, Pallas kernels, fused(): pl.pallas_call(functools.partial(fused_kernel, n), out_shape=(pltpu.VMEM(...  97.8 us

profile of v5, /device:TPU:0, one launch (start us, length us, event | category | flops | bytes accessed | tf_op | source)
XLA Modules:
  0.0 100.0 jit_solution(6619251387513496335)
XLA Ops:
  0.6 97.8 %shard_map.149 = (bf16[64,4096]{1,0:T(8,128)(2,1)S(1)}, bf16[48,4096]{1,0:T(8,128)(2,1)S(1)}) custom-call(bf16[64,4096]{1,0:T(8,128)(2,1)} %x_hbm.1, f32[1,4096]{1,0:T(1,128)} %bitcast.13, s32[2,64]{1,0:T(2,128)} %bitcast.15, f32[2,64]{1,0:T(2,128)} %bitcast.16, bf16[192,512]{1,0:T(8,128)(2,1)} %q_hbm.1, bf16[192,128]{1,0:T(8,128)(2,1)} %k_hbm.1, ...), custom_call_target="tpu_custom_call" | custom-call | tf_op jit(solution)/shard_map/pallas_call | solution.py:844
  98.5 0.7 copy.18
  99.2 0.8 copy.19

commit v6 on v5

--- a/solution.py
+++ b/solution.py
@@ -98,58 +98,58 @@
 
 
 INNER_ORDER = (
-    ("arr", 0, 0), ("F6", 0), ("meta",), ("sel", 4, 0), ("sel", 1, 0), ("F6", 1), ("F5", 0), ("sel", 1, 1),
-    ("arr", 0, 3), ("F6", 2), ("sel", 4, 2), ("sel", 4, 1), ("F5", 1), ("F6", 3), ("sel", 1, 2), ("F3", 1),
-    ("sel", 5, 0), ("F3", 0), ("arr", 4, 0), ("F3", 3), ("arr", 4, 2), ("F5", 3), ("sel", 4, 3),
-    ("sel", 5, 1), ("sel", 2, 3), ("sel", 5, 3), ("sel", 1, 3), ("F3", 2), ("arx", 0, 1, 0), ("F5", 2),
-    ("F7", 1), ("arr", 5, 3), ("sel", 3, 1), ("sel", 2, 0), ("arr", 4, 3), ("F7", 2), ("F7", 3),
-    ("arx", 0, 0, 0), ("arr", 4, 1), ("sel", 3, 0), ("kvf", 0), ("cmp", 4), ("sel", 5, 2), ("sel", 3, 2),
-    ("arx", 1, 0, 0), ("arr", 5, 0), ("arr", 1, 3), ("arr", 1, 2), ("arx", 0, 1, 2), ("arr", 3, 0),
-    ("sel", 2, 1), ("arr", 2, 3), ("sel", 3, 3), ("F7", 0), ("arx", 0, 0, 2), ("arx", 0, 0, 1),
-    ("arx", 1, 1, 3), ("kvs",), ("arx", 0, 1, 3), ("arr", 0, 1), ("arx", 0, 1, 1), ("kvf", 2), ("arr", 1, 0),
-    ("arr", 0, 2), ("arr", 1, 1), ("arx", 0, 0, 3), ("arx", 1, 0, 1), ("arr", 5, 1), ("cmp", 6),
-    ("arr", 5, 2), ("arr", 2, 0), ("cmp", 1), ("fin", 6, 1), ("arr", 3, 3), ("arr", 3, 2), ("fin", 6, 0),
-    ("arx", 1, 0, 3), ("arr", 3, 1), ("arx", 1, 1, 0), ("arx", 1, 1, 1), ("arx", 1, 1, 2), ("cmp", 3),
-    ("arx", 1, 0, 2), ("fin", 6, 3), ("kvf", 1), ("fin", 6, 2), ("cmp", 0), ("fin", 3, 0), ("sel", 2, 2),
-    ("fin", 3, 2), ("fin", 4, 0), ("fin", 1, 3), ("D2", 2), ("cmp", 7), ("D2", 1), ("att", 0), ("D2", 3),
-    ("fin", 7, 1), ("arr", 2, 1), ("fin", 4, 1), ("fin", 3, 1), ("arr", 2, 2), ("cmp", 5), ("fin", 7, 0),
-    ("gat", 3, 2), ("rel", 3, 2), ("gat", 4, 0), ("gat", 3, 0), ("fin", 1, 0), ("fin", 4, 2), ("fin", 3, 3),
-    ("cmp", 2), ("rel", 3, 0), ("fin", 5, 1), ("fin", 7, 3), ("gat", 3, 1), ("fin", 2, 2), ("fin", 7, 2),
-    ("att", 1), ("fin", 2, 1), ("rel", 3, 1), ("rel", 4, 0), ("mixp",), ("fin", 5, 2), ("fin", 4, 3),
-    ("gat", 1, 3), ("gat", 3, 3), ("gat", 4, 2), ("mixs",), ("rel", 4, 2), ("gat", 1, 0), ("fin", 1, 2),
-    ("gat", 5, 2), ("fin", 5, 0), ("fin", 5, 3), ("rel", 5, 2), ("fin", 1, 1), ("gat", 5, 1), ("fin", 2, 0),
-    ("fin", 0, 3), ("rel", 3, 3), ("rel", 5, 1), ("fin", 2, 3), ("gat", 4, 1), ("gat", 5, 3), ("fin", 0, 0),
-    ("gat", 2, 1), ("gat", 4, 3), ("gat", 2, 2), ("rel", 1, 0), ("rel", 2, 2), ("rel", 5, 3), ("gat", 1, 2),
-    ("fin", 0, 2), ("gat", 2, 0), ("gat", 1, 1), ("gat", 5, 0), ("rel", 2, 1), ("rel", 1, 1), ("rel", 1, 2),
-    ("mixf",), ("rel", 1, 3), ("rel", 5, 0), ("rel", 4, 1), ("fin", 0, 1), ("gat", 2, 3), ("rel", 2, 3),
-    ("gat", 0, 1), ("rel", 2, 0), ("rel", 4, 3), ("gat", 0, 3), ("gat", 0, 0), ("gat", 0, 2), ("final", 0),
-    ("final", 3), ("final", 2), ("final", 1),
+    ("F6", 0), ("meta",), ("sel", 1, 0), ("sel", 4, 0), ("F6", 1), ("sel", 2, 1), ("sel", 2, 0),
+    ("sel", 4, 1), ("F5", 1), ("arr", 0, 2), ("F6", 2), ("F6", 3), ("F5", 0), ("sel", 4, 3), ("sel", 4, 2),
+    ("F3", 2), ("sel", 2, 3), ("sel", 1, 2), ("sel", 1, 3), ("arx", 0, 0, 0), ("arr", 2, 0), ("F5", 3),
+    ("arr", 4, 2), ("sel", 2, 2), ("F7", 1), ("F3", 1), ("F5", 2), ("arr", 4, 0), ("arr", 2, 1),
+    ("sel", 5, 0), ("sel", 5, 1), ("F3", 3), ("F3", 0), ("sel", 3, 0), ("arx", 1, 0, 0), ("arr", 4, 1),
+    ("arr", 0, 1), ("sel", 5, 2), ("sel", 3, 2), ("arr", 5, 0), ("sel", 5, 3), ("arr", 2, 3), ("arr", 3, 0),
+    ("F7", 3), ("F7", 2), ("arr", 2, 2), ("sel", 1, 1), ("sel", 3, 1), ("F7", 0), ("kvs",), ("arx", 0, 0, 2),
+    ("arr", 5, 2), ("arx", 1, 0, 2), ("arr", 4, 3), ("sel", 3, 3), ("arx", 0, 1, 1), ("kvf", 1),
+    ("arr", 5, 3), ("arx", 1, 0, 3), ("cmp", 4), ("arx", 0, 1, 0), ("arx", 0, 0, 1), ("arx", 0, 1, 3),
+    ("arr", 1, 2), ("cmp", 2), ("arx", 1, 1, 0), ("arr", 0, 0), ("arr", 3, 2), ("fin", 2, 2), ("arr", 3, 1),
+    ("arr", 1, 3), ("arx", 0, 0, 3), ("kvf", 0), ("arr", 3, 3), ("arr", 1, 0), ("arx", 0, 1, 2),
+    ("arr", 5, 1), ("arr", 1, 1), ("cmp", 6), ("arr", 0, 3), ("cmp", 3), ("fin", 2, 3), ("arx", 1, 1, 3),
+    ("arx", 1, 1, 2), ("kvf", 2), ("fin", 6, 3), ("arx", 1, 1, 1), ("fin", 6, 0), ("arx", 1, 0, 1), ("D2", 2),
+    ("cmp", 5), ("fin", 3, 3), ("cmp", 7), ("fin", 4, 3), ("D2", 1), ("fin", 3, 2), ("fin", 3, 1),
+    ("fin", 7, 0), ("fin", 7, 1), ("fin", 3, 0), ("att", 0), ("cmp", 1), ("fin", 7, 3), ("gat", 3, 3),
+    ("fin", 2, 0), ("cmp", 0), ("D2", 3), ("fin", 4, 0), ("gat", 3, 0), ("fin", 6, 2), ("gat", 3, 2),
+    ("fin", 1, 1), ("gat", 3, 1), ("fin", 1, 3), ("fin", 7, 2), ("fin", 2, 1), ("att", 1), ("fin", 5, 1),
+    ("mixp",), ("gat", 4, 0), ("rel", 3, 0), ("rel", 3, 3), ("gat", 4, 3), ("rel", 3, 1), ("fin", 5, 3),
+    ("fin", 0, 0), ("rel", 4, 0), ("rel", 4, 3), ("fin", 6, 1), ("gat", 2, 2), ("fin", 5, 2), ("fin", 1, 0),
+    ("mixs",), ("gat", 1, 1), ("rel", 3, 2), ("gat", 5, 3), ("gat", 1, 3), ("gat", 2, 0), ("fin", 0, 2),
+    ("rel", 5, 3), ("fin", 4, 1), ("fin", 4, 2), ("fin", 5, 0), ("gat", 2, 3), ("rel", 1, 1), ("gat", 5, 2),
+    ("rel", 5, 2), ("gat", 5, 1), ("fin", 0, 1), ("rel", 2, 3), ("rel", 5, 1), ("gat", 1, 0), ("gat", 0, 2),
+    ("gat", 0, 0), ("gat", 2, 1), ("rel", 1, 0), ("gat", 4, 2), ("fin", 1, 2), ("gat", 4, 1), ("gat", 5, 0),
+    ("fin", 0, 3), ("rel", 2, 2), ("rel", 5, 0), ("gat", 0, 1), ("rel", 1, 3), ("rel", 4, 2), ("rel", 4, 1),
+    ("gat", 1, 2), ("rel", 2, 1), ("mixf",), ("gat", 0, 3), ("rel", 1, 2), ("rel", 2, 0), ("final", 0),
+    ("final", 1), ("final", 2), ("final", 3),
 )
 OUTER_ORDER = (
-    ("meta",), ("arr", 0, 1), ("kvs",), ("arr", 0, 0), ("sel", 2, 0), ("sel", 1, 1), ("arr", 0, 3), ("F3", 1),
-    ("sel", 4, 0), ("sel", 4, 1), ("arr", 0, 2), ("sel", 1, 0), ("sel", 1, 2), ("arr", 4, 0), ("sel", 4, 2),
-    ("arr", 4, 1), ("F3", 0), ("cmp", 0), ("F3", 3), ("sel", 4, 3), ("arx", 0, 0, 1), ("fin", 0, 0),
-    ("fin", 0, 1), ("F3", 2), ("arr", 4, 2), ("arx", 0, 1, 1), ("arx", 0, 0, 2), ("arr", 4, 3), ("fin", 0, 2),
-    ("arr", 1, 2), ("arx", 0, 0, 0), ("arx", 0, 0, 3), ("arx", 0, 1, 0), ("sel", 1, 3), ("arx", 0, 1, 2),
-    ("arx", 0, 1, 3), ("sel", 3, 1), ("cmp", 6), ("sel", 3, 0), ("sel", 3, 3), ("fin", 6, 0), ("cmp", 4),
-    ("fin", 6, 2), ("sel", 3, 2), ("arr", 3, 1), ("sel", 5, 1), ("arr", 3, 3), ("arr", 3, 0), ("fin", 4, 0),
-    ("arr", 3, 2), ("sel", 5, 2), ("cmp", 3), ("fin", 4, 2), ("arr", 5, 1), ("sel", 5, 3), ("arx", 1, 0, 1),
-    ("gat", 4, 0), ("rel", 4, 0), ("fin", 3, 2), ("arr", 1, 1), ("arr", 5, 2), ("sel", 5, 0), ("fin", 3, 1),
-    ("gat", 0, 0), ("arx", 1, 1, 1), ("fin", 3, 0), ("arr", 5, 3), ("gat", 4, 2), ("gat", 3, 2),
-    ("fin", 3, 3), ("arx", 1, 0, 2), ("rel", 4, 2), ("arr", 5, 0), ("kvf", 2), ("arx", 1, 0, 0),
-    ("gat", 3, 1), ("arx", 1, 1, 2), ("arx", 1, 0, 3), ("rel", 3, 1), ("fin", 6, 1), ("fin", 6, 3),
-    ("arx", 1, 1, 3), ("arr", 1, 0), ("arr", 1, 3), ("gat", 3, 0), ("kvf", 1), ("kvf", 0), ("rel", 3, 0),
-    ("arx", 1, 1, 0), ("gat", 3, 3), ("rel", 3, 3), ("cmp", 7), ("cmp", 1), ("fin", 4, 1), ("fin", 7, 2),
-    ("fin", 7, 1), ("cmp", 5), ("fin", 7, 3), ("sel", 2, 1), ("fin", 7, 0), ("rel", 3, 2), ("fin", 4, 3),
-    ("fin", 1, 0), ("att", 0), ("gat", 4, 1), ("rel", 4, 1), ("fin", 5, 2), ("sel", 2, 2), ("arr", 2, 0),
-    ("gat", 4, 3), ("rel", 4, 3), ("arr", 2, 1), ("fin", 5, 1), ("sel", 2, 3), ("att", 1), ("gat", 5, 2),
-    ("gat", 1, 0), ("rel", 1, 0), ("rel", 5, 2), ("fin", 5, 3), ("mixp",), ("arr", 2, 2), ("gat", 5, 1),
-    ("fin", 1, 1), ("arr", 2, 3), ("rel", 5, 1), ("gat", 5, 3), ("fin", 5, 0), ("mixs",), ("fin", 1, 2),
-    ("rel", 5, 3), ("cmp", 2), ("fin", 2, 0), ("gat", 5, 0), ("fin", 2, 2), ("fin", 1, 3), ("fin", 0, 3),
-    ("rel", 5, 0), ("gat", 0, 2), ("fin", 2, 3), ("fin", 2, 1), ("gat", 0, 1), ("gat", 2, 0), ("rel", 2, 0),
-    ("gat", 2, 2), ("gat", 1, 2), ("gat", 1, 1), ("rel", 1, 1), ("rel", 2, 2), ("mixf",), ("rel", 1, 2),
-    ("gat", 2, 3), ("rel", 2, 3), ("gat", 2, 1), ("gat", 1, 3), ("rel", 2, 1), ("rel", 1, 3), ("gat", 0, 3),
-    ("final", 2), ("final", 0), ("final", 3), ("final", 1),
+    ("meta",), ("sel", 2, 0), ("kvs",), ("sel", 1, 1), ("arr", 0, 2), ("arr", 0, 0), ("sel", 4, 0),
+    ("arr", 0, 3), ("arr", 0, 1), ("sel", 1, 0), ("sel", 4, 1), ("cmp", 0), ("arr", 4, 0), ("sel", 4, 2),
+    ("F3", 0), ("sel", 1, 3), ("F3", 2), ("arr", 4, 1), ("sel", 4, 3), ("arx", 0, 0, 0), ("arr", 4, 2),
+    ("F3", 1), ("sel", 1, 2), ("arr", 2, 0), ("arx", 0, 1, 0), ("arx", 0, 0, 2), ("sel", 3, 2), ("arr", 4, 3),
+    ("fin", 0, 2), ("arx", 0, 0, 3), ("arx", 0, 1, 2), ("F3", 3), ("arx", 0, 0, 1), ("sel", 5, 1),
+    ("arx", 0, 1, 1), ("fin", 0, 1), ("arx", 0, 1, 3), ("fin", 0, 0), ("cmp", 6), ("arr", 5, 1), ("cmp", 4),
+    ("fin", 6, 0), ("sel", 3, 3), ("sel", 3, 1), ("fin", 6, 1), ("sel", 3, 0), ("arr", 1, 1), ("fin", 6, 3),
+    ("fin", 4, 0), ("sel", 5, 3), ("arr", 3, 1), ("arr", 3, 3), ("arr", 3, 2), ("arr", 3, 0), ("fin", 4, 1),
+    ("gat", 4, 0), ("arr", 1, 3), ("sel", 5, 2), ("cmp", 3), ("fin", 4, 3), ("sel", 5, 0), ("rel", 4, 0),
+    ("gat", 4, 1), ("fin", 3, 1), ("arr", 5, 3), ("fin", 3, 2), ("arr", 1, 0), ("arr", 1, 2), ("kvf", 0),
+    ("rel", 4, 1), ("arr", 5, 2), ("cmp", 1), ("arr", 5, 0), ("arx", 1, 0, 1), ("fin", 3, 3), ("fin", 6, 2),
+    ("gat", 4, 3), ("gat", 0, 0), ("gat", 3, 1), ("rel", 4, 3), ("arx", 1, 0, 3), ("arx", 1, 1, 2),
+    ("gat", 3, 2), ("rel", 3, 1), ("arx", 1, 1, 3), ("arx", 1, 1, 1), ("gat", 0, 1), ("arx", 1, 0, 0),
+    ("arx", 1, 0, 2), ("arx", 1, 1, 0), ("rel", 3, 2), ("kvf", 2), ("kvf", 1), ("cmp", 7), ("cmp", 5),
+    ("fin", 7, 3), ("fin", 4, 2), ("fin", 7, 2), ("gat", 3, 3), ("fin", 7, 1), ("fin", 3, 0), ("rel", 3, 3),
+    ("sel", 2, 1), ("sel", 2, 2), ("att", 0), ("gat", 4, 2), ("rel", 4, 2), ("fin", 5, 3), ("fin", 7, 0),
+    ("gat", 3, 0), ("rel", 3, 0), ("att", 1), ("fin", 5, 2), ("sel", 2, 3), ("mixp",), ("gat", 5, 3),
+    ("arr", 2, 2), ("arr", 2, 1), ("rel", 5, 3), ("fin", 1, 3), ("gat", 0, 2), ("fin", 5, 1), ("fin", 1, 1),
+    ("gat", 5, 2), ("mixs",), ("arr", 2, 3), ("fin", 5, 0), ("rel", 5, 2), ("cmp", 2), ("gat", 1, 3),
+    ("fin", 1, 0), ("gat", 5, 1), ("rel", 5, 1), ("fin", 2, 2), ("gat", 5, 0), ("rel", 5, 0), ("fin", 2, 0),
+    ("gat", 1, 0), ("fin", 2, 1), ("gat", 1, 1), ("fin", 1, 2), ("rel", 1, 1), ("gat", 2, 2), ("fin", 2, 3),
+    ("rel", 2, 2), ("rel", 1, 0), ("gat", 2, 0), ("rel", 2, 0), ("gat", 1, 2), ("rel", 1, 3), ("fin", 0, 3),
+    ("gat", 2, 1), ("rel", 1, 2), ("gat", 2, 3), ("rel", 2, 1), ("rel", 2, 3), ("gat", 0, 3), ("mixf",),
+    ("final", 1), ("final", 2), ("final", 3), ("final", 0),
 )
 
 

time: 100 us -> 99.6 us (level)
  no operation moved by 1% of the time
where the time goes in v6:
time: 99.6 us; the launch traced here: 99.5 us
  Pallas kernels  97.3 us (98%)
  local copies, waits for them, and re-layouts  1.54 us (2%)
    pallas_call x1, Pallas kernels, fused(): pl.pallas_call(functools.partial(fused_kernel, n), out_shape=(pltpu.VMEM(...  97.3 us

profile of v6, /device:TPU:0, one launch (start us, length us, event | category | flops | bytes accessed | tf_op | source)
XLA Modules:
  0.0 99.5 jit_solution(13925427010584004175)
XLA Ops:
  0.6 97.3 %shard_map.149 = (bf16[64,4096]{1,0:T(8,128)(2,1)S(1)}, bf16[48,4096]{1,0:T(8,128)(2,1)S(1)}) custom-call(bf16[64,4096]{1,0:T(8,128)(2,1)} %x_hbm.1, f32[1,4096]{1,0:T(1,128)} %bitcast.13, s32[2,64]{1,0:T(2,128)} %bitcast.15, f32[2,64]{1,0:T(2,128)} %bitcast.16, bf16[192,512]{1,0:T(8,128)(2,1)} %q_hbm.1, bf16[192,128]{1,0:T(8,128)(2,1)} %k_hbm.1, ...), custom_call_target="tpu_custom_call" | custom-call | tf_op jit(solution)/shard_map/pallas_call | solution.py:844
  97.9 0.7 copy.18
  98.7 0.8 copy.19

commit v7 on v6

--- a/solution.py
+++ b/solution.py
@@ -98,58 +98,58 @@
 
 
 INNER_ORDER = (
-    ("F6", 0), ("meta",), ("sel", 1, 0), ("sel", 4, 0), ("F6", 1), ("sel", 2, 1), ("sel", 2, 0),
-    ("sel", 4, 1), ("F5", 1), ("arr", 0, 2), ("F6", 2), ("F6", 3), ("F5", 0), ("sel", 4, 3), ("sel", 4, 2),
-    ("F3", 2), ("sel", 2, 3), ("sel", 1, 2), ("sel", 1, 3), ("arx", 0, 0, 0), ("arr", 2, 0), ("F5", 3),
-    ("arr", 4, 2), ("sel", 2, 2), ("F7", 1), ("F3", 1), ("F5", 2), ("arr", 4, 0), ("arr", 2, 1),
-    ("sel", 5, 0), ("sel", 5, 1), ("F3", 3), ("F3", 0), ("sel", 3, 0), ("arx", 1, 0, 0), ("arr", 4, 1),
-    ("arr", 0, 1), ("sel", 5, 2), ("sel", 3, 2), ("arr", 5, 0), ("sel", 5, 3), ("arr", 2, 3), ("arr", 3, 0),
-    ("F7", 3), ("F7", 2), ("arr", 2, 2), ("sel", 1, 1), ("sel", 3, 1), ("F7", 0), ("kvs",), ("arx", 0, 0, 2),
-    ("arr", 5, 2), ("arx", 1, 0, 2), ("arr", 4, 3), ("sel", 3, 3), ("arx", 0, 1, 1), ("kvf", 1),
-    ("arr", 5, 3), ("arx", 1, 0, 3), ("cmp", 4), ("arx", 0, 1, 0), ("arx", 0, 0, 1), ("arx", 0, 1, 3),
-    ("arr", 1, 2), ("cmp", 2), ("arx", 1, 1, 0), ("arr", 0, 0), ("arr", 3, 2), ("fin", 2, 2), ("arr", 3, 1),
-    ("arr", 1, 3), ("arx", 0, 0, 3), ("kvf", 0), ("arr", 3, 3), ("arr", 1, 0), ("arx", 0, 1, 2),
-    ("arr", 5, 1), ("arr", 1, 1), ("cmp", 6), ("arr", 0, 3), ("cmp", 3), ("fin", 2, 3), ("arx", 1, 1, 3),
-    ("arx", 1, 1, 2), ("kvf", 2), ("fin", 6, 3), ("arx", 1, 1, 1), ("fin", 6, 0), ("arx", 1, 0, 1), ("D2", 2),
-    ("cmp", 5), ("fin", 3, 3), ("cmp", 7), ("fin", 4, 3), ("D2", 1), ("fin", 3, 2), ("fin", 3, 1),
-    ("fin", 7, 0), ("fin", 7, 1), ("fin", 3, 0), ("att", 0), ("cmp", 1), ("fin", 7, 3), ("gat", 3, 3),
-    ("fin", 2, 0), ("cmp", 0), ("D2", 3), ("fin", 4, 0), ("gat", 3, 0), ("fin", 6, 2), ("gat", 3, 2),
-    ("fin", 1, 1), ("gat", 3, 1), ("fin", 1, 3), ("fin", 7, 2), ("fin", 2, 1), ("att", 1), ("fin", 5, 1),
-    ("mixp",), ("gat", 4, 0), ("rel", 3, 0), ("rel", 3, 3), ("gat", 4, 3), ("rel", 3, 1), ("fin", 5, 3),
-    ("fin", 0, 0), ("rel", 4, 0), ("rel", 4, 3), ("fin", 6, 1), ("gat", 2, 2), ("fin", 5, 2), ("fin", 1, 0),
-    ("mixs",), ("gat", 1, 1), ("rel", 3, 2), ("gat", 5, 3), ("gat", 1, 3), ("gat", 2, 0), ("fin", 0, 2),
-    ("rel", 5, 3), ("fin", 4, 1), ("fin", 4, 2), ("fin", 5, 0), ("gat", 2, 3), ("rel", 1, 1), ("gat", 5, 2),
-    ("rel", 5, 2), ("gat", 5, 1), ("fin", 0, 1), ("rel", 2, 3), ("rel", 5, 1), ("gat", 1, 0), ("gat", 0, 2),
-    ("gat", 0, 0), ("gat", 2, 1), ("rel", 1, 0), ("gat", 4, 2), ("fin", 1, 2), ("gat", 4, 1), ("gat", 5, 0),
-    ("fin", 0, 3), ("rel", 2, 2), ("rel", 5, 0), ("gat", 0, 1), ("rel", 1, 3), ("rel", 4, 2), ("rel", 4, 1),
-    ("gat", 1, 2), ("rel", 2, 1), ("mixf",), ("gat", 0, 3), ("rel", 1, 2), ("rel", 2, 0), ("final", 0),
-    ("final", 1), ("final", 2), ("final", 3),
+    ("F6", 0), ("meta",), ("arr", 0, 1), ("sel", 1, 0), ("F6", 1), ("sel", 4, 1), ("sel", 2, 0), ("F6", 2),
+    ("sel", 4, 0), ("F5", 0), ("sel", 1, 1), ("F6", 3), ("sel", 4, 3), ("arr", 4, 0), ("F5", 2), ("F3", 1),
+    ("arr", 0, 2), ("sel", 4, 2), ("arr", 1, 0), ("arx", 0, 0, 0), ("sel", 5, 0), ("F5", 3), ("sel", 1, 3),
+    ("arr", 1, 1), ("arr", 4, 3), ("F3", 2), ("sel", 5, 2), ("sel", 1, 2), ("arr", 0, 3), ("kvf", 0),
+    ("sel", 2, 1), ("arr", 4, 2), ("arr", 1, 3), ("F7", 2), ("arx", 0, 0, 2), ("F3", 3), ("sel", 3, 0),
+    ("F3", 0), ("arx", 0, 0, 1), ("F5", 1), ("F7", 0), ("arr", 2, 0), ("arr", 1, 2), ("F7", 3), ("sel", 3, 1),
+    ("arx", 0, 1, 3), ("arr", 4, 1), ("sel", 5, 3), ("sel", 3, 3), ("arx", 1, 0, 0), ("arx", 0, 1, 1),
+    ("arx", 0, 1, 0), ("arr", 5, 2), ("arx", 0, 0, 3), ("arx", 0, 1, 2), ("sel", 5, 1), ("arr", 3, 1),
+    ("sel", 3, 2), ("cmp", 6), ("sel", 2, 2), ("arr", 5, 3), ("arr", 5, 0), ("arx", 1, 1, 2), ("F7", 1),
+    ("cmp", 1), ("kvf", 2), ("arr", 5, 1), ("arr", 3, 3), ("arr", 3, 2), ("arx", 1, 0, 3), ("arx", 1, 0, 2),
+    ("kvs",), ("fin", 6, 2), ("arx", 1, 0, 1), ("sel", 2, 3), ("arx", 1, 1, 3), ("arr", 3, 0), ("arr", 2, 1),
+    ("cmp", 3), ("fin", 1, 3), ("arr", 0, 0), ("cmp", 4), ("D2", 2), ("arx", 1, 1, 1), ("fin", 1, 1),
+    ("fin", 3, 2), ("fin", 6, 3), ("kvf", 1), ("arr", 2, 2), ("arx", 1, 1, 0), ("fin", 3, 3), ("fin", 6, 1),
+    ("kvg", 0), ("arr", 2, 3), ("kvp",), ("fin", 4, 2), ("cmp", 7), ("cmp", 0), ("gat", 3, 2), ("fin", 7, 3),
+    ("fin", 3, 1), ("fin", 6, 0), ("fin", 3, 0), ("kvg", 1), ("fin", 1, 0), ("cmp", 2), ("kvg", 2),
+    ("fin", 4, 3), ("fin", 0, 0), ("gat", 3, 3), ("gat", 4, 2), ("fin", 7, 2), ("fin", 1, 2), ("att", 0),
+    ("D2", 1), ("fin", 2, 3), ("fin", 0, 3), ("gat", 1, 0), ("cmp", 5), ("att", 1), ("D2", 3), ("rel", 3, 3),
+    ("gat", 1, 2), ("rel", 1, 0), ("gat", 3, 0), ("fin", 2, 0), ("fin", 7, 1), ("gat", 3, 1), ("fin", 5, 2),
+    ("gat", 1, 1), ("gat", 0, 0), ("fin", 2, 1), ("gat", 4, 3), ("gat", 1, 3), ("rel", 4, 2), ("fin", 7, 0),
+    ("gat", 0, 3), ("gat", 2, 1), ("rel", 4, 3), ("fin", 5, 1), ("rel", 3, 1), ("fin", 4, 0), ("mixp",),
+    ("fin", 5, 0), ("rel", 3, 2), ("rel", 1, 2), ("gat", 5, 1), ("fin", 4, 1), ("rel", 3, 0), ("gat", 5, 2),
+    ("rel", 5, 1), ("rel", 1, 3), ("rel", 1, 1), ("mixs",), ("fin", 2, 2), ("fin", 5, 3), ("gat", 5, 0),
+    ("rel", 5, 0), ("fin", 0, 1), ("gat", 4, 0), ("rel", 2, 1), ("rel", 5, 2), ("gat", 4, 1), ("gat", 2, 0),
+    ("rel", 2, 0), ("gat", 5, 3), ("rel", 5, 3), ("fin", 0, 2), ("gat", 2, 2), ("rel", 2, 2), ("rel", 4, 0),
+    ("gat", 0, 2), ("gat", 2, 3), ("rel", 4, 1), ("rel", 2, 3), ("gat", 0, 1), ("mixf",), ("final", 0),
+    ("final", 2), ("final", 1), ("final", 3),
 )
 OUTER_ORDER = (
-    ("meta",), ("sel", 2, 0), ("kvs",), ("sel", 1, 1), ("arr", 0, 2), ("arr", 0, 0), ("sel", 4, 0),
-    ("arr", 0, 3), ("arr", 0, 1), ("sel", 1, 0), ("sel", 4, 1), ("cmp", 0), ("arr", 4, 0), ("sel", 4, 2),
-    ("F3", 0), ("sel", 1, 3), ("F3", 2), ("arr", 4, 1), ("sel", 4, 3), ("arx", 0, 0, 0), ("arr", 4, 2),
-    ("F3", 1), ("sel", 1, 2), ("arr", 2, 0), ("arx", 0, 1, 0), ("arx", 0, 0, 2), ("sel", 3, 2), ("arr", 4, 3),
-    ("fin", 0, 2), ("arx", 0, 0, 3), ("arx", 0, 1, 2), ("F3", 3), ("arx", 0, 0, 1), ("sel", 5, 1),
-    ("arx", 0, 1, 1), ("fin", 0, 1), ("arx", 0, 1, 3), ("fin", 0, 0), ("cmp", 6), ("arr", 5, 1), ("cmp", 4),
-    ("fin", 6, 0), ("sel", 3, 3), ("sel", 3, 1), ("fin", 6, 1), ("sel", 3, 0), ("arr", 1, 1), ("fin", 6, 3),
-    ("fin", 4, 0), ("sel", 5, 3), ("arr", 3, 1), ("arr", 3, 3), ("arr", 3, 2), ("arr", 3, 0), ("fin", 4, 1),
-    ("gat", 4, 0), ("arr", 1, 3), ("sel", 5, 2), ("cmp", 3), ("fin", 4, 3), ("sel", 5, 0), ("rel", 4, 0),
-    ("gat", 4, 1), ("fin", 3, 1), ("arr", 5, 3), ("fin", 3, 2), ("arr", 1, 0), ("arr", 1, 2), ("kvf", 0),
-    ("rel", 4, 1), ("arr", 5, 2), ("cmp", 1), ("arr", 5, 0), ("arx", 1, 0, 1), ("fin", 3, 3), ("fin", 6, 2),
-    ("gat", 4, 3), ("gat", 0, 0), ("gat", 3, 1), ("rel", 4, 3), ("arx", 1, 0, 3), ("arx", 1, 1, 2),
-    ("gat", 3, 2), ("rel", 3, 1), ("arx", 1, 1, 3), ("arx", 1, 1, 1), ("gat", 0, 1), ("arx", 1, 0, 0),
-    ("arx", 1, 0, 2), ("arx", 1, 1, 0), ("rel", 3, 2), ("kvf", 2), ("kvf", 1), ("cmp", 7), ("cmp", 5),
-    ("fin", 7, 3), ("fin", 4, 2), ("fin", 7, 2), ("gat", 3, 3), ("fin", 7, 1), ("fin", 3, 0), ("rel", 3, 3),
-    ("sel", 2, 1), ("sel", 2, 2), ("att", 0), ("gat", 4, 2), ("rel", 4, 2), ("fin", 5, 3), ("fin", 7, 0),
-    ("gat", 3, 0), ("rel", 3, 0), ("att", 1), ("fin", 5, 2), ("sel", 2, 3), ("mixp",), ("gat", 5, 3),
-    ("arr", 2, 2), ("arr", 2, 1), ("rel", 5, 3), ("fin", 1, 3), ("gat", 0, 2), ("fin", 5, 1), ("fin", 1, 1),
-    ("gat", 5, 2), ("mixs",), ("arr", 2, 3), ("fin", 5, 0), ("rel", 5, 2), ("cmp", 2), ("gat", 1, 3),
-    ("fin", 1, 0), ("gat", 5, 1), ("rel", 5, 1), ("fin", 2, 2), ("gat", 5, 0), ("rel", 5, 0), ("fin", 2, 0),
-    ("gat", 1, 0), ("fin", 2, 1), ("gat", 1, 1), ("fin", 1, 2), ("rel", 1, 1), ("gat", 2, 2), ("fin", 2, 3),
-    ("rel", 2, 2), ("rel", 1, 0), ("gat", 2, 0), ("rel", 2, 0), ("gat", 1, 2), ("rel", 1, 3), ("fin", 0, 3),
-    ("gat", 2, 1), ("rel", 1, 2), ("gat", 2, 3), ("rel", 2, 1), ("rel", 2, 3), ("gat", 0, 3), ("mixf",),
-    ("final", 1), ("final", 2), ("final", 3), ("final", 0),
+    ("kvs",), ("arr", 0, 0), ("arr", 0, 1), ("meta",), ("F3", 0), ("sel", 1, 1), ("F3", 1), ("sel", 1, 0),
+    ("F3", 2), ("sel", 4, 0), ("sel", 4, 1), ("arr", 0, 3), ("arx", 0, 0, 0), ("arr", 4, 0), ("arr", 4, 1),
+    ("arx", 0, 0, 1), ("sel", 4, 2), ("arx", 0, 1, 0), ("sel", 4, 3), ("F3", 3), ("arr", 4, 2), ("arr", 4, 3),
+    ("arx", 0, 0, 2), ("sel", 1, 2), ("arx", 0, 0, 3), ("arx", 0, 1, 2), ("arr", 1, 0), ("arx", 0, 1, 1),
+    ("sel", 3, 2), ("arx", 0, 1, 3), ("sel", 2, 0), ("sel", 3, 1), ("sel", 1, 3), ("cmp", 6), ("arr", 3, 2),
+    ("arr", 0, 2), ("sel", 5, 2), ("fin", 6, 1), ("cmp", 4), ("fin", 6, 2), ("arx", 1, 0, 2), ("arr", 1, 1),
+    ("kvp",), ("sel", 3, 3), ("sel", 3, 0), ("cmp", 0), ("fin", 4, 1), ("sel", 5, 0), ("arr", 3, 3),
+    ("arr", 1, 2), ("arr", 3, 1), ("arr", 3, 0), ("fin", 4, 2), ("arr", 5, 2), ("sel", 5, 3), ("cmp", 3),
+    ("gat", 4, 1), ("arr", 5, 0), ("arr", 2, 0), ("arr", 1, 3), ("rel", 4, 1), ("sel", 5, 1), ("arr", 5, 3),
+    ("fin", 3, 0), ("arx", 1, 0, 3), ("arx", 1, 1, 2), ("gat", 4, 2), ("fin", 3, 3), ("rel", 4, 2),
+    ("cmp", 1), ("arr", 5, 1), ("arx", 1, 0, 1), ("fin", 3, 1), ("fin", 6, 3), ("fin", 6, 0), ("fin", 3, 2),
+    ("gat", 3, 0), ("rel", 3, 0), ("arx", 1, 1, 0), ("arx", 1, 1, 3), ("kvf", 0), ("arx", 1, 0, 0),
+    ("arx", 1, 1, 1), ("gat", 3, 3), ("gat", 3, 1), ("rel", 3, 1), ("rel", 3, 3), ("fin", 1, 1), ("cmp", 7),
+    ("fin", 4, 3), ("cmp", 5), ("fin", 7, 1), ("gat", 3, 2), ("fin", 4, 0), ("fin", 1, 3), ("rel", 3, 2),
+    ("fin", 7, 0), ("sel", 2, 2), ("att", 0), ("gat", 4, 3), ("gat", 4, 0), ("rel", 4, 3), ("fin", 7, 2),
+    ("sel", 2, 1), ("rel", 4, 0), ("fin", 7, 3), ("fin", 5, 1), ("att", 1), ("fin", 5, 0), ("sel", 2, 3),
+    ("arr", 2, 2), ("fin", 1, 2), ("mixp",), ("gat", 5, 1), ("rel", 5, 1), ("fin", 5, 2), ("gat", 1, 3),
+    ("rel", 1, 3), ("mixs",), ("gat", 5, 0), ("arr", 2, 3), ("rel", 5, 0), ("arr", 2, 1), ("fin", 5, 3),
+    ("cmp", 2), ("fin", 1, 0), ("gat", 5, 2), ("rel", 5, 2), ("fin", 2, 2), ("fin", 2, 0), ("gat", 1, 1),
+    ("gat", 1, 2), ("fin", 2, 1), ("fin", 0, 0), ("gat", 5, 3), ("fin", 0, 2), ("rel", 5, 3), ("fin", 0, 1),
+    ("fin", 2, 3), ("rel", 1, 1), ("gat", 2, 2), ("rel", 2, 2), ("gat", 2, 1), ("gat", 1, 0), ("rel", 1, 0),
+    ("rel", 2, 1), ("fin", 0, 3), ("gat", 2, 0), ("rel", 1, 2), ("rel", 2, 0), ("gat", 0, 2), ("gat", 0, 0),
+    ("gat", 2, 3), ("rel", 2, 3), ("gat", 0, 3), ("gat", 0, 1), ("mixf",), ("final", 0), ("final", 3),
+    ("final", 1), ("final", 2),
 )
 
 
@@ -303,22 +303,17 @@
     for load in loads:
         load.start()
 
-    def kv_z(owner, out, place, device):
-        return remote(kv_all.at[:, owner], kv_all.at[:, owner], kvz_out.at[min(out, 1)], kvz_in.at[place], device)
-
     stops = [layer, near, far_inner, far_outer]
 
+    def kv_move(owner, out, arrive, device):
+        return remote(kv_all.at[:, owner], kv_all.at[:, owner], out, arrive, device)
+
+    def kv_hop(stop, column, place, device):
+        first = 0 if stop == 0 and column == 0 and place == 0 else 1
+        return kv_move(stops[stop] * 2 + (y, other_y)[column], kvz_out.at[first], kvz_in.at[column, place], device)
+
     def kv_y(j):
-        owner = stops[j] * 2 + y
-        return remote(kv_all.at[:, owner], kv_all.at[:, owner], kvy_sems.at[0], kvy_sems.at[1], y_peer)
-
-    kv_sends = [
-        kv_z(e, 0, 0, z_peer),
-        kv_z(e, 1, 1, m_peer),
-        kv_z(near * 2 + y, 2, 2, m_peer),
-        kv_z(far_inner * 2 + y, 3, 1, z_peer),
-        kv_z(far_outer * 2 + y, 4, 2, z_peer),
-    ]
+        return kv_move(stops[j] * 2 + y, kvy_sems.at[0, 0], kvy_sems.at[1, j], y_peer)
 
     def block(source, target, number, c, device):
         return remote(
@@ -445,10 +440,11 @@
         elif kind == "og":
             pass_on(1, 0, o_got, o_in, c, z_peer).wait_recv()
         elif kind == "kvz":
-            kv_z(stops[k + 1] * 2 + y, 0, k, z_peer).wait_recv()
+            kv_hop(k + 1, 0, k, z_peer).wait_recv()
+        elif kind == "kvw":
+            kv_hop(k + 1, 1, k, z_peer).wait_recv()
         elif kind == "kvy":
-            four = kv_all.at[:, 0:4]
-            remote(four, four, kvy_sems.at[0], kvy_sems.at[1], y_peer).wait_recv()
+            kv_move(stops[k] * 2 + other_y, kvy_sems.at[0, 0], kvy_sems.at[1, k], y_peer).wait_recv()
         elif kind == "mc":
             mix_core.wait_recv()
         else:
@@ -564,8 +560,12 @@
             return [("og", c), ("pg", 0, c)] + ([("mg", 0, c)] if is_inner else [])
         if kind == "kvf":
             return [("kvz", b)]
+        if kind == "kvp":
+            return [("kvy", 0)]
+        if kind == "kvg":
+            return [("kvw", b)]
         if kind == "att":
-            return [("kvy", 0)]
+            return [] if is_inner else [("kvz", 1), ("kvz", 2), ("kvw", 1), ("kvw", 2), ("kvy", 1)]
         return {"mixs": [("mc",)], "mixf": [("mx",)]}.get(kind, [])
 
     def perform(task, is_inner):
@@ -622,14 +622,23 @@
 
             tiles(c, body)
         elif kind == "kvs":
-            kv_sends[0].start()
+            kv_hop(0, 0, 0, z_peer).start()
             if is_inner:
-                kv_sends[1].start()
+                kv_hop(0, 0, 1, m_peer).start()
             kv_y(0).start()
-        elif kind == "kvf":
+        elif kind == "kvp":
             if is_inner:
-                kv_sends[2 + b].start()
-            kv_y(b + 1).start()
+                kv_hop(0, 1, 1, m_peer).start()
+            else:
+                kv_hop(0, 1, 0, z_peer).start()
+        elif kind in ("kvf", "kvg"):
+            column = int(kind == "kvg")
+            if not is_inner:
+                kv_y(1).start()
+            elif b == 0:
+                kv_hop(1, column, 2, m_peer).start()
+            else:
+                kv_hop(1 + b, column, b, z_peer).start()
         elif kind == "mixs":
             a_send[...] = (f32(a_part[other_side, core]) + f32(a_red[other_side])).astype(jnp.bfloat16)
             mix_side.start()
@@ -799,15 +808,20 @@
     def sent_all(ref, sem):
         remote(ref, ref, sem, meta_sems.at[1], x_peer).wait_send()
 
-    sent_all(kv_all.at[:, 0:4], kvy_sems.at[0])
-    kv_sends[0].wait_send()
+    sent_all(kv_all.at[:, 0], kvz_out.at[0])
     sent_all(meta.at[0:5], meta_sems.at[0])
     sent_all(dense.at[0:3], dn_out.at[0])
 
     @pl.when(inner)
     def _():
-        sent_all(kv_all.at[:, 0:4], kvz_out.at[1])
+        sent_all(kv_all.at[:, 0], kvy_sems.at[0, 0])
+        sent_all(kv_all, kvz_out.at[1])
         sent_all(dense.at[0:4], dn_out.at[1])
+
+    @pl.when(outer)
+    def _():
+        sent_all(kv_all.at[:, 0:2], kvy_sems.at[0, 0])
+        sent_all(kv_all.at[:, 0], kvz_out.at[1])
 
     sent_all(y_send, outs.at[0])
     sent_all(rows.at[:, core], outs.at[1])
@@ -890,8 +904,8 @@
             pltpu.VMEM((tok // 4, width), bf),
             dma((14,)),
             dma((2,)),
-            dma((3,)),
-            dma((2,)),
+            dma((2, 3)),
+            dma((2, 2)),
             dma((2,)),
             dma((5, CHUNKS)),
             dma((2,)),

time: 99.6 us -> 98.5 us (0.989)
  Pallas kernels: 97.3 us -> 96.1 us
    pallas_call x1, Pallas kernels: 97.3 us -> 96.1 us  [fused(): pl.pallas_call(functools.partial(fused_kernel, n), out_shape=(pltpu.VMEM(...]
where the time goes in v7:
time: 98.5 us; the launch traced here: 98.3 us
  Pallas kernels  96.1 us (98%)
  local copies, waits for them, and re-layouts  1.54 us (2%)
    pallas_call x1, Pallas kernels, fused(): pl.pallas_call(functools.partial(fused_kernel, n), out_shape=(pltpu.VMEM(...  96.1 us

profile of v7, /device:TPU:0, one launch (start us, length us, event | category | flops | bytes accessed | tf_op | source)
XLA Modules:
  0.0 98.3 jit_solution(17336991281284660617)
XLA Ops:
  0.6 96.1 %shard_map.149 = (bf16[64,4096]{1,0:T(8,128)(2,1)S(1)}, bf16[48,4096]{1,0:T(8,128)(2,1)S(1)}) custom-call(bf16[64,4096]{1,0:T(8,128)(2,1)} %x_hbm.1, f32[1,4096]{1,0:T(1,128)} %bitcast.13, s32[2,64]{1,0:T(2,128)} %bitcast.15, f32[2,64]{1,0:T(2,128)} %bitcast.16, bf16[192,512]{1,0:T(8,128)(2,1)} %q_hbm.1, bf16[192,128]{1,0:T(8,128)(2,1)} %k_hbm.1, ...), custom_call_target="tpu_custom_call" | custom-call | tf_op jit(solution)/shard_map/pallas_call | solution.py:858
  96.8 0.7 copy.18
  97.5 0.8 copy.19
